TPU v7x, 32 devices: a whole 2x2x4 slice. The times are simulated.
32 devices in a mesh: tp: 4 (over y, x), dp: 8 (over z, core).
Axes of the slice: x: 2, y: 2, z: 4, core: 2. Of those that a mesh axis runs over, the one named last changes fastest.
Arguments:
- tokens: bfloat16 [64, 4096], P('tp', 'dp'), may hold values from -12 to 12, as said below
- norm_gain: float32 [2, 4096], P(None, 'dp'), may hold values from 0.1 to 1.9
- w_input: bfloat16 [2, 4096, 2048], P(None, 'dp', 'tp'), may hold values from -0.09375 to 0.09375
- w_gate: bfloat16 [2, 4096, 2048], P(None, 'dp', 'tp'), may hold values from -0.09375 to 0.09375
- w_recur: bfloat16 [2, 16, 128, 128], P(None, 'tp'), may hold values from -0.5 to 0.5
- w_inject: bfloat16 [2, 16, 128, 128], P(None, 'tp'), may hold values from -0.5 to 0.5
- conv_weight: bfloat16 [2, 4, 2048], P(None, None, 'tp'), may hold values from -3 to 3
- decay_param: float32 [2, 2048], P(None, 'tp'), may hold values from -2 to 5
- w_output: bfloat16 [2, 2048, 4096], P(None, 'tp', 'dp'), may hold values from -0.125 to 0.125
- lengths: int32 [64], P('dp'), may hold values from 1 to 48, 512 in all
- conv_state: bfloat16 [2, 3, 64, 2048], P(None, None, 'dp', 'tp'), may hold values from -6 to 6
- rec_state: float32 [2, 64, 2048], P(None, 'dp', 'tp'), may hold values from -6 to 6
Outputs:
- mixed: bfloat16 [64, 4096], P('tp', 'dp')
- new_conv: bfloat16 [2, 3, 64, 2048], P(None, None, 'dp', 'tp')
- new_rec: float32 [2, 64, 2048], P(None, 'dp', 'tp')
Inputs may be any that keep to these rules, and one draw needn't show every extreme that they name: `tokens`: activations; feature scales vary.
All inputs are finite; a program needn't handle non-finite values. No bound on the sum of `lengths` on one device may be relied on, other than what follows from the above.
Results may differ from a plain program's by a relative error of at most 0.02.
Values may be sent and summed in bfloat16 or wider, within the bound.
No kernel may reach another device: no remote copies, remote signals or barrier semaphores. Data moves between devices by JAX's collectives and lax.ppermute only.
A program may use at most 64 MiB of HBM per device.

v0:
```python
import functools

import jax
import jax.numpy as jnp
from jax import lax
from jax.experimental import pallas as pl
from jax.experimental.pallas import tpu as pltpu
from jax.sharding import PartitionSpec as P


EPS = 1e-06
F32 = jnp.float32
BF16 = jnp.bfloat16

COVER = 1 << 31


def call(kernel, outs, *args, scratch=(), flops=1000000, limit=8):
    single = not isinstance(outs, (list, tuple))
    spec = pl.BlockSpec(memory_space=pltpu.VMEM)
    return pl.pallas_call(
        kernel,
        out_shape=outs,
        in_specs=[spec] * len(args),
        out_specs=spec if single else [spec] * len(outs),
        scratch_shapes=list(scratch),
        compiler_params=pltpu.CompilerParams(vmem_limit_bytes=limit << 20),
        cost_estimate=pl.CostEstimate(flops=flops, bytes_accessed=1 << 20, transcendentals=0),
    )(*args)


def shape(dims, dtype):
    return jax.ShapeDtypeStruct(tuple(dims), dtype)


class Layout:
    def __init__(self, batch, tp, dp):
        self.batch, self.tp, self.dp = batch, tp, dp
        self.rows = batch // dp
        self.half = batch // 2
        self.per_tp = batch // tp
        self.chunks = self.per_tp // self.rows

    def place(self, chunk, z, core):
        side = jnp.where(lax.rem(chunk, 2) == core, 0, self.half)
        return pl.multiple_of(side + ((chunk // 2) ^ z) * self.rows, self.rows)


def mesh_place():
    core = lax.rem(lax.axis_index("dp"), 2)
    return lax.axis_index("tp"), lax.axis_index("dp") // 2, core


def partner_exchange(value, axis, masks):
    count = lax.axis_size(axis)
    return [lax.ppermute(value, axis, [(i, i ^ m) for i in range(count)]) for m in masks]


def doubling(value, axis, masks):
    stack = value[None]
    for mask in masks:
        (got,) = partner_exchange(stack, axis, [mask])
        if mask == masks[-1]:
            return [stack, got]
        stack = call(join_kernel, shape((2 * stack.shape[0],) + stack.shape[1:], stack.dtype), stack, got)


def join_kernel(first_ref, second_ref, out_ref):
    half = first_ref.shape[0]
    out_ref[:half] = first_ref[...]
    out_ref[half:] = second_ref[...]


def entry(stacks, m):
    size = stacks[0].shape[0]
    return stacks[m // size][m % size]


def as_column(row):
    n = row.shape[1]
    eye = lax.broadcasted_iota(jnp.int32, (n, n), 0) == lax.broadcasted_iota(jnp.int32, (n, n), 1)
    return jnp.sum(jnp.where(eye, jnp.broadcast_to(row, (n, n)), 0), axis=1, keepdims=True)


def length_kernel(lengths_ref, out_ref):
    out_ref[...] = jnp.broadcast_to(as_column(lengths_ref[...]), out_ref.shape)


def state_kernel(lengths_ref, taps_ref, conv_ref, rec_ref, out_ref):
    live = lengths_ref[:, 0:1]
    depth = conv_ref.shape[1]
    for layer in range(conv_ref.shape[0]):
        old = jnp.zeros(rec_ref.shape[1:], F32)
        for back in range(1, depth + 1):
            tap = taps_ref[layer, depth - back : depth - back + 1, :].astype(F32)
            old = old + tap * jnp.where(back < live, conv_ref[layer, depth - back].astype(F32), 0.0)
        out_ref[layer, 0] = old
        out_ref[layer, 1] = jnp.where(live > 1, rec_ref[layer], 0.0)


LANES = 128
GROUP = 8


def packed_rows(rows, width):
    return 2 * (width // LANES) * rows + GROUP


def pack(ref, value, gate, square):
    rows, width = value.shape
    count = width // LANES
    for k, block in enumerate((value, gate)):
        for b in range(count):
            start = (k * count + b) * rows
            ref[start : start + rows, :] = block[:, b * LANES : (b + 1) * LANES].astype(ref.dtype)
    high = square.astype(BF16).astype(F32)
    low = square - high
    lane = lax.broadcasted_iota(jnp.int32, (GROUP, LANES), 1)
    tile = jnp.zeros((GROUP, LANES), F32)
    for g in range(rows // GROUP):
        part = slice(g * GROUP, (g + 1) * GROUP)
        tile = jnp.where(lane == g, high[part], jnp.where(lane == g + LANES // 2, low[part], tile))
    ref[2 * count * rows :, :] = tile.astype(ref.dtype)


def unpack(total, rows, width):
    count = width // LANES
    blocks = [total[b * rows : (b + 1) * rows] for b in range(2 * count)]
    value = jnp.concatenate(blocks[:count], axis=1)
    gate = jnp.concatenate(blocks[count:], axis=1)
    tile = total[2 * count * rows :]
    half = LANES // 2
    square = jnp.concatenate(
        [tile[:, g : g + 1] + tile[:, g + half : g + half + 1] for g in range(rows // GROUP)], axis=0
    )
    return value, gate, square


def by_owner(part, mask, zs, size):
    return jnp.concatenate([part[(m ^ mask) * size : ((m ^ mask) + 1) * size] for m in range(zs)], axis=0)


def project(x, gain, wi, wg, keep_ref, send_ref):
    half = x.shape[0] // 2
    square = jnp.sum(x * x, axis=1, keepdims=True)
    scaled = (x * gain).astype(BF16)
    value = jnp.dot(scaled, wi, preferred_element_type=F32)
    gate = jnp.dot(scaled, wg, preferred_element_type=F32)
    pack(keep_ref, value[:half], gate[:half], square[:half])
    pack(send_ref, value[half:], gate[half:], square[half:])


def first_kernel(lay, low_ref, high_ref, gain_ref, wi_ref, wg_ref, x_ref, keep_ref, send_ref):
    me, z, core = mesh_place()
    for mask in range(lay.tp):
        owner = me ^ mask
        rows = entry((low_ref, high_ref), mask).astype(F32)
        for i in range(lay.chunks):
            start = lay.place(owner * lay.chunks + i, z, core)
            x_ref[pl.ds(start, lay.rows), :] = rows[i * lay.rows : (i + 1) * lay.rows]
    project(x_ref[...], gain_ref[0:1, :], wi_ref[0], wg_ref[0], keep_ref, send_ref)


def next_kernel(lay, layer, x_old_ref, *refs):
    parts, (gain_ref, wi_ref, wg_ref, x_ref, keep_ref, send_ref) = refs[: lay.tp], refs[lay.tp :]
    total = parts[0][...].astype(F32)
    for part in parts[1:]:
        total = total + part[...].astype(F32)
    x = (x_old_ref[...] + total).astype(BF16).astype(F32)
    x_ref[...] = x
    project(x, gain_ref[layer : layer + 1, :], wi_ref[layer], wg_ref[layer], keep_ref, send_ref)


def one_minus_exp(u):
    series = 1.0 + u * (1.0 / 6.0)
    for k in (5.0, 4.0, 3.0, 2.0):
        series = 1.0 + u * (1.0 / k) * series
    return jnp.where(u > -0.25, -u * series, 1.0 - jnp.exp(u))


def add_kernel(keep_ref, got_ref, out_ref):
    out_ref[...] = (keep_ref[...] + got_ref[...].astype(F32)).astype(out_ref.dtype)


def recurrence_kernel(lay, layer, features, *refs):
    zs = lay.dp // 2
    sums, refs = refs[:zs], refs[zs:]
    low_ref, high_ref, taps_ref, decay_ref, wr_ref, wj_ref, readout_ref, value_ref, rec_ref = refs
    rows, half, width = lay.rows, lay.half, taps_ref.shape[2]
    states = [entry((low_ref, high_ref), m) for m in range(zs)]
    old = jnp.concatenate([state[layer, 0] for state in states], axis=0)
    previous = jnp.concatenate([state[layer, 1] for state in states], axis=0)
    value_in = gate_in = square = None
    for mask, part in enumerate(sums):
        terms = [by_owner(t, mask, zs, rows) for t in unpack(part[...].astype(F32), half, width)]
        if mask == 0:
            value_in, gate_in, square = terms
        else:
            value_in, gate_in, square = value_in + terms[0], gate_in + terms[1], square + terms[2]
    scale = lax.rsqrt(square / features + EPS)
    value_in = value_in * scale
    gate_in = gate_in * scale
    last = taps_ref.shape[1] - 1
    conv_out = taps_ref[layer, last : last + 1, :].astype(F32) * value_in + old
    conv_low = conv_out.astype(BF16)
    blocks, block = wr_ref.shape[1], wr_ref.shape[2]

    def mapped(ref):
        return jnp.concatenate(
            [
                jnp.dot(conv_low[:, b * block : (b + 1) * block], ref[layer, b], preferred_element_type=F32)
                for b in range(blocks)
            ],
            axis=1,
        )

    rec_gate = jax.nn.sigmoid(mapped(wr_ref))
    inp_gate = jax.nn.sigmoid(mapped(wj_ref))
    log_decay = -8.0 * rec_gate * jax.nn.softplus(-decay_ref[layer : layer + 1, :])
    hidden = jnp.exp(log_decay) * previous + jnp.sqrt(one_minus_exp(2.0 * log_decay)) * (inp_gate * conv_out)
    readout_ref[...] = (hidden * jax.nn.gelu(gate_in)).astype(BF16)
    value_ref[...] = value_in[:rows].astype(BF16)
    rec_ref[...] = hidden[:rows]


def output_kernel(layer, own_ref, other_ref, w_ref, out_ref):
    half = own_ref.shape[0]
    out_ref[:half] = jnp.dot(own_ref[...], w_ref[layer], preferred_element_type=F32).astype(BF16)
    out_ref[half:] = jnp.dot(other_ref[...], w_ref[layer], preferred_element_type=F32).astype(BF16)


def last_output_kernel(lay, layer, own_ref, other_ref, w_ref, x_ref, *refs):
    mine_ref, outs, held = refs[0], refs[1:-1], refs[-1]
    half = own_ref.shape[0]
    held[:half] = jnp.dot(own_ref[...], w_ref[layer], preferred_element_type=F32)
    held[half:] = jnp.dot(other_ref[...], w_ref[layer], preferred_element_type=F32)
    me, z, core = mesh_place()
    for mask, out in enumerate((mine_ref,) + tuple(outs)):
        for i in range(lay.chunks):
            start = lay.place((me ^ mask) * lay.chunks + i, z, core)
            piece = held[pl.ds(start, lay.rows), :]
            if mask == 0:
                piece = piece + x_ref[pl.ds(start, lay.rows), :]
            out[i * lay.rows : (i + 1) * lay.rows, :] = piece.astype(out.dtype)


def final_kernel(own_ref, *refs):
    parts, out_ref = refs[:-1], refs[-1]
    total = own_ref[...]
    for part in parts:
        total = total + part[...].astype(F32)
    out_ref[...] = total.astype(BF16)


def blocks(
    tokens,
    norm_gain,
    w_input,
    w_gate,
    w_recur,
    w_inject,
    conv_weight,
    decay_param,
    w_output,
    lengths,
    conv_state,
    rec_state,
):
    tp, dp = lax.axis_size("tp"), lax.axis_size("dp")
    lay = Layout(tokens.shape[0] * tp, tp, dp)
    depth, features = tokens.shape[1], tokens.shape[1] * dp
    width = rec_state.shape[2]
    half, batch = lay.half, lay.batch
    layers = w_input.shape[0]

    tp_masks = range(1, tp)
    z_masks = [2 * k for k in range(1, dp // 2)]

    tall = packed_rows(half, width)
    bits = lambda n: [1 << k for k in range(n.bit_length() - 1)]
    live = call(length_kernel, shape((lay.rows, LANES), jnp.int32), lengths[None, :], flops=COVER)
    state = call(
        state_kernel,
        shape((layers, 2, lay.rows, width), F32),
        live,
        conv_weight,
        conv_state,
        rec_state,
    )
    rows = doubling(tokens, "tp", bits(tp))
    states = doubling(state, "dp", [2 * m for m in bits(dp // 2)])
    parts = None
    conv_list, rec_list = [], []
    x = None
    for layer in range(layers):
        outs = [shape((batch, depth), F32), shape((tall, LANES), F32), shape((tall, LANES), BF16)]
        weights = (norm_gain, w_input, w_gate)
        if layer == 0:
            x, keep, send = call(functools.partial(first_kernel, lay), outs, *rows, *weights)
        else:
            x, keep, send = call(functools.partial(next_kernel, lay, layer), outs, x, *parts, *weights)
        (got,) = partner_exchange(send, "dp", [1])
        summed = call(add_kernel, shape((tall, LANES), BF16), keep, got)
        readout, value, hidden = call(
            functools.partial(recurrence_kernel, lay, layer, features),
            [
                shape((half, width), BF16),
                shape((lay.rows, width), BF16),
                shape((lay.rows, width), F32),
            ],
            summed,
            *partner_exchange(summed, "dp", z_masks),
            *states,
            conv_weight,
            decay_param,
            w_recur,
            w_inject,
        )
        (other,) = partner_exchange(readout, "dp", [1])
        if layer < layers - 1:
            partial = call(
                functools.partial(output_kernel, layer), shape((batch, depth), BF16), readout, other, w_output
            )
            parts = [partial] + partner_exchange(partial, "tp", tp_masks)
        else:
            own, *pieces = call(
                functools.partial(last_output_kernel, lay, layer),
                [shape((lay.per_tp, depth), F32)] + [shape((lay.per_tp, depth), BF16)] * (tp - 1),
                readout,
                other,
                w_output,
                x,
                scratch=[pltpu.VMEM((batch, depth), F32)],
            )
            parts = [own] + [partner_exchange(p, "tp", [m])[0] for p, m in zip(pieces, tp_masks)]
        conv_list.append(jnp.concatenate([conv_state[layer, 1:], value[None]], axis=0))
        rec_list.append(hidden)
    mixed = call(final_kernel, shape((lay.per_tp, depth), BF16), *parts)
    return mixed, jnp.stack(conv_list), jnp.stack(rec_list)


def solution(mesh):
    placed = (
        P("tp", "dp"),
        P(None, "dp"),
        P(None, "dp", "tp"),
        P(None, "dp", "tp"),
        P(None, "tp", None, None),
        P(None, "tp", None, None),
        P(None, None, "tp"),
        P(None, "tp"),
        P(None, "tp", "dp"),
        P("dp"),
        P(None, None, "dp", "tp"),
        P(None, "dp", "tp"),
    )
    return jax.shard_map(
        blocks,
        mesh=mesh,
        in_specs=placed,
        out_specs=(P("tp", "dp"), P(None, None, "dp", "tp"), P(None, "dp", "tp")),
        check_vma=False,
    )
```

profile of v0, /device:TPU:0, one launch (start us, length us, event | category | flops | bytes accessed | tf_op | source)
XLA Modules:
  0.0 58.8 jit_solution(18102236493057259029)
XLA Ops:
  0.6 0.0 copy-start.11
  0.6 0.6 %copy-done.11 = s32[8]{0:T(128)S(1)} copy-done((s32[8]{0:T(128)S(1)}, s32[8]{0:T(128)}, u32[]{:S(2)}) %copy-start.11) | copy-done | bytes 56
  1.3 0.0 copy-start.1
  1.3 0.1 shard_map.142.lengths_ref
  1.4 0.7 %copy-done.5 = bf16[2,3,8,512]{3,2,1,0:T(8,128)(2,1)S(1)} copy-done((bf16[2,3,8,512]{3,2,1,0:T(8,128)(2,1)S(1)}, bf16[2,3,8,512]{3,2,1,0:T(8,128)(2,1)}, u32[]{:S(2)}) %copy-start.5) | copy-done | bytes 49176
  2.1 0.0 copy-done.6
  2.1 0.0 copy-done.7
  2.1 0.1 shard_map.143
  2.2 3.1 %collective-permute-start.6 = (f32[1,2,2,8,512]{4,3,2,1,0:T(8,128)S(1)}, f32[1,2,2,8,512]{4,3,2,1,0:T(8,128)S(1)}, u32[]{:S(2)}, u32[]{:S(2)}) collective-permute-start(f32[1,2,2,8,512]{4,3,2,1,0:T(8,128)S(1)} %bitcast.15), channel_id=1, source_target_pairs={{0,2},{1,3},{2,0},{3,1},{4,6},{5,7},{6,4},{7,5},{8,10},{9,11},{10,... | collective-permute-start | bytes 196616 | tf_op jit(solution)/shard_map/ppermute | solution.py:56
  5.3 0.0 copy-done.10
  5.3 1.5 %collective-permute-start = (bf16[1,16,512]{2,1,0:T(8,128)(2,1)S(1)}, bf16[1,16,512]{2,1,0:T(8,128)(2,1)S(1)}, u32[]{:S(2)}, u32[]{:S(2)}) collective-permute-start(bf16[1,16,512]{2,1,0:T(8,128)(2,1)S(1)} %bitcast.17), channel_id=1, source_target_pairs={{0,8},{8,0},{16,24},{24,16},{1,9},{9,1},{17,25},{25,17},{2,10},{10... | collective-permute-start | bytes 49160 | tf_op jit(solution)/shard_map/ppermute | solution.py:56
  6.8 2.2 %collective-permute-done.second_ref = bf16[1,16,512]{2,1,0:T(8,128)(2,1)S(1)} collective-permute-done((bf16[1,16,512]{2,1,0:T(8,128)(2,1)S(1)}, bf16[1,16,512]{2,1,0:T(8,128)(2,1)S(1)}, u32[]{:S(2)}, u32[]{:S(2)}) %collective-permute-start) | collective-permute-done | bytes 16416 | tf_op jit(solution)/shard_map/ppermute | solution.py:56
  9.1 1.5 %collective-permute-start.1 = (bf16[2,16,512]{2,1,0:T(8,128)(2,1)S(1)}, bf16[2,16,512]{2,1,0:T(8,128)(2,1)S(1)}, u32[]{:S(2)}, u32[]{:S(2)}) collective-permute-start(bf16[2,16,512]{2,1,0:T(8,128)(2,1)S(1)} %shard_map.139.low_ref), channel_id=1, source_target_pairs={{0,16},{8,24},{16,0},{24,8},{1,17},{9,25},{17,1},{25,9},{2,18},{10... | collective-permute-start | bytes 98312 | tf_op jit(solution)/shard_map/ppermute | solution.py:56
  10.6 2.4 %collective-permute-done.1.high_ref = bf16[2,16,512]{2,1,0:T(8,128)(2,1)S(1)} collective-permute-done((bf16[2,16,512]{2,1,0:T(8,128)(2,1)S(1)}, bf16[2,16,512]{2,1,0:T(8,128)(2,1)S(1)}, u32[]{:S(2)}, u32[]{:S(2)}) %collective-permute-start.1) | collective-permute-done | bytes 32800 | tf_op jit(solution)/shard_map/ppermute | solution.py:56
  13.0 0.0 copy-done
  13.0 0.0 copy-done.8
  13.0 0.0 copy-start.3
  13.0 0.0 copy-start.4
  13.0 0.0 copy-start.9
  13.0 0.3 shard_map.140
  13.4 0.0 copy-start.2
  13.4 0.1 collective-permute-start.2
  13.4 0.0 collective-permute-done.6.second_ref
  13.5 2.7 %collective-permute-start.7 = (f32[2,2,2,8,512]{4,3,2,1,0:T(8,128)S(1)}, f32[2,2,2,8,512]{4,3,2,1,0:T(8,128)S(1)}, u32[]{:S(2)}, u32[]{:S(2)}) collective-permute-start(f32[2,2,2,8,512]{4,3,2,1,0:T(8,128)S(1)} %shard_map.144.refs_4_), channel_id=1, source_target_pairs={{0,4},{1,5},{2,6},{3,7},{4,0},{5,1},{6,2},{7,3},{8,12},{9,13},{10,... | collective-permute-start | bytes 393224 | tf_op jit(solution)/shard_map/ppermute | solution.py:56
  16.1 0.0 collective-permute-done.2.got_ref
  16.2 0.6 %collective-permute-start.3 = (bf16[264,128]{1,0:T(8,128)(2,1)S(1)}, bf16[264,128]{1,0:T(8,128)(2,1)S(1)}, u32[]{:S(2)}, u32[]{:S(2)}) collective-permute-start(bf16[264,128]{1,0:T(8,128)(2,1)S(1)} %shard_map.141.refs_0_), channel_id=1, source_target_pairs={{0,2},{1,3},{2,0},{3,1},{4,6},{5,7},{6,4},{7,5},{8,10},{9,11},{10,... | collective-permute-start | bytes 202760 | tf_op jit(solution)/shard_map/ppermute | solution.py:56
  16.8 1.1 %collective-permute-start.4 = (bf16[264,128]{1,0:T(8,128)(2,1)S(1)}, bf16[264,128]{1,0:T(8,128)(2,1)S(1)}, u32[]{:S(2)}, u32[]{:S(2)}) collective-permute-start(bf16[264,128]{1,0:T(8,128)(2,1)S(1)} %shard_map.141.refs_0_), channel_id=1, source_target_pairs={{0,4},{1,5},{2,6},{3,7},{4,0},{5,1},{6,2},{7,3},{8,12},{9,13},{10,... | collective-permute-start | bytes 202760 | tf_op jit(solution)/shard_map/ppermute | solution.py:56
  17.9 2.7 %collective-permute-start.5 = (bf16[264,128]{1,0:T(8,128)(2,1)S(1)}, bf16[264,128]{1,0:T(8,128)(2,1)S(1)}, u32[]{:S(2)}, u32[]{:S(2)}) collective-permute-start(bf16[264,128]{1,0:T(8,128)(2,1)S(1)} %shard_map.141.refs_0_), channel_id=1, source_target_pairs={{0,6},{1,7},{2,4},{3,5},{4,2},{5,3},{6,0},{7,1},{8,14},{9,15},{10,... | collective-permute-start | bytes 202760 | tf_op jit(solution)/shard_map/ppermute | solution.py:56
  20.6 0.9 %collective-permute-done.3.refs_1_ = bf16[264,128]{1,0:T(8,128)(2,1)S(1)} collective-permute-done((bf16[264,128]{1,0:T(8,128)(2,1)S(1)}, bf16[264,128]{1,0:T(8,128)(2,1)S(1)}, u32[]{:S(2)}, u32[]{:S(2)}) %collective-permute-start.3) | collective-permute-done | bytes 67616 | tf_op jit(solution)/shard_map/ppermute | solution.py:56
  21.5 6.0 %collective-permute-done.4.refs_2_ = bf16[264,128]{1,0:T(8,128)(2,1)S(1)} collective-permute-done((bf16[264,128]{1,0:T(8,128)(2,1)S(1)}, bf16[264,128]{1,0:T(8,128)(2,1)S(1)}, u32[]{:S(2)}, u32[]{:S(2)}) %collective-permute-start.4) | collective-permute-done | bytes 67616 | tf_op jit(solution)/shard_map/ppermute | solution.py:56
  27.5 0.0 collective-permute-done.5.refs_3_
  27.5 0.0 collective-permute-done.7.refs_5_
  27.5 0.5 shard_map.145
  28.0 0.1 collective-permute-start.8
  28.1 1.2 %collective-permute-done.8.other_ref = bf16[32,512]{1,0:T(8,128)(2,1)S(1)} collective-permute-done((bf16[32,512]{1,0:T(8,128)(2,1)S(1)}, bf16[32,512]{1,0:T(8,128)(2,1)S(1)}, u32[]{:S(2)}, u32[]{:S(2)}) %collective-permute-start.8) | collective-permute-done | bytes 32800 | tf_op jit(solution)/shard_map/ppermute | solution.py:56
  29.3 0.3 shard_map.146.refs_0_
  29.6 1.5 %collective-permute-start.10 = (bf16[64,512]{1,0:T(8,128)(2,1)S(1)}, bf16[64,512]{1,0:T(8,128)(2,1)S(1)}, u32[]{:S(2)}, u32[]{:S(2)}) collective-permute-start(bf16[64,512]{1,0:T(8,128)(2,1)S(1)} %shard_map.146.refs_0_), channel_id=1, source_target_pairs={{0,16},{8,24},{16,0},{24,8},{1,17},{9,25},{17,1},{25,9},{2,18},{10... | collective-permute-start | bytes 196616 | tf_op jit(solution)/shard_map/ppermute | solution.py:56
  31.1 1.4 %collective-permute-start.11 = (bf16[64,512]{1,0:T(8,128)(2,1)S(1)}, bf16[64,512]{1,0:T(8,128)(2,1)S(1)}, u32[]{:S(2)}, u32[]{:S(2)}) collective-permute-start(bf16[64,512]{1,0:T(8,128)(2,1)S(1)} %shard_map.146.refs_0_), channel_id=1, source_target_pairs={{0,24},{8,16},{16,8},{24,0},{1,25},{9,17},{17,9},{25,1},{2,26},{10... | collective-permute-start | bytes 196616 | tf_op jit(solution)/shard_map/ppermute | solution.py:56
  32.5 0.5 collective-permute-start.9
  33.1 0.8 %collective-permute-done.10.refs_2_ = bf16[64,512]{1,0:T(8,128)(2,1)S(1)} collective-permute-done((bf16[64,512]{1,0:T(8,128)(2,1)S(1)}, bf16[64,512]{1,0:T(8,128)(2,1)S(1)}, u32[]{:S(2)}, u32[]{:S(2)}) %collective-permute-start.10) | collective-permute-done | bytes 65568 | tf_op jit(solution)/shard_map/ppermute | solution.py:56
  33.9 3.0 %collective-permute-done.11.refs_3_ = bf16[64,512]{1,0:T(8,128)(2,1)S(1)} collective-permute-done((bf16[64,512]{1,0:T(8,128)(2,1)S(1)}, bf16[64,512]{1,0:T(8,128)(2,1)S(1)}, u32[]{:S(2)}, u32[]{:S(2)}) %collective-permute-start.11) | collective-permute-done | bytes 65568 | tf_op jit(solution)/shard_map/ppermute | solution.py:56
  36.9 0.0 collective-permute-done.9.refs_1_
  36.9 0.3 shard_map.147
  37.1 0.1 collective-permute-start.12
  37.2 1.2 %collective-permute-done.12.got_ref = bf16[264,128]{1,0:T(8,128)(2,1)S(1)} collective-permute-done((bf16[264,128]{1,0:T(8,128)(2,1)S(1)}, bf16[264,128]{1,0:T(8,128)(2,1)S(1)}, u32[]{:S(2)}, u32[]{:S(2)}) %collective-permute-start.12) | collective-permute-done | bytes 67616 | tf_op jit(solution)/shard_map/ppermute | solution.py:56
  38.5 2.0 %collective-permute-start.13 = (bf16[264,128]{1,0:T(8,128)(2,1)S(1)}, bf16[264,128]{1,0:T(8,128)(2,1)S(1)}, u32[]{:S(2)}, u32[]{:S(2)}) collective-permute-start(bf16[264,128]{1,0:T(8,128)(2,1)S(1)} %shard_map.148.refs_0_), channel_id=1, source_target_pairs={{0,2},{1,3},{2,0},{3,1},{4,6},{5,7},{6,4},{7,5},{8,10},{9,11},{10,... | collective-permute-start | bytes 202760 | tf_op jit(solution)/shard_map/ppermute | solution.py:56
  40.5 1.6 %collective-permute-start.14 = (bf16[264,128]{1,0:T(8,128)(2,1)S(1)}, bf16[264,128]{1,0:T(8,128)(2,1)S(1)}, u32[]{:S(2)}, u32[]{:S(2)}) collective-permute-start(bf16[264,128]{1,0:T(8,128)(2,1)S(1)} %shard_map.148.refs_0_), channel_id=1, source_target_pairs={{0,4},{1,5},{2,6},{3,7},{4,0},{5,1},{6,2},{7,3},{8,12},{9,13},{10,... | collective-permute-start | bytes 202760 | tf_op jit(solution)/shard_map/ppermute | solution.py:56
  42.2 1.0 %collective-permute-start.15 = (bf16[264,128]{1,0:T(8,128)(2,1)S(1)}, bf16[264,128]{1,0:T(8,128)(2,1)S(1)}, u32[]{:S(2)}, u32[]{:S(2)}) collective-permute-start(bf16[264,128]{1,0:T(8,128)(2,1)S(1)} %shard_map.148.refs_0_), channel_id=1, source_target_pairs={{0,6},{1,7},{2,4},{3,5},{4,2},{5,3},{6,0},{7,1},{8,14},{9,15},{10,... | collective-permute-start | bytes 202760 | tf_op jit(solution)/shard_map/ppermute | solution.py:56
  43.1 0.0 collective-permute-done.13.refs_1_
  43.1 5.8 %collective-permute-done.14.refs_2_ = bf16[264,128]{1,0:T(8,128)(2,1)S(1)} collective-permute-done((bf16[264,128]{1,0:T(8,128)(2,1)S(1)}, bf16[264,128]{1,0:T(8,128)(2,1)S(1)}, u32[]{:S(2)}, u32[]{:S(2)}) %collective-permute-start.14) | collective-permute-done | bytes 67616 | tf_op jit(solution)/shard_map/ppermute | solution.py:56
  48.9 0.0 collective-permute-done.15.refs_3_
  48.9 0.5 shard_map.149
  49.4 0.1 collective-permute-start.16
  49.5 0.6 %pad_maximum_fusion = bf16[2,3,8,512]{3,2,1,0:T(8,128)(2,1)} fusion(bf16[1,3,8,512]{3,2,1,0:T(8,128)(2,1)S(1)} %get-tuple-element.38, bf16[1,3,8,512]{3,2,1,0:T(8,128)(2,1)S(1)} %get-tuple-element.37), kind=kLoop, calls=%fused_computation | loop fusion | flops 24576 | bytes 98304 | tf_op jit(solution)/shard_map/stack | solution.py:339
  50.1 0.6 collective-permute-done.16.other_ref
  50.7 0.3 shard_map.150
  51.0 1.3 %collective-permute-start.17 = (bf16[16,512]{1,0:T(8,128)(2,1)S(1)}, bf16[16,512]{1,0:T(8,128)(2,1)S(1)}, u32[]{:S(2)}, u32[]{:S(2)}) collective-permute-start(bf16[16,512]{1,0:T(8,128)(2,1)S(1)} %get-tuple-element.28), channel_id=1, source_target_pairs={{0,8},{8,0},{16,24},{24,16},{1,9},{9,1},{17,25},{25,17},{2,10},{10... | collective-permute-start | bytes 49160 | tf_op jit(solution)/shard_map/ppermute | solution.py:56
  52.3 1.3 %collective-permute-start.18 = (bf16[16,512]{1,0:T(8,128)(2,1)S(1)}, bf16[16,512]{1,0:T(8,128)(2,1)S(1)}, u32[]{:S(2)}, u32[]{:S(2)}) collective-permute-start(bf16[16,512]{1,0:T(8,128)(2,1)S(1)} %get-tuple-element.29), channel_id=1, source_target_pairs={{0,16},{8,24},{16,0},{24,8},{1,17},{9,25},{17,1},{25,9},{2,18},{10... | collective-permute-start | bytes 49160 | tf_op jit(solution)/shard_map/ppermute | solution.py:56
  53.5 1.0 %collective-permute-start.19 = (bf16[16,512]{1,0:T(8,128)(2,1)S(1)}, bf16[16,512]{1,0:T(8,128)(2,1)S(1)}, u32[]{:S(2)}, u32[]{:S(2)}) collective-permute-start(bf16[16,512]{1,0:T(8,128)(2,1)S(1)} %get-tuple-element.30), channel_id=1, source_target_pairs={{0,24},{8,16},{16,8},{24,0},{1,25},{9,17},{17,9},{25,1},{2,26},{10... | collective-permute-start | bytes 49160 | tf_op jit(solution)/shard_map/ppermute | solution.py:56
  54.5 0.6 %pad_maximum_fusion.1 = f32[2,8,512]{2,1,0:T(8,128)} fusion(f32[1,8,512]{2,1,0:T(8,128)S(1)} %bitcast.20, f32[1,8,512]{2,1,0:T(8,128)S(1)} %bitcast.19), kind=kLoop, calls=%fused_computation.1 | loop fusion | flops 8192 | bytes 65536 | tf_op jit(solution)/shard_map/stack | solution.py:339
  55.1 0.0 collective-permute-done.17.refs_0_
  55.1 0.9 %collective-permute-done.18.refs_1_ = bf16[16,512]{1,0:T(8,128)(2,1)S(1)} collective-permute-done((bf16[16,512]{1,0:T(8,128)(2,1)S(1)}, bf16[16,512]{1,0:T(8,128)(2,1)S(1)}, u32[]{:S(2)}, u32[]{:S(2)}) %collective-permute-start.18) | collective-permute-done | bytes 16416 | tf_op jit(solution)/shard_map/ppermute | solution.py:56
  56.0 2.2 %collective-permute-done.19.refs_2_ = bf16[16,512]{1,0:T(8,128)(2,1)S(1)} collective-permute-done((bf16[16,512]{1,0:T(8,128)(2,1)S(1)}, bf16[16,512]{1,0:T(8,128)(2,1)S(1)}, u32[]{:S(2)}, u32[]{:S(2)}) %collective-permute-start.19) | collective-permute-done | bytes 16416 | tf_op jit(solution)/shard_map/ppermute | solution.py:56
  58.1 0.6 %shard_map.151 = bf16[16,512]{1,0:T(8,128)(2,1)} custom-call(f32[16,512]{1,0:T(8,128)S(1)} %get-tuple-element.27.own_ref, bf16[16,512]{1,0:T(8,128)(2,1)S(1)} %collective-permute-done.17.refs_0_, bf16[16,512]{1,0:T(8,128)(2,1)S(1)} %collective-permute-done.18.refs_1_, bf16[16,512]{1,0:T(8,128)(2,1)S(1)} %collective-permute-done.19.refs_2_), custom_call_target="tpu_custom_call" | custom-call | flops 1000000 | bytes 1048576 | tf_op jit(solution)/shard_map/pallas_call | solution.py:21
  (17 shorter events, 0.1 us)
Async XLA Ops:
  0.6 0.7 %copy-start.11 = (s32[8]{0:T(128)S(1)}, s32[8]{0:T(128)}, u32[]{:S(2)}) copy-start(s32[8]{0:T(128)} %param.21) | copy-start | bytes 100
  1.3 0.8 %copy-start.5 = (bf16[2,3,8,512]{3,2,1,0:T(8,128)(2,1)S(1)}, bf16[2,3,8,512]{3,2,1,0:T(8,128)(2,1)}, u32[]{:S(2)}) copy-start(bf16[2,3,8,512]{3,2,1,0:T(8,128)(2,1)} %conv_ref.1) | copy-start | bytes 147460
  1.3 0.8 %copy-start.6 = (bf16[2,4,512]{2,1,0:T(4,128)(2,1)S(1)}, bf16[2,4,512]{2,1,0:T(4,128)(2,1)}, u32[]{:S(2)}) copy-start(bf16[2,4,512]{2,1,0:T(4,128)(2,1)} %refs_6_.5) | copy-start | bytes 24580
  1.3 0.8 %copy-start.7 = (f32[2,8,512]{2,1,0:T(8,128)S(1)}, f32[2,8,512]{2,1,0:T(8,128)}, u32[]{:S(2)}) copy-start(f32[2,8,512]{2,1,0:T(8,128)} %rec_ref.1) | copy-start | bytes 98308
  1.3 11.7 %copy-start = (bf16[2,512,512]{2,1,0:T(8,128)(2,1)S(1)}, bf16[2,512,512]{2,1,0:T(8,128)(2,1)}, u32[]{:S(2)}) copy-start(bf16[2,512,512]{2,1,0:T(8,128)(2,1)} %refs_5_.1) | copy-start | bytes 3145732
  1.3 11.7 %copy-start.1 = (bf16[2,512,512]{2,1,0:T(8,128)(2,1)S(1)}, bf16[2,512,512]{2,1,0:T(8,128)(2,1)}, u32[]{:S(2)}) copy-start(bf16[2,512,512]{2,1,0:T(8,128)(2,1)} %refs_6_.4) | copy-start | bytes 3145732
  2.1 3.2 %copy-start.10 = (bf16[16,512]{1,0:T(8,128)(2,1)S(1)}, bf16[16,512]{1,0:T(8,128)(2,1)}, u32[]{:S(2)}) copy-start(bf16[16,512]{1,0:T(8,128)(2,1)} %param.12) | copy-start | bytes 49156
  2.2 11.3 %collective-permute-start.6 = (f32[1,2,2,8,512]{4,3,2,1,0:T(8,128)S(1)}, f32[1,2,2,8,512]{4,3,2,1,0:T(8,128)S(1)}, u32[]{:S(2)}, u32[]{:S(2)}) collective-permute-start(f32[1,2,2,8,512]{4,3,2,1,0:T(8,128)S(1)} %bitcast.15), channel_id=1, source_target_pairs={{0,2},{1,3},{2,0},{3,1},{4,6},{5,7},{6,4},{7,5},{8,10},{9,11},{10,... | collective-permute-start | bytes 196616 | tf_op jit(solution)/shard_map/ppermute | solution.py:56
  5.3 7.7 %copy-start.8 = (f32[2,512]{1,0:T(2,128)S(1)}, f32[2,512]{1,0:T(2,128)}, u32[]{:S(2)}) copy-start(f32[2,512]{1,0:T(2,128)} %refs_4_.1) | copy-start | bytes 12292
  5.3 3.7 %collective-permute-start = (bf16[1,16,512]{2,1,0:T(8,128)(2,1)S(1)}, bf16[1,16,512]{2,1,0:T(8,128)(2,1)S(1)}, u32[]{:S(2)}, u32[]{:S(2)}) collective-permute-start(bf16[1,16,512]{2,1,0:T(8,128)(2,1)S(1)} %bitcast.17), channel_id=1, source_target_pairs={{0,8},{8,0},{16,24},{24,16},{1,9},{9,1},{17,25},{25,17},{2,10},{10... | collective-permute-start | bytes 49160 | tf_op jit(solution)/shard_map/ppermute | solution.py:56
  9.1 3.9 %collective-permute-start.1 = (bf16[2,16,512]{2,1,0:T(8,128)(2,1)S(1)}, bf16[2,16,512]{2,1,0:T(8,128)(2,1)S(1)}, u32[]{:S(2)}, u32[]{:S(2)}) collective-permute-start(bf16[2,16,512]{2,1,0:T(8,128)(2,1)S(1)} %shard_map.139.low_ref), channel_id=1, source_target_pairs={{0,16},{8,24},{16,0},{24,8},{1,17},{9,25},{17,1},{25,9},{2,18},{10... | collective-permute-start | bytes 98312 | tf_op jit(solution)/shard_map/ppermute | solution.py:56
  13.0 14.5 %copy-start.3 = (bf16[2,4,128,128]{3,2,1,0:T(8,128)(2,1)S(1)}, bf16[2,4,128,128]{3,2,1,0:T(8,128)(2,1)}, u32[]{:S(2)}) copy-start(bf16[2,4,128,128]{3,2,1,0:T(8,128)(2,1)} %refs_8_.3) | copy-start | bytes 786436
  13.0 14.5 %copy-start.4 = (bf16[2,4,128,128]{3,2,1,0:T(8,128)(2,1)S(1)}, bf16[2,4,128,128]{3,2,1,0:T(8,128)(2,1)}, u32[]{:S(2)}) copy-start(bf16[2,4,128,128]{3,2,1,0:T(8,128)(2,1)} %refs_9_.3) | copy-start | bytes 786436
  13.0 14.5 %copy-start.9 = (f32[2,512]{1,0:T(2,128)S(1)}, f32[2,512]{1,0:T(2,128)}, u32[]{:S(2)}) copy-start(f32[2,512]{1,0:T(2,128)} %refs_7_.3) | copy-start | bytes 12292
  13.4 15.9 %copy-start.2 = (bf16[2,512,512]{2,1,0:T(8,128)(2,1)S(1)}, bf16[2,512,512]{2,1,0:T(8,128)(2,1)}, u32[]{:S(2)}) copy-start(bf16[2,512,512]{2,1,0:T(8,128)(2,1)} %w_ref.3) | copy-start | bytes 3145732
  13.4 2.8 %collective-permute-start.2 = (bf16[264,128]{1,0:T(8,128)(2,1)S(1)}, bf16[264,128]{1,0:T(8,128)(2,1)S(1)}, u32[]{:S(2)}, u32[]{:S(2)}) collective-permute-start(bf16[264,128]{1,0:T(8,128)(2,1)S(1)} %get-tuple-element.21), channel_id=1, source_target_pairs={{0,1},{1,0},{2,3},{3,2},{4,5},{5,4},{6,7},{7,6},{8,9},{9,8},{10,11... | collective-permute-start | bytes 202760 | tf_op jit(solution)/shard_map/ppermute | solution.py:56
  13.5 14.0 %collective-permute-start.7 = (f32[2,2,2,8,512]{4,3,2,1,0:T(8,128)S(1)}, f32[2,2,2,8,512]{4,3,2,1,0:T(8,128)S(1)}, u32[]{:S(2)}, u32[]{:S(2)}) collective-permute-start(f32[2,2,2,8,512]{4,3,2,1,0:T(8,128)S(1)} %shard_map.144.refs_4_), channel_id=1, source_target_pairs={{0,4},{1,5},{2,6},{3,7},{4,0},{5,1},{6,2},{7,3},{8,12},{9,13},{10,... | collective-permute-start | bytes 393224 | tf_op jit(solution)/shard_map/ppermute | solution.py:56
  16.2 5.4 %collective-permute-start.3 = (bf16[264,128]{1,0:T(8,128)(2,1)S(1)}, bf16[264,128]{1,0:T(8,128)(2,1)S(1)}, u32[]{:S(2)}, u32[]{:S(2)}) collective-permute-start(bf16[264,128]{1,0:T(8,128)(2,1)S(1)} %shard_map.141.refs_0_), channel_id=1, source_target_pairs={{0,2},{1,3},{2,0},{3,1},{4,6},{5,7},{6,4},{7,5},{8,10},{9,11},{10,... | collective-permute-start | bytes 202760 | tf_op jit(solution)/shard_map/ppermute | solution.py:56
  16.8 10.7 %collective-permute-start.4 = (bf16[264,128]{1,0:T(8,128)(2,1)S(1)}, bf16[264,128]{1,0:T(8,128)(2,1)S(1)}, u32[]{:S(2)}, u32[]{:S(2)}) collective-permute-start(bf16[264,128]{1,0:T(8,128)(2,1)S(1)} %shard_map.141.refs_0_), channel_id=1, source_target_pairs={{0,4},{1,5},{2,6},{3,7},{4,0},{5,1},{6,2},{7,3},{8,12},{9,13},{10,... | collective-permute-start | bytes 202760 | tf_op jit(solution)/shard_map/ppermute | solution.py:56
  17.9 9.6 %collective-permute-start.5 = (bf16[264,128]{1,0:T(8,128)(2,1)S(1)}, bf16[264,128]{1,0:T(8,128)(2,1)S(1)}, u32[]{:S(2)}, u32[]{:S(2)}) collective-permute-start(bf16[264,128]{1,0:T(8,128)(2,1)S(1)} %shard_map.141.refs_0_), channel_id=1, source_target_pairs={{0,6},{1,7},{2,4},{3,5},{4,2},{5,3},{6,0},{7,1},{8,14},{9,15},{10,... | collective-permute-start | bytes 202760 | tf_op jit(solution)/shard_map/ppermute | solution.py:56
  28.0 1.3 %collective-permute-start.8 = (bf16[32,512]{1,0:T(8,128)(2,1)S(1)}, bf16[32,512]{1,0:T(8,128)(2,1)S(1)}, u32[]{:S(2)}, u32[]{:S(2)}) collective-permute-start(bf16[32,512]{1,0:T(8,128)(2,1)S(1)} %get-tuple-element.22.own_ref), channel_id=1, source_target_pairs={{0,1},{1,0},{2,3},{3,2},{4,5},{5,4},{6,7},{7,6},{8,9},{9,8},{10,11... | collective-permute-start | bytes 98312 | tf_op jit(solution)/shard_map/ppermute | solution.py:56
  29.6 4.3 %collective-permute-start.10 = (bf16[64,512]{1,0:T(8,128)(2,1)S(1)}, bf16[64,512]{1,0:T(8,128)(2,1)S(1)}, u32[]{:S(2)}, u32[]{:S(2)}) collective-permute-start(bf16[64,512]{1,0:T(8,128)(2,1)S(1)} %shard_map.146.refs_0_), channel_id=1, source_target_pairs={{0,16},{8,24},{16,0},{24,8},{1,17},{9,25},{17,1},{25,9},{2,18},{10... | collective-permute-start | bytes 196616 | tf_op jit(solution)/shard_map/ppermute | solution.py:56
  31.1 5.7 %collective-permute-start.11 = (bf16[64,512]{1,0:T(8,128)(2,1)S(1)}, bf16[64,512]{1,0:T(8,128)(2,1)S(1)}, u32[]{:S(2)}, u32[]{:S(2)}) collective-permute-start(bf16[64,512]{1,0:T(8,128)(2,1)S(1)} %shard_map.146.refs_0_), channel_id=1, source_target_pairs={{0,24},{8,16},{16,8},{24,0},{1,25},{9,17},{17,9},{25,1},{2,26},{10... | collective-permute-start | bytes 196616 | tf_op jit(solution)/shard_map/ppermute | solution.py:56
  32.5 4.3 %collective-permute-start.9 = (bf16[64,512]{1,0:T(8,128)(2,1)S(1)}, bf16[64,512]{1,0:T(8,128)(2,1)S(1)}, u32[]{:S(2)}, u32[]{:S(2)}) collective-permute-start(bf16[64,512]{1,0:T(8,128)(2,1)S(1)} %shard_map.146.refs_0_), channel_id=1, source_target_pairs={{0,8},{8,0},{16,24},{24,16},{1,9},{9,1},{17,25},{25,17},{2,10},{10... | collective-permute-start | bytes 196616 | tf_op jit(solution)/shard_map/ppermute | solution.py:56
  37.1 1.3 %collective-permute-start.12 = (bf16[264,128]{1,0:T(8,128)(2,1)S(1)}, bf16[264,128]{1,0:T(8,128)(2,1)S(1)}, u32[]{:S(2)}, u32[]{:S(2)}) collective-permute-start(bf16[264,128]{1,0:T(8,128)(2,1)S(1)} %get-tuple-element.24), channel_id=1, source_target_pairs={{0,1},{1,0},{2,3},{3,2},{4,5},{5,4},{6,7},{7,6},{8,9},{9,8},{10,11... | collective-permute-start | bytes 202760 | tf_op jit(solution)/shard_map/ppermute | solution.py:56
  38.5 4.6 %collective-permute-start.13 = (bf16[264,128]{1,0:T(8,128)(2,1)S(1)}, bf16[264,128]{1,0:T(8,128)(2,1)S(1)}, u32[]{:S(2)}, u32[]{:S(2)}) collective-permute-start(bf16[264,128]{1,0:T(8,128)(2,1)S(1)} %shard_map.148.refs_0_), channel_id=1, source_target_pairs={{0,2},{1,3},{2,0},{3,1},{4,6},{5,7},{6,4},{7,5},{8,10},{9,11},{10,... | collective-permute-start | bytes 202760 | tf_op jit(solution)/shard_map/ppermute | solution.py:56
  40.5 8.4 %collective-permute-start.14 = (bf16[264,128]{1,0:T(8,128)(2,1)S(1)}, bf16[264,128]{1,0:T(8,128)(2,1)S(1)}, u32[]{:S(2)}, u32[]{:S(2)}) collective-permute-start(bf16[264,128]{1,0:T(8,128)(2,1)S(1)} %shard_map.148.refs_0_), channel_id=1, source_target_pairs={{0,4},{1,5},{2,6},{3,7},{4,0},{5,1},{6,2},{7,3},{8,12},{9,13},{10,... | collective-permute-start | bytes 202760 | tf_op jit(solution)/shard_map/ppermute | solution.py:56
  42.2 6.8 %collective-permute-start.15 = (bf16[264,128]{1,0:T(8,128)(2,1)S(1)}, bf16[264,128]{1,0:T(8,128)(2,1)S(1)}, u32[]{:S(2)}, u32[]{:S(2)}) collective-permute-start(bf16[264,128]{1,0:T(8,128)(2,1)S(1)} %shard_map.148.refs_0_), channel_id=1, source_target_pairs={{0,6},{1,7},{2,4},{3,5},{4,2},{5,3},{6,0},{7,1},{8,14},{9,15},{10,... | collective-permute-start | bytes 202760 | tf_op jit(solution)/shard_map/ppermute | solution.py:56
  49.4 1.3 %collective-permute-start.16 = (bf16[32,512]{1,0:T(8,128)(2,1)S(1)}, bf16[32,512]{1,0:T(8,128)(2,1)S(1)}, u32[]{:S(2)}, u32[]{:S(2)}) collective-permute-start(bf16[32,512]{1,0:T(8,128)(2,1)S(1)} %get-tuple-element.25.own_ref), channel_id=1, source_target_pairs={{0,1},{1,0},{2,3},{3,2},{4,5},{5,4},{6,7},{7,6},{8,9},{9,8},{10,11... | collective-permute-start | bytes 98312 | tf_op jit(solution)/shard_map/ppermute | solution.py:56
  51.0 4.2 %collective-permute-start.17 = (bf16[16,512]{1,0:T(8,128)(2,1)S(1)}, bf16[16,512]{1,0:T(8,128)(2,1)S(1)}, u32[]{:S(2)}, u32[]{:S(2)}) collective-permute-start(bf16[16,512]{1,0:T(8,128)(2,1)S(1)} %get-tuple-element.28), channel_id=1, source_target_pairs={{0,8},{8,0},{16,24},{24,16},{1,9},{9,1},{17,25},{25,17},{2,10},{10... | collective-permute-start | bytes 49160 | tf_op jit(solution)/shard_map/ppermute | solution.py:56
  52.3 3.7 %collective-permute-start.18 = (bf16[16,512]{1,0:T(8,128)(2,1)S(1)}, bf16[16,512]{1,0:T(8,128)(2,1)S(1)}, u32[]{:S(2)}, u32[]{:S(2)}) collective-permute-start(bf16[16,512]{1,0:T(8,128)(2,1)S(1)} %get-tuple-element.29), channel_id=1, source_target_pairs={{0,16},{8,24},{16,0},{24,8},{1,17},{9,25},{17,1},{25,9},{2,18},{10... | collective-permute-start | bytes 49160 | tf_op jit(solution)/shard_map/ppermute | solution.py:56
  53.5 4.6 %collective-permute-start.19 = (bf16[16,512]{1,0:T(8,128)(2,1)S(1)}, bf16[16,512]{1,0:T(8,128)(2,1)S(1)}, u32[]{:S(2)}, u32[]{:S(2)}) collective-permute-start(bf16[16,512]{1,0:T(8,128)(2,1)S(1)} %get-tuple-element.30), channel_id=1, source_target_pairs={{0,24},{8,16},{16,8},{24,0},{1,25},{9,17},{17,9},{25,1},{2,26},{10... | collective-permute-start | bytes 49160 | tf_op jit(solution)/shard_map/ppermute | solution.py:56
where the time goes:
time: 58.9 us; the launch traced here: 58.8 us
  waiting for transfers between devices  27.1 us (46%)
  starting transfers between devices  25.2 us (43%)
  Pallas kernels  2.96 us (5%)
  local copies, waits for them, and re-layouts  1.39 us (2%)
  other arithmetic  1.25 us (2%)
  between operations  0.81 us (1%)
    ppermute x20, waiting for transfers between devices, partner_exchange(): lax.ppermute(value, axis, [(i, i ^ m) for i in range(count)])  27.1 us
    ppermute x20, starting transfers between devices, partner_exchange(): lax.ppermute(value, axis, [(i, i ^ m) for i in range(count)])  25.2 us
    pallas_call x13, Pallas kernels, call(): pl.pallas_call(kernel, out_shape=outs, in_specs=[spec] * len(args), out_s...  2.96 us
    unnamed x24, local copies, waits for them, and re-layouts  1.39 us
    another operation x3, other arithmetic, blocks(): return (mixed, jnp.stack(conv_list), jnp.stack(rec_list))  1.25 us
  transfers between devices with their start and end apart: 20, of which 12 were waited for; matrix products, arithmetic and copies ran while one was open for 2% of the time, Pallas kernels for 1%

commit v1 on v0

--- a/solution.py
+++ b/solution.py
@@ -41,6 +41,9 @@
         self.per_tp = batch // tp
         self.chunks = self.per_tp // self.rows
 
+    def side(self, owner, z):
+        return pl.multiple_of((owner ^ z) * self.rows, self.rows)
+
     def place(self, chunk, z, core):
         side = jnp.where(lax.rem(chunk, 2) == core, 0, self.half)
         return pl.multiple_of(side + ((chunk // 2) ^ z) * self.rows, self.rows)
@@ -53,7 +56,10 @@
 
 def partner_exchange(value, axis, masks):
     count = lax.axis_size(axis)
-    return [lax.ppermute(value, axis, [(i, i ^ m) for i in range(count)]) for m in masks]
+    got = []
+    for m in masks:
+        got.append(lax.ppermute(value, axis, [(i, i ^ m) for i in range(count)]))
+    return got
 
 
 def doubling(value, axis, masks):
@@ -120,7 +126,7 @@
     for g in range(rows // GROUP):
         part = slice(g * GROUP, (g + 1) * GROUP)
         tile = jnp.where(lane == g, high[part], jnp.where(lane == g + LANES // 2, low[part], tile))
-    ref[2 * count * rows :, :] = tile.astype(ref.dtype)
+    ref[2 * count * rows : 2 * count * rows + GROUP, :] = tile.astype(ref.dtype)
 
 
 def unpack(total, rows, width):
@@ -140,14 +146,16 @@
     return jnp.concatenate([part[(m ^ mask) * size : ((m ^ mask) + 1) * size] for m in range(zs)], axis=0)
 
 
-def project(x, gain, wi, wg, keep_ref, send_ref):
-    half = x.shape[0] // 2
-    square = jnp.sum(x * x, axis=1, keepdims=True)
-    scaled = (x * gain).astype(BF16)
-    value = jnp.dot(scaled, wi, preferred_element_type=F32)
-    gate = jnp.dot(scaled, wg, preferred_element_type=F32)
-    pack(keep_ref, value[:half], gate[:half], square[:half])
-    pack(send_ref, value[half:], gate[half:], square[half:])
+def to_blocks(ref, start, rows):
+    count = rows.shape[0]
+    for b in range(rows.shape[1] // LANES):
+        ref[start + b * count : start + (b + 1) * count, :] = rows[:, b * LANES : (b + 1) * LANES].astype(ref.dtype)
+
+
+def from_blocks(ref, start, rows, width):
+    return jnp.concatenate(
+        [ref[start + b * rows : start + (b + 1) * rows, :] for b in range(width // LANES)], axis=1
+    )
 
 
 def first_kernel(lay, low_ref, high_ref, gain_ref, wi_ref, wg_ref, x_ref, keep_ref, send_ref):
@@ -158,17 +166,39 @@
         for i in range(lay.chunks):
             start = lay.place(owner * lay.chunks + i, z, core)
             x_ref[pl.ds(start, lay.rows), :] = rows[i * lay.rows : (i + 1) * lay.rows]
-    project(x_ref[...], gain_ref[0:1, :], wi_ref[0], wg_ref[0], keep_ref, send_ref)
-
-
-def next_kernel(lay, layer, x_old_ref, *refs):
-    parts, (gain_ref, wi_ref, wg_ref, x_ref, keep_ref, send_ref) = refs[: lay.tp], refs[lay.tp :]
+    x = x_ref[...]
+    half, tall = lay.half, keep_ref.shape[0]
+    square = jnp.sum(x * x, axis=1, keepdims=True)
+    scaled = (x * gain_ref[0:1, :]).astype(BF16)
+    value = jnp.dot(scaled, wi_ref[0], preferred_element_type=F32)
+    gate = jnp.dot(scaled, wg_ref[0], preferred_element_type=F32)
+    pack(keep_ref, value[:half], gate[:half], square[:half])
+    pack(send_ref, value[half:], gate[half:], square[half:])
+    to_blocks(send_ref, tall, x[half:])
+
+
+def next_kernel(lay, layer, x_old_ref, got_ref, *refs):
+    parts, refs = refs[: lay.tp], refs[lay.tp :]
+    gain_ref, wi_ref, wg_ref, gain2_ref, wi2_ref, wg2_ref, x_ref, out_ref = refs
+    half, depth = lay.half, x_old_ref.shape[1]
+    start = got_ref.shape[0] - half * depth // LANES
     total = parts[0][...].astype(F32)
     for part in parts[1:]:
         total = total + part[...].astype(F32)
-    x = (x_old_ref[...] + total).astype(BF16).astype(F32)
-    x_ref[...] = x
-    project(x, gain_ref[layer : layer + 1, :], wi_ref[layer], wg_ref[layer], keep_ref, send_ref)
+    x = (x_old_ref[:half] + total[:, :depth]).astype(BF16).astype(F32)
+    y = (from_blocks(got_ref, start, half, depth).astype(F32) + total[:, depth:]).astype(BF16).astype(F32)
+    x_ref[:, :depth] = x
+    x_ref[:, depth:] = y
+    square = jnp.sum(x * x, axis=1, keepdims=True) + jnp.sum(y * y, axis=1, keepdims=True)
+    scaled = (x * gain_ref[layer : layer + 1, :]).astype(BF16)
+    scaled2 = (y * gain2_ref[layer : layer + 1, :]).astype(BF16)
+
+    def both(w, w2):
+        return jnp.dot(scaled, w[layer], preferred_element_type=F32) + jnp.dot(
+            scaled2, w2[layer], preferred_element_type=F32
+        )
+
+    pack(out_ref, both(wi_ref, wi2_ref), both(wg_ref, wg2_ref), square)
 
 
 def one_minus_exp(u):
@@ -179,13 +209,13 @@
 
 
 def add_kernel(keep_ref, got_ref, out_ref):
-    out_ref[...] = (keep_ref[...] + got_ref[...].astype(F32)).astype(out_ref.dtype)
+    out_ref[...] = (keep_ref[...] + got_ref[: keep_ref.shape[0]].astype(F32)).astype(out_ref.dtype)
 
 
 def recurrence_kernel(lay, layer, features, *refs):
     zs = lay.dp // 2
     sums, refs = refs[:zs], refs[zs:]
-    low_ref, high_ref, taps_ref, decay_ref, wr_ref, wj_ref, readout_ref, value_ref, rec_ref = refs
+    low_ref, high_ref, taps_ref, decay_ref, wr_ref, wj_ref, *extra, readout_ref, value_ref, rec_ref = refs
     rows, half, width = lay.rows, lay.half, taps_ref.shape[2]
     states = [entry((low_ref, high_ref), m) for m in range(zs)]
     old = jnp.concatenate([state[layer, 0] for state in states], axis=0)
@@ -218,30 +248,38 @@
     inp_gate = jax.nn.sigmoid(mapped(wj_ref))
     log_decay = -8.0 * rec_gate * jax.nn.softplus(-decay_ref[layer : layer + 1, :])
     hidden = jnp.exp(log_decay) * previous + jnp.sqrt(one_minus_exp(2.0 * log_decay)) * (inp_gate * conv_out)
-    readout_ref[...] = (hidden * jax.nn.gelu(gate_in)).astype(BF16)
+    readout_ref[:half] = (hidden * jax.nn.gelu(gate_in)).astype(BF16)
+    for x_ref in extra:
+        me, z, _ = mesh_place()
+        depth = x_ref.shape[1] // 2
+        for i in range(lay.chunks // 2):
+            start = lay.side(me * (lay.chunks // 2) + i, z)
+            readout_ref[half + i * rows : half + (i + 1) * rows] = x_ref[pl.ds(start, rows), depth:].astype(BF16)
     value_ref[...] = value_in[:rows].astype(BF16)
     rec_ref[...] = hidden[:rows]
 
 
-def output_kernel(layer, own_ref, other_ref, w_ref, out_ref):
-    half = own_ref.shape[0]
-    out_ref[:half] = jnp.dot(own_ref[...], w_ref[layer], preferred_element_type=F32).astype(BF16)
-    out_ref[half:] = jnp.dot(other_ref[...], w_ref[layer], preferred_element_type=F32).astype(BF16)
+def output_kernel(layer, rows_ref, w_ref, w2_ref, out_ref):
+    width = w_ref.shape[2]
+    out_ref[:, :width] = jnp.dot(rows_ref[...], w_ref[layer], preferred_element_type=F32).astype(BF16)
+    out_ref[:, width:] = jnp.dot(rows_ref[...], w2_ref[layer], preferred_element_type=F32).astype(BF16)
 
 
 def last_output_kernel(lay, layer, own_ref, other_ref, w_ref, x_ref, *refs):
-    mine_ref, outs, held = refs[0], refs[1:-1], refs[-1]
-    half = own_ref.shape[0]
-    held[:half] = jnp.dot(own_ref[...], w_ref[layer], preferred_element_type=F32)
-    held[half:] = jnp.dot(other_ref[...], w_ref[layer], preferred_element_type=F32)
+    outs, held = refs[:-1], refs[-1]
+    half, rows, depth = lay.half, lay.rows, held.shape[1]
+    held[:half] = jnp.dot(own_ref[:half], w_ref[layer], preferred_element_type=F32)
+    held[half:] = jnp.dot(other_ref[:half], w_ref[layer], preferred_element_type=F32)
     me, z, core = mesh_place()
-    for mask, out in enumerate((mine_ref,) + tuple(outs)):
+    far = other_ref[half:].astype(F32)
+    for mask, out in enumerate(outs):
         for i in range(lay.chunks):
             start = lay.place((me ^ mask) * lay.chunks + i, z, core)
-            piece = held[pl.ds(start, lay.rows), :]
+            piece = held[pl.ds(start, rows), :]
             if mask == 0:
-                piece = piece + x_ref[pl.ds(start, lay.rows), :]
-            out[i * lay.rows : (i + 1) * lay.rows, :] = piece.astype(out.dtype)
+                near = x_ref[pl.ds(lay.side(me * (lay.chunks // 2) + i // 2, z), rows), :depth]
+                piece = piece + jnp.where(core == i % 2, near, far[i // 2 * rows : (i // 2 + 1) * rows])
+            out[i * rows : (i + 1) * rows, :] = piece.astype(out.dtype)
 
 
 def final_kernel(own_ref, *refs):
@@ -289,40 +327,61 @@
     )
     rows = doubling(tokens, "tp", bits(tp))
     states = doubling(state, "dp", [2 * m for m in bits(dp // 2)])
-    parts = None
+    sent = half * depth // LANES
+    block = [
+        shape((half, width), BF16),
+        shape((lay.rows, width), BF16),
+        shape((lay.rows, width), F32),
+    ]
+    weights = (norm_gain, w_input, w_gate)
+    x, keep, send = call(
+        functools.partial(first_kernel, lay),
+        [shape((batch, depth), F32), shape((tall, LANES), F32), shape((tall + sent, LANES), BF16)],
+        *rows,
+        *weights,
+    )
+    (got,) = partner_exchange(send, "dp", [1])
+    summed = call(add_kernel, shape((tall, LANES), BF16), keep, got)
     conv_list, rec_list = [], []
-    x = None
     for layer in range(layers):
-        outs = [shape((batch, depth), F32), shape((tall, LANES), F32), shape((tall, LANES), BF16)]
-        weights = (norm_gain, w_input, w_gate)
+        last = layer == layers - 1
+        if layer > 0:
+            x, summed = call(
+                functools.partial(next_kernel, lay, layer),
+                [shape((half, 2 * depth), F32), shape((tall, LANES), BF16)],
+                *before,
+                *parts,
+                *weights,
+                *weights2,
+            )
+        sums = [summed] + partner_exchange(summed, "dp", z_masks)
         if layer == 0:
-            x, keep, send = call(functools.partial(first_kernel, lay), outs, *rows, *weights)
-        else:
-            x, keep, send = call(functools.partial(next_kernel, lay, layer), outs, x, *parts, *weights)
-        (got,) = partner_exchange(send, "dp", [1])
-        summed = call(add_kernel, shape((tall, LANES), BF16), keep, got)
+            out2, *weights2 = [partner_exchange(w, "dp", [1])[0] for w in (w_output,) + weights]
+        if last:
+            block[0] = shape((half + lay.per_tp // 2, width), BF16)
         readout, value, hidden = call(
             functools.partial(recurrence_kernel, lay, layer, features),
-            [
-                shape((half, width), BF16),
-                shape((lay.rows, width), BF16),
-                shape((lay.rows, width), F32),
-            ],
-            summed,
-            *partner_exchange(summed, "dp", z_masks),
+            block,
+            *sums,
             *states,
             conv_weight,
             decay_param,
             w_recur,
             w_inject,
+            *([x] if last else []),
         )
-        (other,) = partner_exchange(readout, "dp", [1])
-        if layer < layers - 1:
+        if not last:
             partial = call(
-                functools.partial(output_kernel, layer), shape((batch, depth), BF16), readout, other, w_output
+                functools.partial(output_kernel, layer),
+                shape((half, 2 * depth), BF16),
+                readout,
+                w_output,
+                out2,
             )
             parts = [partial] + partner_exchange(partial, "tp", tp_masks)
+            before = (x, got)
         else:
+            (other,) = partner_exchange(readout, "dp", [1])
             own, *pieces = call(
                 functools.partial(last_output_kernel, lay, layer),
                 [shape((lay.per_tp, depth), F32)] + [shape((lay.per_tp, depth), BF16)] * (tp - 1),

time: 58.9 us -> 58 us (0.985)
  waiting for transfers between devices: 27.1 us -> 23.1 us
  starting transfers between devices: 25.2 us -> 28.1 us
    ppermute x20 -> x22, waiting for transfers between devices: 27.1 us -> 23.1 us  [partner_exchange(): got.append(lax.ppermute(value, axis, [(i, i ^ m) for i in range(count)]))]
    ppermute x20 -> x22, starting transfers between devices: 25.2 us -> 28.1 us  [partner_exchange(): got.append(lax.ppermute(value, axis, [(i, i ^ m) for i in range(count)]))]
    pallas_call x13 -> x12, Pallas kernels: 2.96 us -> 3.08 us  [call(): pl.pallas_call(kernel, out_shape=outs, in_specs=[spec] * len(args), out_s...]
  transfers between devices with their start and end apart: 20 -> 22, of which waited for: 12 -> 13; matrix products, arithmetic and copies ran while one was open for 2% -> 2% of each run, Pallas kernels for 1% -> 2%
where the time goes in v1:
time: 58 us; the launch traced here: 57.8 us
  starting transfers between devices  28.1 us (48%)
  waiting for transfers between devices  23.1 us (40%)
  Pallas kernels  3.08 us (5%)
  local copies, waits for them, and re-layouts  1.46 us (3%)
  other arithmetic  1.25 us (2%)
  between operations  0.82 us (1%)
    ppermute x22, starting transfers between devices, partner_exchange(): got.append(lax.ppermute(value, axis, [(i, i ^ m) for i in range(count)]))  28.1 us
    ppermute x22, waiting for transfers between devices, partner_exchange(): got.append(lax.ppermute(value, axis, [(i, i ^ m) for i in range(count)]))  23.1 us
    pallas_call x12, Pallas kernels, call(): pl.pallas_call(kernel, out_shape=outs, in_specs=[spec] * len(args), out_s...  3.08 us
    unnamed x24, local copies, waits for them, and re-layouts  1.45 us
    another operation x3, other arithmetic, blocks(): return (mixed, jnp.stack(conv_list), jnp.stack(rec_list))  1.25 us
  transfers between devices with their start and end apart: 22, of which 13 were waited for; matrix products, arithmetic and copies ran while one was open for 2% of the time, Pallas kernels for 2%

profile of v1, /device:TPU:0, one launch (start us, length us, event | category | flops | bytes accessed | tf_op | source)
XLA Modules:
  0.0 57.8 jit_solution(17493054654370380125)
XLA Ops:
  0.6 0.6 collective-permute-start.8
  1.2 0.1 collective-permute-start.13
  1.3 0.4 collective-permute-start.14
  1.7 2.6 %collective-permute-start = (bf16[1,16,512]{2,1,0:T(8,128)(2,1)}, bf16[1,16,512]{2,1,0:T(8,128)(2,1)S(1)}, u32[]{:S(2)}, u32[]{:S(2)}) collective-permute-start(bf16[1,16,512]{2,1,0:T(8,128)(2,1)} %bitcast.17), channel_id=1, source_target_pairs={{0,8},{8,0},{16,24},{24,16},{1,9},{9,1},{17,25},{25,17},{2,10},{10... | collective-permute-start | bytes 49160 | tf_op jit(solution)/shard_map/ppermute | solution.py:61
  4.3 1.9 %collective-permute-done.second_ref = bf16[1,16,512]{2,1,0:T(8,128)(2,1)S(1)} collective-permute-done((bf16[1,16,512]{2,1,0:T(8,128)(2,1)}, bf16[1,16,512]{2,1,0:T(8,128)(2,1)S(1)}, u32[]{:S(2)}, u32[]{:S(2)}) %collective-permute-start) | collective-permute-done | bytes 16416 | tf_op jit(solution)/shard_map/ppermute | solution.py:61
  6.2 0.7 %copy-done.9 = bf16[16,512]{1,0:T(8,128)(2,1)S(1)} copy-done((bf16[16,512]{1,0:T(8,128)(2,1)S(1)}, bf16[16,512]{1,0:T(8,128)(2,1)}, u32[]{:S(2)}) %copy-start.9) | copy-done | bytes 16408
  6.9 2.1 %collective-permute-start.1 = (bf16[2,16,512]{2,1,0:T(8,128)(2,1)S(1)}, bf16[2,16,512]{2,1,0:T(8,128)(2,1)S(1)}, u32[]{:S(2)}, u32[]{:S(2)}) collective-permute-start(bf16[2,16,512]{2,1,0:T(8,128)(2,1)S(1)} %shard_map.139.low_ref), channel_id=1, source_target_pairs={{0,16},{8,24},{16,0},{24,8},{1,17},{9,25},{17,1},{25,9},{2,18},{10... | collective-permute-start | bytes 98312 | tf_op jit(solution)/shard_map/ppermute | solution.py:61
  9.0 0.0 copy-done.11
  9.0 0.0 copy-start.1
  9.0 0.0 copy-start.2
  9.0 0.1 shard_map.142.lengths_ref
  9.1 0.7 %copy-done.5 = bf16[2,3,8,512]{3,2,1,0:T(8,128)(2,1)S(1)} copy-done((bf16[2,3,8,512]{3,2,1,0:T(8,128)(2,1)S(1)}, bf16[2,3,8,512]{3,2,1,0:T(8,128)(2,1)}, u32[]{:S(2)}) %copy-start.5) | copy-done | bytes 49176
  9.8 0.1 shard_map.143
  9.9 1.6 %collective-permute-start.6 = (f32[1,2,2,8,512]{4,3,2,1,0:T(8,128)S(1)}, f32[1,2,2,8,512]{4,3,2,1,0:T(8,128)S(1)}, u32[]{:S(2)}, u32[]{:S(2)}) collective-permute-start(f32[1,2,2,8,512]{4,3,2,1,0:T(8,128)S(1)} %bitcast.15), channel_id=1, source_target_pairs={{0,2},{1,3},{2,0},{3,1},{4,6},{5,7},{6,4},{7,5},{8,10},{9,11},{10,... | collective-permute-start | bytes 196616 | tf_op jit(solution)/shard_map/ppermute | solution.py:61
  11.5 0.0 collective-permute-done.1.high_ref
  11.5 0.0 copy-start.3
  11.5 0.0 copy-start.4
  11.5 0.0 copy-start.8
  11.6 0.3 shard_map.140
  11.9 0.0 copy-start
  11.9 0.1 collective-permute-start.2
  12.0 2.2 %collective-permute-done.6.second_ref = f32[1,2,2,8,512]{4,3,2,1,0:T(8,128)S(1)} collective-permute-done((f32[1,2,2,8,512]{4,3,2,1,0:T(8,128)S(1)}, f32[1,2,2,8,512]{4,3,2,1,0:T(8,128)S(1)}, u32[]{:S(2)}, u32[]{:S(2)}) %collective-permute-start.6) | collective-permute-done | bytes 65568 | tf_op jit(solution)/shard_map/ppermute | solution.py:61
  14.2 2.7 %collective-permute-start.7 = (f32[2,2,2,8,512]{4,3,2,1,0:T(8,128)S(1)}, f32[2,2,2,8,512]{4,3,2,1,0:T(8,128)S(1)}, u32[]{:S(2)}, u32[]{:S(2)}) collective-permute-start(f32[2,2,2,8,512]{4,3,2,1,0:T(8,128)S(1)} %shard_map.144.refs_4_), channel_id=1, source_target_pairs={{0,4},{1,5},{2,6},{3,7},{4,0},{5,1},{6,2},{7,3},{8,12},{9,13},{10,... | collective-permute-start | bytes 393224 | tf_op jit(solution)/shard_map/ppermute | solution.py:61
  16.9 0.0 collective-permute-done.2.got_ref
  16.9 1.6 %collective-permute-start.3 = (bf16[264,128]{1,0:T(8,128)(2,1)S(1)}, bf16[264,128]{1,0:T(8,128)(2,1)S(1)}, u32[]{:S(2)}, u32[]{:S(2)}) collective-permute-start(bf16[264,128]{1,0:T(8,128)(2,1)S(1)} %shard_map.141.refs_0_), channel_id=1, source_target_pairs={{0,2},{1,3},{2,0},{3,1},{4,6},{5,7},{6,4},{7,5},{8,10},{9,11},{10,... | collective-permute-start | bytes 202760 | tf_op jit(solution)/shard_map/ppermute | solution.py:61
  18.5 3.2 %collective-permute-done.7.refs_5_ = f32[2,2,2,8,512]{4,3,2,1,0:T(8,128)S(1)} collective-permute-done((f32[2,2,2,8,512]{4,3,2,1,0:T(8,128)S(1)}, f32[2,2,2,8,512]{4,3,2,1,0:T(8,128)S(1)}, u32[]{:S(2)}, u32[]{:S(2)}) %collective-permute-start.7) | collective-permute-done | bytes 131104 | tf_op jit(solution)/shard_map/ppermute | solution.py:61
  21.7 1.1 %collective-permute-start.4 = (bf16[264,128]{1,0:T(8,128)(2,1)S(1)}, bf16[264,128]{1,0:T(8,128)(2,1)S(1)}, u32[]{:S(2)}, u32[]{:S(2)}) collective-permute-start(bf16[264,128]{1,0:T(8,128)(2,1)S(1)} %shard_map.141.refs_0_), channel_id=1, source_target_pairs={{0,4},{1,5},{2,6},{3,7},{4,0},{5,1},{6,2},{7,3},{8,12},{9,13},{10,... | collective-permute-start | bytes 202760 | tf_op jit(solution)/shard_map/ppermute | solution.py:61
  22.8 0.0 collective-permute-done.3.refs_1_
  22.8 3.0 %collective-permute-start.5 = (bf16[264,128]{1,0:T(8,128)(2,1)S(1)}, bf16[264,128]{1,0:T(8,128)(2,1)S(1)}, u32[]{:S(2)}, u32[]{:S(2)}) collective-permute-start(bf16[264,128]{1,0:T(8,128)(2,1)S(1)} %shard_map.141.refs_0_), channel_id=1, source_target_pairs={{0,6},{1,7},{2,4},{3,5},{4,2},{5,3},{6,0},{7,1},{8,14},{9,15},{10,... | collective-permute-start | bytes 202760 | tf_op jit(solution)/shard_map/ppermute | solution.py:61
  25.9 3.2 %collective-permute-done.4.refs_2_ = bf16[264,128]{1,0:T(8,128)(2,1)S(1)} collective-permute-done((bf16[264,128]{1,0:T(8,128)(2,1)S(1)}, bf16[264,128]{1,0:T(8,128)(2,1)S(1)}, u32[]{:S(2)}, u32[]{:S(2)}) %collective-permute-start.4) | collective-permute-done | bytes 67616 | tf_op jit(solution)/shard_map/ppermute | solution.py:61
  29.0 0.0 collective-permute-start.12
  29.0 0.0 collective-permute-done.5.refs_3_
  29.1 0.5 shard_map.145
  29.5 0.0 collective-permute-done.8.w2_ref
  29.5 0.3 shard_map.146.refs_0_
  29.8 2.6 %collective-permute-start.10 = (bf16[32,1024]{1,0:T(8,128)(2,1)S(1)}, bf16[32,1024]{1,0:T(8,128)(2,1)S(1)}, u32[]{:S(2)}, u32[]{:S(2)}) collective-permute-start(bf16[32,1024]{1,0:T(8,128)(2,1)S(1)} %shard_map.146.refs_0_), channel_id=1, source_target_pairs={{0,16},{8,24},{16,0},{24,8},{1,17},{9,25},{17,1},{25,9},{2,18},{10... | collective-permute-start | bytes 196616 | tf_op jit(solution)/shard_map/ppermute | solution.py:61
  32.5 1.0 %collective-permute-start.11 = (bf16[32,1024]{1,0:T(8,128)(2,1)S(1)}, bf16[32,1024]{1,0:T(8,128)(2,1)S(1)}, u32[]{:S(2)}, u32[]{:S(2)}) collective-permute-start(bf16[32,1024]{1,0:T(8,128)(2,1)S(1)} %shard_map.146.refs_0_), channel_id=1, source_target_pairs={{0,24},{8,16},{16,8},{24,0},{1,25},{9,17},{17,9},{25,1},{2,26},{10... | collective-permute-start | bytes 196616 | tf_op jit(solution)/shard_map/ppermute | solution.py:61
  33.5 0.0 collective-permute-done.12.refs_7_
  33.5 0.5 collective-permute-start.9
  34.0 0.0 collective-permute-done.13.refs_8_
  34.0 0.0 collective-permute-done.14.refs_9_
  34.0 1.9 %collective-permute-done.10.refs_2_ = bf16[32,1024]{1,0:T(8,128)(2,1)S(1)} collective-permute-done((bf16[32,1024]{1,0:T(8,128)(2,1)S(1)}, bf16[32,1024]{1,0:T(8,128)(2,1)S(1)}, u32[]{:S(2)}, u32[]{:S(2)}) %collective-permute-start.10) | collective-permute-done | bytes 65568 | tf_op jit(solution)/shard_map/ppermute | solution.py:61
  35.9 1.9 %collective-permute-done.11.refs_3_ = bf16[32,1024]{1,0:T(8,128)(2,1)S(1)} collective-permute-done((bf16[32,1024]{1,0:T(8,128)(2,1)S(1)}, bf16[32,1024]{1,0:T(8,128)(2,1)S(1)}, u32[]{:S(2)}, u32[]{:S(2)}) %collective-permute-start.11) | collective-permute-done | bytes 65568 | tf_op jit(solution)/shard_map/ppermute | solution.py:61
  37.8 0.1 collective-permute-done.9.refs_1_
  37.9 0.4 shard_map.147
  38.3 1.5 %collective-permute-start.15 = (bf16[264,128]{1,0:T(8,128)(2,1)S(1)}, bf16[264,128]{1,0:T(8,128)(2,1)S(1)}, u32[]{:S(2)}, u32[]{:S(2)}) collective-permute-start(bf16[264,128]{1,0:T(8,128)(2,1)S(1)} %get-tuple-element.22.refs_0_), channel_id=1, source_target_pairs={{0,2},{1,3},{2,0},{3,1},{4,6},{5,7},{6,4},{7,5},{8,10},{9,11},{10,... | collective-permute-start | bytes 202760 | tf_op jit(solution)/shard_map/ppermute | solution.py:61
  39.8 1.4 %collective-permute-start.16 = (bf16[264,128]{1,0:T(8,128)(2,1)S(1)}, bf16[264,128]{1,0:T(8,128)(2,1)S(1)}, u32[]{:S(2)}, u32[]{:S(2)}) collective-permute-start(bf16[264,128]{1,0:T(8,128)(2,1)S(1)} %get-tuple-element.22.refs_0_), channel_id=1, source_target_pairs={{0,4},{1,5},{2,6},{3,7},{4,0},{5,1},{6,2},{7,3},{8,12},{9,13},{10,... | collective-permute-start | bytes 202760 | tf_op jit(solution)/shard_map/ppermute | solution.py:61
  41.3 1.5 %collective-permute-start.17 = (bf16[264,128]{1,0:T(8,128)(2,1)S(1)}, bf16[264,128]{1,0:T(8,128)(2,1)S(1)}, u32[]{:S(2)}, u32[]{:S(2)}) collective-permute-start(bf16[264,128]{1,0:T(8,128)(2,1)S(1)} %get-tuple-element.22.refs_0_), channel_id=1, source_target_pairs={{0,6},{1,7},{2,4},{3,5},{4,2},{5,3},{6,0},{7,1},{8,14},{9,15},{10,... | collective-permute-start | bytes 202760 | tf_op jit(solution)/shard_map/ppermute | solution.py:61
  42.7 0.3 collective-permute-done.15.refs_1_
  43.0 3.4 %collective-permute-done.16.refs_2_ = bf16[264,128]{1,0:T(8,128)(2,1)S(1)} collective-permute-done((bf16[264,128]{1,0:T(8,128)(2,1)S(1)}, bf16[264,128]{1,0:T(8,128)(2,1)S(1)}, u32[]{:S(2)}, u32[]{:S(2)}) %collective-permute-start.16) | collective-permute-done | bytes 67616 | tf_op jit(solution)/shard_map/ppermute | solution.py:61
  46.5 1.0 %collective-permute-done.17.refs_3_ = bf16[264,128]{1,0:T(8,128)(2,1)S(1)} collective-permute-done((bf16[264,128]{1,0:T(8,128)(2,1)S(1)}, bf16[264,128]{1,0:T(8,128)(2,1)S(1)}, u32[]{:S(2)}, u32[]{:S(2)}) %collective-permute-start.17) | collective-permute-done | bytes 67616 | tf_op jit(solution)/shard_map/ppermute | solution.py:61
  47.4 0.5 shard_map.148
  47.9 0.1 collective-permute-start.18
  48.0 0.6 %pad_maximum_fusion = bf16[2,3,8,512]{3,2,1,0:T(8,128)(2,1)} fusion(bf16[1,3,8,512]{3,2,1,0:T(8,128)(2,1)S(1)} %get-tuple-element.36, bf16[1,3,8,512]{3,2,1,0:T(8,128)(2,1)S(1)} %get-tuple-element.35), kind=kLoop, calls=%fused_computation | loop fusion | flops 24576 | bytes 98304 | tf_op jit(solution)/shard_map/stack | solution.py:398
  48.6 0.6 collective-permute-done.18.other_ref
  49.2 0.3 shard_map.149
  49.5 1.8 %collective-permute-start.19 = (bf16[16,512]{1,0:T(8,128)(2,1)S(1)}, bf16[16,512]{1,0:T(8,128)(2,1)S(1)}, u32[]{:S(2)}, u32[]{:S(2)}) collective-permute-start(bf16[16,512]{1,0:T(8,128)(2,1)S(1)} %get-tuple-element.26), channel_id=1, source_target_pairs={{0,8},{8,0},{16,24},{24,16},{1,9},{9,1},{17,25},{25,17},{2,10},{10... | collective-permute-start | bytes 49160 | tf_op jit(solution)/shard_map/ppermute | solution.py:61
  51.3 1.3 %collective-permute-start.20 = (bf16[16,512]{1,0:T(8,128)(2,1)S(1)}, bf16[16,512]{1,0:T(8,128)(2,1)S(1)}, u32[]{:S(2)}, u32[]{:S(2)}) collective-permute-start(bf16[16,512]{1,0:T(8,128)(2,1)S(1)} %get-tuple-element.27), channel_id=1, source_target_pairs={{0,16},{8,24},{16,0},{24,8},{1,17},{9,25},{17,1},{25,9},{2,18},{10... | collective-permute-start | bytes 49160 | tf_op jit(solution)/shard_map/ppermute | solution.py:61
  52.5 0.5 collective-permute-start.21
  53.1 0.6 %pad_maximum_fusion.1 = f32[2,8,512]{2,1,0:T(8,128)} fusion(f32[1,8,512]{2,1,0:T(8,128)S(1)} %bitcast.20, f32[1,8,512]{2,1,0:T(8,128)S(1)} %bitcast.19), kind=kLoop, calls=%fused_computation.1 | loop fusion | flops 8192 | bytes 65536 | tf_op jit(solution)/shard_map/stack | solution.py:398
  53.7 0.0 collective-permute-done.19.refs_0_
  53.7 1.3 %collective-permute-done.20.refs_1_ = bf16[16,512]{1,0:T(8,128)(2,1)S(1)} collective-permute-done((bf16[16,512]{1,0:T(8,128)(2,1)S(1)}, bf16[16,512]{1,0:T(8,128)(2,1)S(1)}, u32[]{:S(2)}, u32[]{:S(2)}) %collective-permute-start.20) | collective-permute-done | bytes 16416 | tf_op jit(solution)/shard_map/ppermute | solution.py:61
  55.0 2.2 %collective-permute-done.21.refs_2_ = bf16[16,512]{1,0:T(8,128)(2,1)S(1)} collective-permute-done((bf16[16,512]{1,0:T(8,128)(2,1)S(1)}, bf16[16,512]{1,0:T(8,128)(2,1)S(1)}, u32[]{:S(2)}, u32[]{:S(2)}) %collective-permute-start.21) | collective-permute-done | bytes 16416 | tf_op jit(solution)/shard_map/ppermute | solution.py:61
  57.2 0.6 %shard_map.150 = bf16[16,512]{1,0:T(8,128)(2,1)} custom-call(f32[16,512]{1,0:T(8,128)S(1)} %get-tuple-element.25.own_ref, bf16[16,512]{1,0:T(8,128)(2,1)S(1)} %collective-permute-done.19.refs_0_, bf16[16,512]{1,0:T(8,128)(2,1)S(1)} %collective-permute-done.20.refs_1_, bf16[16,512]{1,0:T(8,128)(2,1)S(1)} %collective-permute-done.21.refs_2_), custom_call_target="tpu_custom_call" | custom-call | flops 1000000 | bytes 1048576 | tf_op jit(solution)/shard_map/pallas_call | solution.py:21
  (20 shorter events, 0.1 us)
Async XLA Ops:
  0.6 28.9 %collective-permute-start.8 = (bf16[2,512,512]{2,1,0:T(8,128)(2,1)}, bf16[2,512,512]{2,1,0:T(8,128)(2,1)S(1)}, u32[]{:S(2)}, u32[]{:S(2)}) collective-permute-start(bf16[2,512,512]{2,1,0:T(8,128)(2,1)} %w_ref.3), channel_id=1, source_target_pairs={{0,1},{1,0},{2,3},{3,2},{4,5},{5,4},{6,7},{7,6},{8,9},{9,8},{10,11... | collective-permute-start | bytes 3145736 | tf_op jit(solution)/shard_map/ppermute | solution.py:61
  1.2 32.8 %collective-permute-start.13 = (bf16[2,512,512]{2,1,0:T(8,128)(2,1)}, bf16[2,512,512]{2,1,0:T(8,128)(2,1)S(1)}, u32[]{:S(2)}, u32[]{:S(2)}) collective-permute-start(bf16[2,512,512]{2,1,0:T(8,128)(2,1)} %refs_5_.1), channel_id=1, source_target_pairs={{0,1},{1,0},{2,3},{3,2},{4,5},{5,4},{6,7},{7,6},{8,9},{9,8},{10,11... | collective-permute-start | bytes 3145736 | tf_op jit(solution)/shard_map/ppermute | solution.py:61
  1.3 32.7 %collective-permute-start.14 = (bf16[2,512,512]{2,1,0:T(8,128)(2,1)}, bf16[2,512,512]{2,1,0:T(8,128)(2,1)S(1)}, u32[]{:S(2)}, u32[]{:S(2)}) collective-permute-start(bf16[2,512,512]{2,1,0:T(8,128)(2,1)} %refs_6_.4), channel_id=1, source_target_pairs={{0,1},{1,0},{2,3},{3,2},{4,5},{5,4},{6,7},{7,6},{8,9},{9,8},{10,11... | collective-permute-start | bytes 3145736 | tf_op jit(solution)/shard_map/ppermute | solution.py:61
  1.7 4.5 %collective-permute-start = (bf16[1,16,512]{2,1,0:T(8,128)(2,1)}, bf16[1,16,512]{2,1,0:T(8,128)(2,1)S(1)}, u32[]{:S(2)}, u32[]{:S(2)}) collective-permute-start(bf16[1,16,512]{2,1,0:T(8,128)(2,1)} %bitcast.17), channel_id=1, source_target_pairs={{0,8},{8,0},{16,24},{24,16},{1,9},{9,1},{17,25},{25,17},{2,10},{10... | collective-permute-start | bytes 49160 | tf_op jit(solution)/shard_map/ppermute | solution.py:61
  6.2 0.7 %copy-start.9 = (bf16[16,512]{1,0:T(8,128)(2,1)S(1)}, bf16[16,512]{1,0:T(8,128)(2,1)}, u32[]{:S(2)}) copy-start(bf16[16,512]{1,0:T(8,128)(2,1)} %param.12) | copy-start | bytes 49156
  6.9 2.1 %copy-start.11 = (s32[8]{0:T(128)S(1)}, s32[8]{0:T(128)}, u32[]{:S(2)}) copy-start(s32[8]{0:T(128)} %param.21) | copy-start | bytes 100
  6.9 4.6 %collective-permute-start.1 = (bf16[2,16,512]{2,1,0:T(8,128)(2,1)S(1)}, bf16[2,16,512]{2,1,0:T(8,128)(2,1)S(1)}, u32[]{:S(2)}, u32[]{:S(2)}) collective-permute-start(bf16[2,16,512]{2,1,0:T(8,128)(2,1)S(1)} %shard_map.139.low_ref), channel_id=1, source_target_pairs={{0,16},{8,24},{16,0},{24,8},{1,17},{9,25},{17,1},{25,9},{2,18},{10... | collective-permute-start | bytes 98312 | tf_op jit(solution)/shard_map/ppermute | solution.py:61
  9.0 0.8 %copy-start.5 = (bf16[2,3,8,512]{3,2,1,0:T(8,128)(2,1)S(1)}, bf16[2,3,8,512]{3,2,1,0:T(8,128)(2,1)}, u32[]{:S(2)}) copy-start(bf16[2,3,8,512]{3,2,1,0:T(8,128)(2,1)} %conv_ref.1) | copy-start | bytes 147460
  9.0 0.8 %copy-start.6 = (bf16[2,4,512]{2,1,0:T(4,128)(2,1)S(1)}, bf16[2,4,512]{2,1,0:T(4,128)(2,1)}, u32[]{:S(2)}) copy-start(bf16[2,4,512]{2,1,0:T(4,128)(2,1)} %refs_6_.5) | copy-start | bytes 24580
  9.0 0.8 %copy-start.7 = (f32[2,8,512]{2,1,0:T(8,128)S(1)}, f32[2,8,512]{2,1,0:T(8,128)}, u32[]{:S(2)}) copy-start(f32[2,8,512]{2,1,0:T(8,128)} %rec_ref.1) | copy-start | bytes 98308
  9.0 2.5 %copy-start.1 = (bf16[2,512,512]{2,1,0:T(8,128)(2,1)S(1)}, bf16[2,512,512]{2,1,0:T(8,128)(2,1)}, u32[]{:S(2)}) copy-start(bf16[2,512,512]{2,1,0:T(8,128)(2,1)} %refs_5_.1) | copy-start | bytes 3145732
  9.0 2.5 %copy-start.2 = (bf16[2,512,512]{2,1,0:T(8,128)(2,1)S(1)}, bf16[2,512,512]{2,1,0:T(8,128)(2,1)}, u32[]{:S(2)}) copy-start(bf16[2,512,512]{2,1,0:T(8,128)(2,1)} %refs_6_.4) | copy-start | bytes 3145732
  9.8 1.7 %copy-start.10 = (f32[2,512]{1,0:T(2,128)S(1)}, f32[2,512]{1,0:T(2,128)}, u32[]{:S(2)}) copy-start(f32[2,512]{1,0:T(2,128)} %refs_4_.1) | copy-start | bytes 12292
  9.9 4.3 %collective-permute-start.6 = (f32[1,2,2,8,512]{4,3,2,1,0:T(8,128)S(1)}, f32[1,2,2,8,512]{4,3,2,1,0:T(8,128)S(1)}, u32[]{:S(2)}, u32[]{:S(2)}) collective-permute-start(f32[1,2,2,8,512]{4,3,2,1,0:T(8,128)S(1)} %bitcast.15), channel_id=1, source_target_pairs={{0,2},{1,3},{2,0},{3,1},{4,6},{5,7},{6,4},{7,5},{8,10},{9,11},{10,... | collective-permute-start | bytes 196616 | tf_op jit(solution)/shard_map/ppermute | solution.py:61
  11.5 17.5 %copy-start.3 = (bf16[2,4,128,128]{3,2,1,0:T(8,128)(2,1)S(1)}, bf16[2,4,128,128]{3,2,1,0:T(8,128)(2,1)}, u32[]{:S(2)}) copy-start(bf16[2,4,128,128]{3,2,1,0:T(8,128)(2,1)} %refs_8_.3) | copy-start | bytes 786436
  11.5 17.5 %copy-start.4 = (bf16[2,4,128,128]{3,2,1,0:T(8,128)(2,1)S(1)}, bf16[2,4,128,128]{3,2,1,0:T(8,128)(2,1)}, u32[]{:S(2)}) copy-start(bf16[2,4,128,128]{3,2,1,0:T(8,128)(2,1)} %refs_9_.3) | copy-start | bytes 786436
  11.5 17.5 %copy-start.8 = (f32[2,512]{1,0:T(2,128)S(1)}, f32[2,512]{1,0:T(2,128)}, u32[]{:S(2)}) copy-start(f32[2,512]{1,0:T(2,128)} %refs_7_.3) | copy-start | bytes 12292
  11.9 17.6 %copy-start = (bf16[2,512,512]{2,1,0:T(8,128)(2,1)S(1)}, bf16[2,512,512]{2,1,0:T(8,128)(2,1)}, u32[]{:S(2)}) copy-start(bf16[2,512,512]{2,1,0:T(8,128)(2,1)} %w_ref.3) | copy-start | bytes 3145732
  11.9 4.9 %collective-permute-start.2 = (bf16[392,128]{1,0:T(8,128)(2,1)S(1)}, bf16[392,128]{1,0:T(8,128)(2,1)S(1)}, u32[]{:S(2)}, u32[]{:S(2)}) collective-permute-start(bf16[392,128]{1,0:T(8,128)(2,1)S(1)} %get-tuple-element.19), channel_id=1, source_target_pairs={{0,1},{1,0},{2,3},{3,2},{4,5},{5,4},{6,7},{7,6},{8,9},{9,8},{10,11... | collective-permute-start | bytes 301064 | tf_op jit(solution)/shard_map/ppermute | solution.py:61
  14.2 7.5 %collective-permute-start.7 = (f32[2,2,2,8,512]{4,3,2,1,0:T(8,128)S(1)}, f32[2,2,2,8,512]{4,3,2,1,0:T(8,128)S(1)}, u32[]{:S(2)}, u32[]{:S(2)}) collective-permute-start(f32[2,2,2,8,512]{4,3,2,1,0:T(8,128)S(1)} %shard_map.144.refs_4_), channel_id=1, source_target_pairs={{0,4},{1,5},{2,6},{3,7},{4,0},{5,1},{6,2},{7,3},{8,12},{9,13},{10,... | collective-permute-start | bytes 393224 | tf_op jit(solution)/shard_map/ppermute | solution.py:61
  16.9 5.9 %collective-permute-start.3 = (bf16[264,128]{1,0:T(8,128)(2,1)S(1)}, bf16[264,128]{1,0:T(8,128)(2,1)S(1)}, u32[]{:S(2)}, u32[]{:S(2)}) collective-permute-start(bf16[264,128]{1,0:T(8,128)(2,1)S(1)} %shard_map.141.refs_0_), channel_id=1, source_target_pairs={{0,2},{1,3},{2,0},{3,1},{4,6},{5,7},{6,4},{7,5},{8,10},{9,11},{10,... | collective-permute-start | bytes 202760 | tf_op jit(solution)/shard_map/ppermute | solution.py:61
  21.7 7.3 %collective-permute-start.4 = (bf16[264,128]{1,0:T(8,128)(2,1)S(1)}, bf16[264,128]{1,0:T(8,128)(2,1)S(1)}, u32[]{:S(2)}, u32[]{:S(2)}) collective-permute-start(bf16[264,128]{1,0:T(8,128)(2,1)S(1)} %shard_map.141.refs_0_), channel_id=1, source_target_pairs={{0,4},{1,5},{2,6},{3,7},{4,0},{5,1},{6,2},{7,3},{8,12},{9,13},{10,... | collective-permute-start | bytes 202760 | tf_op jit(solution)/shard_map/ppermute | solution.py:61
  22.8 6.2 %collective-permute-start.5 = (bf16[264,128]{1,0:T(8,128)(2,1)S(1)}, bf16[264,128]{1,0:T(8,128)(2,1)S(1)}, u32[]{:S(2)}, u32[]{:S(2)}) collective-permute-start(bf16[264,128]{1,0:T(8,128)(2,1)S(1)} %shard_map.141.refs_0_), channel_id=1, source_target_pairs={{0,6},{1,7},{2,4},{3,5},{4,2},{5,3},{6,0},{7,1},{8,14},{9,15},{10,... | collective-permute-start | bytes 202760 | tf_op jit(solution)/shard_map/ppermute | solution.py:61
  29.0 4.4 %collective-permute-start.12 = (f32[2,512]{1,0:T(2,128)S(1)}, f32[2,512]{1,0:T(2,128)S(1)}, u32[]{:S(2)}, u32[]{:S(2)}) collective-permute-start(f32[2,512]{1,0:T(2,128)S(1)} %copy-done.10), channel_id=1, source_target_pairs={{0,1},{1,0},{2,3},{3,2},{4,5},{5,4},{6,7},{7,6},{8,9},{9,8},{10,11... | collective-permute-start | bytes 12296 | tf_op jit(solution)/shard_map/ppermute | solution.py:61
  29.8 6.1 %collective-permute-start.10 = (bf16[32,1024]{1,0:T(8,128)(2,1)S(1)}, bf16[32,1024]{1,0:T(8,128)(2,1)S(1)}, u32[]{:S(2)}, u32[]{:S(2)}) collective-permute-start(bf16[32,1024]{1,0:T(8,128)(2,1)S(1)} %shard_map.146.refs_0_), channel_id=1, source_target_pairs={{0,16},{8,24},{16,0},{24,8},{1,17},{9,25},{17,1},{25,9},{2,18},{10... | collective-permute-start | bytes 196616 | tf_op jit(solution)/shard_map/ppermute | solution.py:61
  32.5 5.4 %collective-permute-start.11 = (bf16[32,1024]{1,0:T(8,128)(2,1)S(1)}, bf16[32,1024]{1,0:T(8,128)(2,1)S(1)}, u32[]{:S(2)}, u32[]{:S(2)}) collective-permute-start(bf16[32,1024]{1,0:T(8,128)(2,1)S(1)} %shard_map.146.refs_0_), channel_id=1, source_target_pairs={{0,24},{8,16},{16,8},{24,0},{1,25},{9,17},{17,9},{25,1},{2,26},{10... | collective-permute-start | bytes 196616 | tf_op jit(solution)/shard_map/ppermute | solution.py:61
  33.5 4.4 %collective-permute-start.9 = (bf16[32,1024]{1,0:T(8,128)(2,1)S(1)}, bf16[32,1024]{1,0:T(8,128)(2,1)S(1)}, u32[]{:S(2)}, u32[]{:S(2)}) collective-permute-start(bf16[32,1024]{1,0:T(8,128)(2,1)S(1)} %shard_map.146.refs_0_), channel_id=1, source_target_pairs={{0,8},{8,0},{16,24},{24,16},{1,9},{9,1},{17,25},{25,17},{2,10},{10... | collective-permute-start | bytes 196616 | tf_op jit(solution)/shard_map/ppermute | solution.py:61
  38.3 4.7 %collective-permute-start.15 = (bf16[264,128]{1,0:T(8,128)(2,1)S(1)}, bf16[264,128]{1,0:T(8,128)(2,1)S(1)}, u32[]{:S(2)}, u32[]{:S(2)}) collective-permute-start(bf16[264,128]{1,0:T(8,128)(2,1)S(1)} %get-tuple-element.22.refs_0_), channel_id=1, source_target_pairs={{0,2},{1,3},{2,0},{3,1},{4,6},{5,7},{6,4},{7,5},{8,10},{9,11},{10,... | collective-permute-start | bytes 202760 | tf_op jit(solution)/shard_map/ppermute | solution.py:61
  39.8 6.6 %collective-permute-start.16 = (bf16[264,128]{1,0:T(8,128)(2,1)S(1)}, bf16[264,128]{1,0:T(8,128)(2,1)S(1)}, u32[]{:S(2)}, u32[]{:S(2)}) collective-permute-start(bf16[264,128]{1,0:T(8,128)(2,1)S(1)} %get-tuple-element.22.refs_0_), channel_id=1, source_target_pairs={{0,4},{1,5},{2,6},{3,7},{4,0},{5,1},{6,2},{7,3},{8,12},{9,13},{10,... | collective-permute-start | bytes 202760 | tf_op jit(solution)/shard_map/ppermute | solution.py:61
  41.3 6.2 %collective-permute-start.17 = (bf16[264,128]{1,0:T(8,128)(2,1)S(1)}, bf16[264,128]{1,0:T(8,128)(2,1)S(1)}, u32[]{:S(2)}, u32[]{:S(2)}) collective-permute-start(bf16[264,128]{1,0:T(8,128)(2,1)S(1)} %get-tuple-element.22.refs_0_), channel_id=1, source_target_pairs={{0,6},{1,7},{2,4},{3,5},{4,2},{5,3},{6,0},{7,1},{8,14},{9,15},{10,... | collective-permute-start | bytes 202760 | tf_op jit(solution)/shard_map/ppermute | solution.py:61
  47.9 1.3 %collective-permute-start.18 = (bf16[40,512]{1,0:T(8,128)(2,1)S(1)}, bf16[40,512]{1,0:T(8,128)(2,1)S(1)}, u32[]{:S(2)}, u32[]{:S(2)}) collective-permute-start(bf16[40,512]{1,0:T(8,128)(2,1)S(1)} %get-tuple-element.24.own_ref), channel_id=1, source_target_pairs={{0,1},{1,0},{2,3},{3,2},{4,5},{5,4},{6,7},{7,6},{8,9},{9,8},{10,11... | collective-permute-start | bytes 122888 | tf_op jit(solution)/shard_map/ppermute | solution.py:61
  49.5 4.2 %collective-permute-start.19 = (bf16[16,512]{1,0:T(8,128)(2,1)S(1)}, bf16[16,512]{1,0:T(8,128)(2,1)S(1)}, u32[]{:S(2)}, u32[]{:S(2)}) collective-permute-start(bf16[16,512]{1,0:T(8,128)(2,1)S(1)} %get-tuple-element.26), channel_id=1, source_target_pairs={{0,8},{8,0},{16,24},{24,16},{1,9},{9,1},{17,25},{25,17},{2,10},{10... | collective-permute-start | bytes 49160 | tf_op jit(solution)/shard_map/ppermute | solution.py:61
  51.3 3.7 %collective-permute-start.20 = (bf16[16,512]{1,0:T(8,128)(2,1)S(1)}, bf16[16,512]{1,0:T(8,128)(2,1)S(1)}, u32[]{:S(2)}, u32[]{:S(2)}) collective-permute-start(bf16[16,512]{1,0:T(8,128)(2,1)S(1)} %get-tuple-element.27), channel_id=1, source_target_pairs={{0,16},{8,24},{16,0},{24,8},{1,17},{9,25},{17,1},{25,9},{2,18},{10... | collective-permute-start | bytes 49160 | tf_op jit(solution)/shard_map/ppermute | solution.py:61
  52.5 4.6 %collective-permute-start.21 = (bf16[16,512]{1,0:T(8,128)(2,1)S(1)}, bf16[16,512]{1,0:T(8,128)(2,1)S(1)}, u32[]{:S(2)}, u32[]{:S(2)}) collective-permute-start(bf16[16,512]{1,0:T(8,128)(2,1)S(1)} %get-tuple-element.28), channel_id=1, source_target_pairs={{0,24},{8,16},{16,8},{24,0},{1,25},{9,17},{17,9},{25,1},{2,26},{10... | collective-permute-start | bytes 49160 | tf_op jit(solution)/shard_map/ppermute | solution.py:61

commit v2 on v1

--- a/solution.py
+++ b/solution.py
@@ -92,7 +92,7 @@
     out_ref[...] = jnp.broadcast_to(as_column(lengths_ref[...]), out_ref.shape)
 
 
-def state_kernel(lengths_ref, taps_ref, conv_ref, rec_ref, out_ref):
+def state_kernel(lengths_ref, taps_ref, conv_ref, rec_ref, out_ref, low_ref):
     live = lengths_ref[:, 0:1]
     depth = conv_ref.shape[1]
     for layer in range(conv_ref.shape[0]):
@@ -102,6 +102,7 @@
             old = old + tap * jnp.where(back < live, conv_ref[layer, depth - back].astype(F32), 0.0)
         out_ref[layer, 0] = old
         out_ref[layer, 1] = jnp.where(live > 1, rec_ref[layer], 0.0)
+    low_ref[...] = out_ref[...].astype(BF16)
 
 
 LANES = 128
@@ -215,11 +216,11 @@
 def recurrence_kernel(lay, layer, features, *refs):
     zs = lay.dp // 2
     sums, refs = refs[:zs], refs[zs:]
-    low_ref, high_ref, taps_ref, decay_ref, wr_ref, wj_ref, *extra, readout_ref, value_ref, rec_ref = refs
+    own_ref, low_ref, high_ref, taps_ref, decay_ref, wr_ref, wj_ref, *extra, readout_ref, value_ref, rec_ref = refs
     rows, half, width = lay.rows, lay.half, taps_ref.shape[2]
-    states = [entry((low_ref, high_ref), m) for m in range(zs)]
-    old = jnp.concatenate([state[layer, 0] for state in states], axis=0)
-    previous = jnp.concatenate([state[layer, 1] for state in states], axis=0)
+    states = [own_ref] + [entry((low_ref, high_ref), m) for m in range(1, zs)]
+    old = jnp.concatenate([state[layer, 0].astype(F32) for state in states], axis=0)
+    previous = jnp.concatenate([state[layer, 1].astype(F32) for state in states], axis=0)
     value_in = gate_in = square = None
     for mask, part in enumerate(sums):
         terms = [by_owner(t, mask, zs, rows) for t in unpack(part[...].astype(F32), half, width)]
@@ -317,16 +318,16 @@
     tall = packed_rows(half, width)
     bits = lambda n: [1 << k for k in range(n.bit_length() - 1)]
     live = call(length_kernel, shape((lay.rows, LANES), jnp.int32), lengths[None, :], flops=COVER)
-    state = call(
+    state, low = call(
         state_kernel,
-        shape((layers, 2, lay.rows, width), F32),
+        [shape((layers, 2, lay.rows, width), t) for t in (F32, BF16)],
         live,
         conv_weight,
         conv_state,
         rec_state,
     )
     rows = doubling(tokens, "tp", bits(tp))
-    states = doubling(state, "dp", [2 * m for m in bits(dp // 2)])
+    states = [state] + doubling(low, "dp", [2 * m for m in bits(dp // 2)])
     sent = half * depth // LANES
     block = [
         shape((half, width), BF16),
@@ -413,6 +414,7 @@
         P(None, None, "dp", "tp"),
         P(None, "dp", "tp"),
     )
+
     return jax.shard_map(
         blocks,
         mesh=mesh,

time: 58 us -> 60.4 us (1.041)
  local copies, waits for them, and re-layouts: 1.46 us -> 4.46 us
  waiting for transfers between devices: 23.1 us -> 22 us
    unnamed x24 -> x28, local copies, waits for them, and re-layouts: 1.45 us -> 4.46 us
    ppermute x22, waiting for transfers between devices: 23.1 us -> 22 us  [partner_exchange(): got.append(lax.ppermute(value, axis, [(i, i ^ m) for i in range(count)]))]
  transfers between devices with their start and end apart: 22 -> 22, of which waited for: 13 -> 15; matrix products, arithmetic and copies ran while one was open for 2% -> 2% of each run, Pallas kernels for 2% -> 2%
where the time goes in v2:
time: 60.4 us; the launch traced here: 60.1 us
  starting transfers between devices  28.5 us (47%)
  waiting for transfers between devices  22 us (36%)
  local copies, waits for them, and re-layouts  4.46 us (7%)
  Pallas kernels  3.08 us (5%)
  other arithmetic  1.25 us (2%)
  between operations  0.78 us (1%)
    ppermute x22, starting transfers between devices, partner_exchange(): got.append(lax.ppermute(value, axis, [(i, i ^ m) for i in range(count)]))  28.5 us
    ppermute x22, waiting for transfers between devices, partner_exchange(): got.append(lax.ppermute(value, axis, [(i, i ^ m) for i in range(count)]))  22 us
    unnamed x28, local copies, waits for them, and re-layouts  4.46 us
    pallas_call x12, Pallas kernels, call(): pl.pallas_call(kernel, out_shape=outs, in_specs=[spec] * len(args), out_s...  3.08 us
    another operation x3, other arithmetic, blocks(): return (mixed, jnp.stack(conv_list), jnp.stack(rec_list))  1.25 us
  transfers between devices with their start and end apart: 22, of which 15 were waited for; matrix products, arithmetic and copies ran while one was open for 2% of the time, Pallas kernels for 2%

profile of v2, /device:TPU:0, one launch (start us, length us, event | category | flops | bytes accessed | tf_op | source)
XLA Modules:
  0.0 60.1 jit_solution(13533938973895963910)
XLA Ops:
  0.6 0.6 collective-permute-start.8
  1.2 0.1 collective-permute-start.13
  1.3 0.4 collective-permute-start.14
  1.7 2.6 %collective-permute-start = (bf16[1,16,512]{2,1,0:T(8,128)(2,1)}, bf16[1,16,512]{2,1,0:T(8,128)(2,1)S(1)}, u32[]{:S(2)}, u32[]{:S(2)}) collective-permute-start(bf16[1,16,512]{2,1,0:T(8,128)(2,1)} %bitcast.17), channel_id=1, source_target_pairs={{0,8},{8,0},{16,24},{24,16},{1,9},{9,1},{17,25},{25,17},{2,10},{10... | collective-permute-start | bytes 49160 | tf_op jit(solution)/shard_map/ppermute | solution.py:61
  4.3 1.9 %collective-permute-done.second_ref = bf16[1,16,512]{2,1,0:T(8,128)(2,1)S(1)} collective-permute-done((bf16[1,16,512]{2,1,0:T(8,128)(2,1)}, bf16[1,16,512]{2,1,0:T(8,128)(2,1)S(1)}, u32[]{:S(2)}, u32[]{:S(2)}) %collective-permute-start) | collective-permute-done | bytes 16416 | tf_op jit(solution)/shard_map/ppermute | solution.py:61
  6.2 0.7 %copy-done.11 = bf16[16,512]{1,0:T(8,128)(2,1)S(1)} copy-done((bf16[16,512]{1,0:T(8,128)(2,1)S(1)}, bf16[16,512]{1,0:T(8,128)(2,1)}, u32[]{:S(2)}) %copy-start.11) | copy-done | bytes 16408
  6.9 2.1 %collective-permute-start.1 = (bf16[2,16,512]{2,1,0:T(8,128)(2,1)S(1)}, bf16[2,16,512]{2,1,0:T(8,128)(2,1)S(1)}, u32[]{:S(2)}, u32[]{:S(2)}) collective-permute-start(bf16[2,16,512]{2,1,0:T(8,128)(2,1)S(1)} %shard_map.139.low_ref), channel_id=1, source_target_pairs={{0,16},{8,24},{16,0},{24,8},{1,17},{9,25},{17,1},{25,9},{2,18},{10... | collective-permute-start | bytes 98312 | tf_op jit(solution)/shard_map/ppermute | solution.py:61
  9.0 1.9 %collective-permute-done.1.high_ref = bf16[2,16,512]{2,1,0:T(8,128)(2,1)S(1)} collective-permute-done((bf16[2,16,512]{2,1,0:T(8,128)(2,1)S(1)}, bf16[2,16,512]{2,1,0:T(8,128)(2,1)S(1)}, u32[]{:S(2)}, u32[]{:S(2)}) %collective-permute-start.1) | collective-permute-done | bytes 32800 | tf_op jit(solution)/shard_map/ppermute | solution.py:61
  10.9 1.2 %copy-done.1 = bf16[2,512,512]{2,1,0:T(8,128)(2,1)S(1)} copy-done((bf16[2,512,512]{2,1,0:T(8,128)(2,1)S(1)}, bf16[2,512,512]{2,1,0:T(8,128)(2,1)}, u32[]{:S(2)}) %copy-start.1) | copy-done | bytes 1048600
  12.1 1.2 %copy-done.3 = bf16[2,512,512]{2,1,0:T(8,128)(2,1)S(1)} copy-done((bf16[2,512,512]{2,1,0:T(8,128)(2,1)S(1)}, bf16[2,512,512]{2,1,0:T(8,128)(2,1)}, u32[]{:S(2)}) %copy-start.3) | copy-done | bytes 1048600
  13.3 0.3 shard_map.140
  13.6 0.0 copy-start.13
  13.7 0.1 collective-permute-start.2
  13.7 0.6 copy-done.13
  14.3 0.0 copy-start.6
  14.3 0.0 copy-start.10
  14.3 0.1 shard_map.142.lengths_ref
  14.4 0.7 %copy-done.7 = bf16[2,3,8,512]{3,2,1,0:T(8,128)(2,1)S(1)} copy-done((bf16[2,3,8,512]{3,2,1,0:T(8,128)(2,1)S(1)}, bf16[2,3,8,512]{3,2,1,0:T(8,128)(2,1)}, u32[]{:S(2)}) %copy-start.7) | copy-done | bytes 49176
  15.1 0.1 shard_map.143
  15.2 2.1 %collective-permute-start.6 = (bf16[1,2,2,8,512]{4,3,2,1,0:T(8,128)(2,1)S(1)}, bf16[1,2,2,8,512]{4,3,2,1,0:T(8,128)(2,1)S(1)}, u32[]{:S(2)}, u32[]{:S(2)}) collective-permute-start(bf16[1,2,2,8,512]{4,3,2,1,0:T(8,128)(2,1)S(1)} %bitcast.15), channel_id=1, source_target_pairs={{0,2},{1,3},{2,0},{3,1},{4,6},{5,7},{6,4},{7,5},{8,10},{9,11},{10,... | collective-permute-start | bytes 98312 | tf_op jit(solution)/shard_map/ppermute | solution.py:61
  17.3 1.9 %collective-permute-done.6.second_ref = bf16[1,2,2,8,512]{4,3,2,1,0:T(8,128)(2,1)S(1)} collective-permute-done((bf16[1,2,2,8,512]{4,3,2,1,0:T(8,128)(2,1)S(1)}, bf16[1,2,2,8,512]{4,3,2,1,0:T(8,128)(2,1)S(1)}, u32[]{:S(2)}, u32[]{:S(2)}) %collective-permute-start.6) | collective-permute-done | bytes 32800 | tf_op jit(solution)/shard_map/ppermute | solution.py:61
  19.2 3.0 %collective-permute-start.7 = (bf16[2,2,2,8,512]{4,3,2,1,0:T(8,128)(2,1)S(1)}, bf16[2,2,2,8,512]{4,3,2,1,0:T(8,128)(2,1)S(1)}, u32[]{:S(2)}, u32[]{:S(2)}) collective-permute-start(bf16[2,2,2,8,512]{4,3,2,1,0:T(8,128)(2,1)S(1)} %shard_map.144.refs_5_), channel_id=1, source_target_pairs={{0,4},{1,5},{2,6},{3,7},{4,0},{5,1},{6,2},{7,3},{8,12},{9,13},{10,... | collective-permute-start | bytes 196616 | tf_op jit(solution)/shard_map/ppermute | solution.py:61
  22.3 0.0 collective-permute-done.2.got_ref
  22.3 1.6 %collective-permute-start.3 = (bf16[264,128]{1,0:T(8,128)(2,1)S(1)}, bf16[264,128]{1,0:T(8,128)(2,1)S(1)}, u32[]{:S(2)}, u32[]{:S(2)}) collective-permute-start(bf16[264,128]{1,0:T(8,128)(2,1)S(1)} %shard_map.141.refs_0_), channel_id=1, source_target_pairs={{0,2},{1,3},{2,0},{3,1},{4,6},{5,7},{6,4},{7,5},{8,10},{9,11},{10,... | collective-permute-start | bytes 202760 | tf_op jit(solution)/shard_map/ppermute | solution.py:61
  23.9 0.7 %collective-permute-done.7.refs_6_ = bf16[2,2,2,8,512]{4,3,2,1,0:T(8,128)(2,1)S(1)} collective-permute-done((bf16[2,2,2,8,512]{4,3,2,1,0:T(8,128)(2,1)S(1)}, bf16[2,2,2,8,512]{4,3,2,1,0:T(8,128)(2,1)S(1)}, u32[]{:S(2)}, u32[]{:S(2)}) %collective-permute-start.7) | collective-permute-done | bytes 65568 | tf_op jit(solution)/shard_map/ppermute | solution.py:61
  24.6 2.9 %collective-permute-start.4 = (bf16[264,128]{1,0:T(8,128)(2,1)S(1)}, bf16[264,128]{1,0:T(8,128)(2,1)S(1)}, u32[]{:S(2)}, u32[]{:S(2)}) collective-permute-start(bf16[264,128]{1,0:T(8,128)(2,1)S(1)} %shard_map.141.refs_0_), channel_id=1, source_target_pairs={{0,4},{1,5},{2,6},{3,7},{4,0},{5,1},{6,2},{7,3},{8,12},{9,13},{10,... | collective-permute-start | bytes 202760 | tf_op jit(solution)/shard_map/ppermute | solution.py:61
  27.5 0.0 collective-permute-done.3.refs_1_
  27.5 1.5 %collective-permute-start.5 = (bf16[264,128]{1,0:T(8,128)(2,1)S(1)}, bf16[264,128]{1,0:T(8,128)(2,1)S(1)}, u32[]{:S(2)}, u32[]{:S(2)}) collective-permute-start(bf16[264,128]{1,0:T(8,128)(2,1)S(1)} %shard_map.141.refs_0_), channel_id=1, source_target_pairs={{0,6},{1,7},{2,4},{3,5},{4,2},{5,3},{6,0},{7,1},{8,14},{9,15},{10,... | collective-permute-start | bytes 202760 | tf_op jit(solution)/shard_map/ppermute | solution.py:61
  29.1 2.8 %collective-permute-done.4.refs_2_ = bf16[264,128]{1,0:T(8,128)(2,1)S(1)} collective-permute-done((bf16[264,128]{1,0:T(8,128)(2,1)S(1)}, bf16[264,128]{1,0:T(8,128)(2,1)S(1)}, u32[]{:S(2)}, u32[]{:S(2)}) %collective-permute-start.4) | collective-permute-done | bytes 67616 | tf_op jit(solution)/shard_map/ppermute | solution.py:61
  31.9 0.0 collective-permute-start.12
  31.9 1.8 %collective-permute-done.5.refs_3_ = bf16[264,128]{1,0:T(8,128)(2,1)S(1)} collective-permute-done((bf16[264,128]{1,0:T(8,128)(2,1)S(1)}, bf16[264,128]{1,0:T(8,128)(2,1)S(1)}, u32[]{:S(2)}, u32[]{:S(2)}) %collective-permute-start.5) | collective-permute-done | bytes 67616 | tf_op jit(solution)/shard_map/ppermute | solution.py:61
  33.7 0.5 shard_map.145
  34.2 0.0 collective-permute-done.8.w2_ref
  34.2 0.0 copy-start.2
  34.2 0.0 copy-start.4
  34.2 0.3 shard_map.146.refs_0_
  34.5 1.5 %collective-permute-start.10 = (bf16[32,1024]{1,0:T(8,128)(2,1)S(1)}, bf16[32,1024]{1,0:T(8,128)(2,1)S(1)}, u32[]{:S(2)}, u32[]{:S(2)}) collective-permute-start(bf16[32,1024]{1,0:T(8,128)(2,1)S(1)} %shard_map.146.refs_0_), channel_id=1, source_target_pairs={{0,16},{8,24},{16,0},{24,8},{1,17},{9,25},{17,1},{25,9},{2,18},{10... | collective-permute-start | bytes 196616 | tf_op jit(solution)/shard_map/ppermute | solution.py:61
  36.0 1.4 %collective-permute-start.11 = (bf16[32,1024]{1,0:T(8,128)(2,1)S(1)}, bf16[32,1024]{1,0:T(8,128)(2,1)S(1)}, u32[]{:S(2)}, u32[]{:S(2)}) collective-permute-start(bf16[32,1024]{1,0:T(8,128)(2,1)S(1)} %shard_map.146.refs_0_), channel_id=1, source_target_pairs={{0,24},{8,16},{16,8},{24,0},{1,25},{9,17},{17,9},{25,1},{2,26},{10... | collective-permute-start | bytes 196616 | tf_op jit(solution)/shard_map/ppermute | solution.py:61
  37.5 0.0 collective-permute-done.12.refs_7_
  37.5 0.5 collective-permute-start.9
  38.0 0.0 collective-permute-done.14.refs_9_
  38.0 1.4 %collective-permute-done.10.refs_2_ = bf16[32,1024]{1,0:T(8,128)(2,1)S(1)} collective-permute-done((bf16[32,1024]{1,0:T(8,128)(2,1)S(1)}, bf16[32,1024]{1,0:T(8,128)(2,1)S(1)}, u32[]{:S(2)}, u32[]{:S(2)}) %collective-permute-start.10) | collective-permute-done | bytes 65568 | tf_op jit(solution)/shard_map/ppermute | solution.py:61
  39.4 1.8 %collective-permute-done.11.refs_3_ = bf16[32,1024]{1,0:T(8,128)(2,1)S(1)} collective-permute-done((bf16[32,1024]{1,0:T(8,128)(2,1)S(1)}, bf16[32,1024]{1,0:T(8,128)(2,1)S(1)}, u32[]{:S(2)}, u32[]{:S(2)}) %collective-permute-start.11) | collective-permute-done | bytes 65568 | tf_op jit(solution)/shard_map/ppermute | solution.py:61
  41.2 0.5 collective-permute-done.9.refs_1_
  41.7 0.4 shard_map.147
  42.2 0.9 %collective-permute-start.15 = (bf16[264,128]{1,0:T(8,128)(2,1)S(1)}, bf16[264,128]{1,0:T(8,128)(2,1)S(1)}, u32[]{:S(2)}, u32[]{:S(2)}) collective-permute-start(bf16[264,128]{1,0:T(8,128)(2,1)S(1)} %get-tuple-element.26.refs_0_), channel_id=1, source_target_pairs={{0,2},{1,3},{2,0},{3,1},{4,6},{5,7},{6,4},{7,5},{8,10},{9,11},{10,... | collective-permute-start | bytes 202760 | tf_op jit(solution)/shard_map/ppermute | solution.py:61
  43.1 1.2 %collective-permute-start.16 = (bf16[264,128]{1,0:T(8,128)(2,1)S(1)}, bf16[264,128]{1,0:T(8,128)(2,1)S(1)}, u32[]{:S(2)}, u32[]{:S(2)}) collective-permute-start(bf16[264,128]{1,0:T(8,128)(2,1)S(1)} %get-tuple-element.26.refs_0_), channel_id=1, source_target_pairs={{0,4},{1,5},{2,6},{3,7},{4,0},{5,1},{6,2},{7,3},{8,12},{9,13},{10,... | collective-permute-start | bytes 202760 | tf_op jit(solution)/shard_map/ppermute | solution.py:61
  44.3 2.3 %collective-permute-start.17 = (bf16[264,128]{1,0:T(8,128)(2,1)S(1)}, bf16[264,128]{1,0:T(8,128)(2,1)S(1)}, u32[]{:S(2)}, u32[]{:S(2)}) collective-permute-start(bf16[264,128]{1,0:T(8,128)(2,1)S(1)} %get-tuple-element.26.refs_0_), channel_id=1, source_target_pairs={{0,6},{1,7},{2,4},{3,5},{4,2},{5,3},{6,0},{7,1},{8,14},{9,15},{10,... | collective-permute-start | bytes 202760 | tf_op jit(solution)/shard_map/ppermute | solution.py:61
  46.6 0.2 collective-permute-done.15.refs_1_
  46.8 2.3 %collective-permute-done.16.refs_2_ = bf16[264,128]{1,0:T(8,128)(2,1)S(1)} collective-permute-done((bf16[264,128]{1,0:T(8,128)(2,1)S(1)}, bf16[264,128]{1,0:T(8,128)(2,1)S(1)}, u32[]{:S(2)}, u32[]{:S(2)}) %collective-permute-start.16) | collective-permute-done | bytes 67616 | tf_op jit(solution)/shard_map/ppermute | solution.py:61
  49.1 1.4 %collective-permute-done.17.refs_3_ = bf16[264,128]{1,0:T(8,128)(2,1)S(1)} collective-permute-done((bf16[264,128]{1,0:T(8,128)(2,1)S(1)}, bf16[264,128]{1,0:T(8,128)(2,1)S(1)}, u32[]{:S(2)}, u32[]{:S(2)}) %collective-permute-start.17) | collective-permute-done | bytes 67616 | tf_op jit(solution)/shard_map/ppermute | solution.py:61
  50.5 0.5 shard_map.148
  51.0 0.1 collective-permute-start.18
  51.1 0.6 %pad_maximum_fusion = bf16[2,3,8,512]{3,2,1,0:T(8,128)(2,1)} fusion(bf16[1,3,8,512]{3,2,1,0:T(8,128)(2,1)S(1)} %get-tuple-element.40, bf16[1,3,8,512]{3,2,1,0:T(8,128)(2,1)S(1)} %get-tuple-element.39), kind=kLoop, calls=%fused_computation | loop fusion | flops 24576 | bytes 98304 | tf_op jit(solution)/shard_map/stack | solution.py:399
  51.7 0.6 collective-permute-done.18.other_ref
  52.3 0.3 shard_map.149
  52.6 1.0 %collective-permute-start.19 = (bf16[16,512]{1,0:T(8,128)(2,1)S(1)}, bf16[16,512]{1,0:T(8,128)(2,1)S(1)}, u32[]{:S(2)}, u32[]{:S(2)}) collective-permute-start(bf16[16,512]{1,0:T(8,128)(2,1)S(1)} %get-tuple-element.30), channel_id=1, source_target_pairs={{0,8},{8,0},{16,24},{24,16},{1,9},{9,1},{17,25},{25,17},{2,10},{10... | collective-permute-start | bytes 49160 | tf_op jit(solution)/shard_map/ppermute | solution.py:61
  53.6 1.3 %collective-permute-start.20 = (bf16[16,512]{1,0:T(8,128)(2,1)S(1)}, bf16[16,512]{1,0:T(8,128)(2,1)S(1)}, u32[]{:S(2)}, u32[]{:S(2)}) collective-permute-start(bf16[16,512]{1,0:T(8,128)(2,1)S(1)} %get-tuple-element.31), channel_id=1, source_target_pairs={{0,16},{8,24},{16,0},{24,8},{1,17},{9,25},{17,1},{25,9},{2,18},{10... | collective-permute-start | bytes 49160 | tf_op jit(solution)/shard_map/ppermute | solution.py:61
  54.8 1.3 %collective-permute-start.21 = (bf16[16,512]{1,0:T(8,128)(2,1)S(1)}, bf16[16,512]{1,0:T(8,128)(2,1)S(1)}, u32[]{:S(2)}, u32[]{:S(2)}) collective-permute-start(bf16[16,512]{1,0:T(8,128)(2,1)S(1)} %get-tuple-element.32), channel_id=1, source_target_pairs={{0,24},{8,16},{16,8},{24,0},{1,25},{9,17},{17,9},{25,1},{2,26},{10... | collective-permute-start | bytes 49160 | tf_op jit(solution)/shard_map/ppermute | solution.py:61
  56.1 0.6 %pad_maximum_fusion.1 = f32[2,8,512]{2,1,0:T(8,128)} fusion(f32[1,8,512]{2,1,0:T(8,128)S(1)} %bitcast.20, f32[1,8,512]{2,1,0:T(8,128)S(1)} %bitcast.19), kind=kLoop, calls=%fused_computation.1 | loop fusion | flops 8192 | bytes 65536 | tf_op jit(solution)/shard_map/stack | solution.py:399
  56.7 0.0 collective-permute-done.19.refs_0_
  56.7 0.6 collective-permute-done.20.refs_1_
  57.3 2.2 %collective-permute-done.21.refs_2_ = bf16[16,512]{1,0:T(8,128)(2,1)S(1)} collective-permute-done((bf16[16,512]{1,0:T(8,128)(2,1)S(1)}, bf16[16,512]{1,0:T(8,128)(2,1)S(1)}, u32[]{:S(2)}, u32[]{:S(2)}) %collective-permute-start.21) | collective-permute-done | bytes 16416 | tf_op jit(solution)/shard_map/ppermute | solution.py:61
  59.5 0.6 %shard_map.150 = bf16[16,512]{1,0:T(8,128)(2,1)} custom-call(f32[16,512]{1,0:T(8,128)S(1)} %get-tuple-element.29.own_ref, bf16[16,512]{1,0:T(8,128)(2,1)S(1)} %collective-permute-done.19.refs_0_, bf16[16,512]{1,0:T(8,128)(2,1)S(1)} %collective-permute-done.20.refs_1_, bf16[16,512]{1,0:T(8,128)(2,1)S(1)} %collective-permute-done.21.refs_2_), custom_call_target="tpu_custom_call" | custom-call | flops 1000000 | bytes 1048576 | tf_op jit(solution)/shard_map/pallas_call | solution.py:21
  (24 shorter events, 0.1 us)
Async XLA Ops:
  0.6 33.6 %collective-permute-start.8 = (bf16[2,512,512]{2,1,0:T(8,128)(2,1)}, bf16[2,512,512]{2,1,0:T(8,128)(2,1)S(1)}, u32[]{:S(2)}, u32[]{:S(2)}) collective-permute-start(bf16[2,512,512]{2,1,0:T(8,128)(2,1)} %w_ref.3), channel_id=1, source_target_pairs={{0,1},{1,0},{2,3},{3,2},{4,5},{5,4},{6,7},{7,6},{8,9},{9,8},{10,11... | collective-permute-start | bytes 3145736 | tf_op jit(solution)/shard_map/ppermute | solution.py:61
  1.2 36.8 %collective-permute-start.13 = (bf16[2,512,512]{2,1,0:T(8,128)(2,1)}, bf16[2,512,512]{2,1,0:T(8,128)(2,1)S(1)}, u32[]{:S(2)}, u32[]{:S(2)}) collective-permute-start(bf16[2,512,512]{2,1,0:T(8,128)(2,1)} %refs_5_.1), channel_id=1, source_target_pairs={{0,1},{1,0},{2,3},{3,2},{4,5},{5,4},{6,7},{7,6},{8,9},{9,8},{10,11... | collective-permute-start | bytes 3145736 | tf_op jit(solution)/shard_map/ppermute | solution.py:61
  1.3 36.7 %collective-permute-start.14 = (bf16[2,512,512]{2,1,0:T(8,128)(2,1)}, bf16[2,512,512]{2,1,0:T(8,128)(2,1)S(1)}, u32[]{:S(2)}, u32[]{:S(2)}) collective-permute-start(bf16[2,512,512]{2,1,0:T(8,128)(2,1)} %refs_6_.1), channel_id=1, source_target_pairs={{0,1},{1,0},{2,3},{3,2},{4,5},{5,4},{6,7},{7,6},{8,9},{9,8},{10,11... | collective-permute-start | bytes 3145736 | tf_op jit(solution)/shard_map/ppermute | solution.py:61
  1.7 4.5 %collective-permute-start = (bf16[1,16,512]{2,1,0:T(8,128)(2,1)}, bf16[1,16,512]{2,1,0:T(8,128)(2,1)S(1)}, u32[]{:S(2)}, u32[]{:S(2)}) collective-permute-start(bf16[1,16,512]{2,1,0:T(8,128)(2,1)} %bitcast.17), channel_id=1, source_target_pairs={{0,8},{8,0},{16,24},{24,16},{1,9},{9,1},{17,25},{25,17},{2,10},{10... | collective-permute-start | bytes 49160 | tf_op jit(solution)/shard_map/ppermute | solution.py:61
  6.2 0.7 %copy-start.11 = (bf16[16,512]{1,0:T(8,128)(2,1)S(1)}, bf16[16,512]{1,0:T(8,128)(2,1)}, u32[]{:S(2)}) copy-start(bf16[16,512]{1,0:T(8,128)(2,1)} %param.12) | copy-start | bytes 49156
  6.9 4.0 %copy-start.12 = (f32[2,512]{1,0:T(2,128)S(1)}, f32[2,512]{1,0:T(2,128)}, u32[]{:S(2)}) copy-start(f32[2,512]{1,0:T(2,128)} %refs_4_.1) | copy-start | bytes 12292
  6.9 3.9 %collective-permute-start.1 = (bf16[2,16,512]{2,1,0:T(8,128)(2,1)S(1)}, bf16[2,16,512]{2,1,0:T(8,128)(2,1)S(1)}, u32[]{:S(2)}, u32[]{:S(2)}) collective-permute-start(bf16[2,16,512]{2,1,0:T(8,128)(2,1)S(1)} %shard_map.139.low_ref), channel_id=1, source_target_pairs={{0,16},{8,24},{16,0},{24,8},{1,17},{9,25},{17,1},{25,9},{2,18},{10... | collective-permute-start | bytes 98312 | tf_op jit(solution)/shard_map/ppermute | solution.py:61
  10.9 1.2 %copy-start.1 = (bf16[2,512,512]{2,1,0:T(8,128)(2,1)S(1)}, bf16[2,512,512]{2,1,0:T(8,128)(2,1)}, u32[]{:S(2)}) copy-start(bf16[2,512,512]{2,1,0:T(8,128)(2,1)} %refs_5_.1) | copy-start | bytes 3145732
  12.1 1.2 %copy-start.3 = (bf16[2,512,512]{2,1,0:T(8,128)(2,1)S(1)}, bf16[2,512,512]{2,1,0:T(8,128)(2,1)}, u32[]{:S(2)}) copy-start(bf16[2,512,512]{2,1,0:T(8,128)(2,1)} %refs_6_.1) | copy-start | bytes 3145732
  13.6 0.7 %copy-start.13 = (s32[8]{0:T(128)S(1)}, s32[8]{0:T(128)}, u32[]{:S(2)}) copy-start(s32[8]{0:T(128)} %param.21) | copy-start | bytes 100
  13.7 8.6 %collective-permute-start.2 = (bf16[392,128]{1,0:T(8,128)(2,1)S(1)}, bf16[392,128]{1,0:T(8,128)(2,1)S(1)}, u32[]{:S(2)}, u32[]{:S(2)}) collective-permute-start(bf16[392,128]{1,0:T(8,128)(2,1)S(1)} %get-tuple-element.21), channel_id=1, source_target_pairs={{0,1},{1,0},{2,3},{3,2},{4,5},{5,4},{6,7},{7,6},{8,9},{9,8},{10,11... | collective-permute-start | bytes 301064 | tf_op jit(solution)/shard_map/ppermute | solution.py:61
  14.3 0.8 %copy-start.7 = (bf16[2,3,8,512]{3,2,1,0:T(8,128)(2,1)S(1)}, bf16[2,3,8,512]{3,2,1,0:T(8,128)(2,1)}, u32[]{:S(2)}) copy-start(bf16[2,3,8,512]{3,2,1,0:T(8,128)(2,1)} %conv_ref.1) | copy-start | bytes 147460
  14.3 0.8 %copy-start.8 = (bf16[2,4,512]{2,1,0:T(4,128)(2,1)S(1)}, bf16[2,4,512]{2,1,0:T(4,128)(2,1)}, u32[]{:S(2)}) copy-start(bf16[2,4,512]{2,1,0:T(4,128)(2,1)} %refs_7_.3) | copy-start | bytes 24580
  14.3 0.8 %copy-start.9 = (f32[2,8,512]{2,1,0:T(8,128)S(1)}, f32[2,8,512]{2,1,0:T(8,128)}, u32[]{:S(2)}) copy-start(f32[2,8,512]{2,1,0:T(8,128)} %rec_ref.1) | copy-start | bytes 98308
  14.3 19.4 %copy-start.5 = (bf16[2,4,128,128]{3,2,1,0:T(8,128)(2,1)S(1)}, bf16[2,4,128,128]{3,2,1,0:T(8,128)(2,1)}, u32[]{:S(2)}) copy-start(bf16[2,4,128,128]{3,2,1,0:T(8,128)(2,1)} %refs_9_.3) | copy-start | bytes 786436
  14.3 19.4 %copy-start.6 = (bf16[2,4,128,128]{3,2,1,0:T(8,128)(2,1)S(1)}, bf16[2,4,128,128]{3,2,1,0:T(8,128)(2,1)}, u32[]{:S(2)}) copy-start(bf16[2,4,128,128]{3,2,1,0:T(8,128)(2,1)} %refs_10_.3) | copy-start | bytes 786436
  14.3 19.4 %copy-start.10 = (f32[2,512]{1,0:T(2,128)S(1)}, f32[2,512]{1,0:T(2,128)}, u32[]{:S(2)}) copy-start(f32[2,512]{1,0:T(2,128)} %refs_8_.3) | copy-start | bytes 12292
  15.1 19.1 %copy-start = (bf16[2,512,512]{2,1,0:T(8,128)(2,1)S(1)}, bf16[2,512,512]{2,1,0:T(8,128)(2,1)}, u32[]{:S(2)}) copy-start(bf16[2,512,512]{2,1,0:T(8,128)(2,1)} %w_ref.3) | copy-start | bytes 3145732
  15.2 4.0 %collective-permute-start.6 = (bf16[1,2,2,8,512]{4,3,2,1,0:T(8,128)(2,1)S(1)}, bf16[1,2,2,8,512]{4,3,2,1,0:T(8,128)(2,1)S(1)}, u32[]{:S(2)}, u32[]{:S(2)}) collective-permute-start(bf16[1,2,2,8,512]{4,3,2,1,0:T(8,128)(2,1)S(1)} %bitcast.15), channel_id=1, source_target_pairs={{0,2},{1,3},{2,0},{3,1},{4,6},{5,7},{6,4},{7,5},{8,10},{9,11},{10,... | collective-permute-start | bytes 98312 | tf_op jit(solution)/shard_map/ppermute | solution.py:61
  19.2 5.4 %collective-permute-start.7 = (bf16[2,2,2,8,512]{4,3,2,1,0:T(8,128)(2,1)S(1)}, bf16[2,2,2,8,512]{4,3,2,1,0:T(8,128)(2,1)S(1)}, u32[]{:S(2)}, u32[]{:S(2)}) collective-permute-start(bf16[2,2,2,8,512]{4,3,2,1,0:T(8,128)(2,1)S(1)} %shard_map.144.refs_5_), channel_id=1, source_target_pairs={{0,4},{1,5},{2,6},{3,7},{4,0},{5,1},{6,2},{7,3},{8,12},{9,13},{10,... | collective-permute-start | bytes 196616 | tf_op jit(solution)/shard_map/ppermute | solution.py:61
  22.3 5.2 %collective-permute-start.3 = (bf16[264,128]{1,0:T(8,128)(2,1)S(1)}, bf16[264,128]{1,0:T(8,128)(2,1)S(1)}, u32[]{:S(2)}, u32[]{:S(2)}) collective-permute-start(bf16[264,128]{1,0:T(8,128)(2,1)S(1)} %shard_map.141.refs_0_), channel_id=1, source_target_pairs={{0,2},{1,3},{2,0},{3,1},{4,6},{5,7},{6,4},{7,5},{8,10},{9,11},{10,... | collective-permute-start | bytes 202760 | tf_op jit(solution)/shard_map/ppermute | solution.py:61
  24.6 7.3 %collective-permute-start.4 = (bf16[264,128]{1,0:T(8,128)(2,1)S(1)}, bf16[264,128]{1,0:T(8,128)(2,1)S(1)}, u32[]{:S(2)}, u32[]{:S(2)}) collective-permute-start(bf16[264,128]{1,0:T(8,128)(2,1)S(1)} %shard_map.141.refs_0_), channel_id=1, source_target_pairs={{0,4},{1,5},{2,6},{3,7},{4,0},{5,1},{6,2},{7,3},{8,12},{9,13},{10,... | collective-permute-start | bytes 202760 | tf_op jit(solution)/shard_map/ppermute | solution.py:61
  27.5 6.2 %collective-permute-start.5 = (bf16[264,128]{1,0:T(8,128)(2,1)S(1)}, bf16[264,128]{1,0:T(8,128)(2,1)S(1)}, u32[]{:S(2)}, u32[]{:S(2)}) collective-permute-start(bf16[264,128]{1,0:T(8,128)(2,1)S(1)} %shard_map.141.refs_0_), channel_id=1, source_target_pairs={{0,6},{1,7},{2,4},{3,5},{4,2},{5,3},{6,0},{7,1},{8,14},{9,15},{10,... | collective-permute-start | bytes 202760 | tf_op jit(solution)/shard_map/ppermute | solution.py:61
  31.9 5.6 %collective-permute-start.12 = (f32[2,512]{1,0:T(2,128)S(1)}, f32[2,512]{1,0:T(2,128)S(1)}, u32[]{:S(2)}, u32[]{:S(2)}) collective-permute-start(f32[2,512]{1,0:T(2,128)S(1)} %copy-done.12), channel_id=1, source_target_pairs={{0,1},{1,0},{2,3},{3,2},{4,5},{5,4},{6,7},{7,6},{8,9},{9,8},{10,11... | collective-permute-start | bytes 12296 | tf_op jit(solution)/shard_map/ppermute | solution.py:61
  34.2 7.5 %copy-start.2 = (bf16[2,512,512]{2,1,0:T(8,128)(2,1)S(1)}, bf16[2,512,512]{2,1,0:T(8,128)(2,1)}, u32[]{:S(2)}) copy-start(bf16[2,512,512]{2,1,0:T(8,128)(2,1)} %refs_5_.1) | copy-start | bytes 3145732
  34.2 7.5 %copy-start.4 = (bf16[2,512,512]{2,1,0:T(8,128)(2,1)S(1)}, bf16[2,512,512]{2,1,0:T(8,128)(2,1)}, u32[]{:S(2)}) copy-start(bf16[2,512,512]{2,1,0:T(8,128)(2,1)} %refs_6_.1) | copy-start | bytes 3145732
  34.5 4.9 %collective-permute-start.10 = (bf16[32,1024]{1,0:T(8,128)(2,1)S(1)}, bf16[32,1024]{1,0:T(8,128)(2,1)S(1)}, u32[]{:S(2)}, u32[]{:S(2)}) collective-permute-start(bf16[32,1024]{1,0:T(8,128)(2,1)S(1)} %shard_map.146.refs_0_), channel_id=1, source_target_pairs={{0,16},{8,24},{16,0},{24,8},{1,17},{9,25},{17,1},{25,9},{2,18},{10... | collective-permute-start | bytes 196616 | tf_op jit(solution)/shard_map/ppermute | solution.py:61
  36.0 5.2 %collective-permute-start.11 = (bf16[32,1024]{1,0:T(8,128)(2,1)S(1)}, bf16[32,1024]{1,0:T(8,128)(2,1)S(1)}, u32[]{:S(2)}, u32[]{:S(2)}) collective-permute-start(bf16[32,1024]{1,0:T(8,128)(2,1)S(1)} %shard_map.146.refs_0_), channel_id=1, source_target_pairs={{0,24},{8,16},{16,8},{24,0},{1,25},{9,17},{17,9},{25,1},{2,26},{10... | collective-permute-start | bytes 196616 | tf_op jit(solution)/shard_map/ppermute | solution.py:61
  37.5 4.3 %collective-permute-start.9 = (bf16[32,1024]{1,0:T(8,128)(2,1)S(1)}, bf16[32,1024]{1,0:T(8,128)(2,1)S(1)}, u32[]{:S(2)}, u32[]{:S(2)}) collective-permute-start(bf16[32,1024]{1,0:T(8,128)(2,1)S(1)} %shard_map.146.refs_0_), channel_id=1, source_target_pairs={{0,8},{8,0},{16,24},{24,16},{1,9},{9,1},{17,25},{25,17},{2,10},{10... | collective-permute-start | bytes 196616 | tf_op jit(solution)/shard_map/ppermute | solution.py:61
  42.2 4.6 %collective-permute-start.15 = (bf16[264,128]{1,0:T(8,128)(2,1)S(1)}, bf16[264,128]{1,0:T(8,128)(2,1)S(1)}, u32[]{:S(2)}, u32[]{:S(2)}) collective-permute-start(bf16[264,128]{1,0:T(8,128)(2,1)S(1)} %get-tuple-element.26.refs_0_), channel_id=1, source_target_pairs={{0,2},{1,3},{2,0},{3,1},{4,6},{5,7},{6,4},{7,5},{8,10},{9,11},{10,... | collective-permute-start | bytes 202760 | tf_op jit(solution)/shard_map/ppermute | solution.py:61
  43.1 5.9 %collective-permute-start.16 = (bf16[264,128]{1,0:T(8,128)(2,1)S(1)}, bf16[264,128]{1,0:T(8,128)(2,1)S(1)}, u32[]{:S(2)}, u32[]{:S(2)}) collective-permute-start(bf16[264,128]{1,0:T(8,128)(2,1)S(1)} %get-tuple-element.26.refs_0_), channel_id=1, source_target_pairs={{0,4},{1,5},{2,6},{3,7},{4,0},{5,1},{6,2},{7,3},{8,12},{9,13},{10,... | collective-permute-start | bytes 202760 | tf_op jit(solution)/shard_map/ppermute | solution.py:61
  44.3 6.2 %collective-permute-start.17 = (bf16[264,128]{1,0:T(8,128)(2,1)S(1)}, bf16[264,128]{1,0:T(8,128)(2,1)S(1)}, u32[]{:S(2)}, u32[]{:S(2)}) collective-permute-start(bf16[264,128]{1,0:T(8,128)(2,1)S(1)} %get-tuple-element.26.refs_0_), channel_id=1, source_target_pairs={{0,6},{1,7},{2,4},{3,5},{4,2},{5,3},{6,0},{7,1},{8,14},{9,15},{10,... | collective-permute-start | bytes 202760 | tf_op jit(solution)/shard_map/ppermute | solution.py:61
  51.0 1.3 %collective-permute-start.18 = (bf16[40,512]{1,0:T(8,128)(2,1)S(1)}, bf16[40,512]{1,0:T(8,128)(2,1)S(1)}, u32[]{:S(2)}, u32[]{:S(2)}) collective-permute-start(bf16[40,512]{1,0:T(8,128)(2,1)S(1)} %get-tuple-element.28.own_ref), channel_id=1, source_target_pairs={{0,1},{1,0},{2,3},{3,2},{4,5},{5,4},{6,7},{7,6},{8,9},{9,8},{10,11... | collective-permute-start | bytes 122888 | tf_op jit(solution)/shard_map/ppermute | solution.py:61
  52.6 4.2 %collective-permute-start.19 = (bf16[16,512]{1,0:T(8,128)(2,1)S(1)}, bf16[16,512]{1,0:T(8,128)(2,1)S(1)}, u32[]{:S(2)}, u32[]{:S(2)}) collective-permute-start(bf16[16,512]{1,0:T(8,128)(2,1)S(1)} %get-tuple-element.30), channel_id=1, source_target_pairs={{0,8},{8,0},{16,24},{24,16},{1,9},{9,1},{17,25},{25,17},{2,10},{10... | collective-permute-start | bytes 49160 | tf_op jit(solution)/shard_map/ppermute | solution.py:61
  53.6 3.7 %collective-permute-start.20 = (bf16[16,512]{1,0:T(8,128)(2,1)S(1)}, bf16[16,512]{1,0:T(8,128)(2,1)S(1)}, u32[]{:S(2)}, u32[]{:S(2)}) collective-permute-start(bf16[16,512]{1,0:T(8,128)(2,1)S(1)} %get-tuple-element.31), channel_id=1, source_target_pairs={{0,16},{8,24},{16,0},{24,8},{1,17},{9,25},{17,1},{25,9},{2,18},{10... | collective-permute-start | bytes 49160 | tf_op jit(solution)/shard_map/ppermute | solution.py:61
  54.8 4.6 %collective-permute-start.21 = (bf16[16,512]{1,0:T(8,128)(2,1)S(1)}, bf16[16,512]{1,0:T(8,128)(2,1)S(1)}, u32[]{:S(2)}, u32[]{:S(2)}) collective-permute-start(bf16[16,512]{1,0:T(8,128)(2,1)S(1)} %get-tuple-element.32), channel_id=1, source_target_pairs={{0,24},{8,16},{16,8},{24,0},{1,25},{9,17},{17,9},{25,1},{2,26},{10... | collective-permute-start | bytes 49160 | tf_op jit(solution)/shard_map/ppermute | solution.py:61

commit v3 on v2

--- a/solution.py
+++ b/solution.py
@@ -59,6 +59,34 @@
     got = []
     for m in masks:
         got.append(lax.ppermute(value, axis, [(i, i ^ m) for i in range(count)]))
+    return got
+
+
+ORDERS = {
+    "sum0": ((3, 1, 2), (3, 1, 2)),
+    "sum1": ((2, 3, 1), (2, 3, 1)),
+    "out0": ((3, 2, 1), (2, 3, 1)),
+    "last": ((3, 2, 1), (3, 2, 1)),
+}
+
+
+def orders(name, count):
+    if name in ORDERS and len(ORDERS[name][0]) == count - 1:
+        return ORDERS[name]
+    return (tuple(range(1, count)),) * 2
+
+
+def core_exchange(values, axis, name):
+    tp, dp = lax.axis_size("tp"), lax.axis_size("dp")
+    got = []
+    for k, masks in enumerate(zip(*orders(name, tp if axis == "tp" else dp // 2))):
+        pairs = []
+        for t in range(tp):
+            for d in range(dp):
+                m = masks[d % 2]
+                to = (t ^ m, d) if axis == "tp" else (t, d ^ (2 * m))
+                pairs.append((t * dp + d, to[0] * dp + to[1]))
+        got.append(lax.ppermute(values[k % len(values)], ("tp", "dp"), pairs))
     return got
 
 
@@ -202,11 +230,16 @@
     pack(out_ref, both(wi_ref, wi2_ref), both(wg_ref, wg2_ref), square)
 
 
-def one_minus_exp(u):
+def sigmoid(x):
+    return 0.5 * jnp.tanh(0.5 * x) + 0.5
+
+
+def one_minus_square(decay, log_decay):
+    u = 2.0 * log_decay
     series = 1.0 + u * (1.0 / 6.0)
     for k in (5.0, 4.0, 3.0, 2.0):
         series = 1.0 + u * (1.0 / k) * series
-    return jnp.where(u > -0.25, -u * series, 1.0 - jnp.exp(u))
+    return jnp.where(u > -0.25, -u * series, 1.0 - decay * decay)
 
 
 def add_kernel(keep_ref, got_ref, out_ref):
@@ -216,14 +249,22 @@
 def recurrence_kernel(lay, layer, features, *refs):
     zs = lay.dp // 2
     sums, refs = refs[:zs], refs[zs:]
-    own_ref, low_ref, high_ref, taps_ref, decay_ref, wr_ref, wj_ref, *extra, readout_ref, value_ref, rec_ref = refs
+    own_ref, low_ref, high_ref, taps_ref, decay_ref, wr_ref, wj_ref, *extra, out_ref, value_ref, rec_ref = refs
     rows, half, width = lay.rows, lay.half, taps_ref.shape[2]
     states = [own_ref] + [entry((low_ref, high_ref), m) for m in range(1, zs)]
     old = jnp.concatenate([state[layer, 0].astype(F32) for state in states], axis=0)
     previous = jnp.concatenate([state[layer, 1].astype(F32) for state in states], axis=0)
     value_in = gate_in = square = None
-    for mask, part in enumerate(sums):
-        terms = [by_owner(t, mask, zs, rows) for t in unpack(part[...].astype(F32), half, width)]
+    me, z, core = mesh_place()
+    south, north = orders(f"sum{layer}", zs)
+    for mask in range(zs):
+        if mask == 0:
+            part = sums[0][...]
+        elif south.index(mask) == north.index(mask):
+            part = sums[1 + south.index(mask)][...]
+        else:
+            part = jnp.where(core == 0, sums[1 + south.index(mask)][...], sums[1 + north.index(mask)][...])
+        terms = [by_owner(t, mask, zs, rows) for t in unpack(part.astype(F32), half, width)]
         if mask == 0:
             value_in, gate_in, square = terms
         else:
@@ -236,34 +277,35 @@
     conv_low = conv_out.astype(BF16)
     blocks, block = wr_ref.shape[1], wr_ref.shape[2]
 
-    def mapped(ref):
-        return jnp.concatenate(
-            [
-                jnp.dot(conv_low[:, b * block : (b + 1) * block], ref[layer, b], preferred_element_type=F32)
-                for b in range(blocks)
-            ],
-            axis=1,
+    maps = [
+        jnp.dot(
+            conv_low[:, b * block : (b + 1) * block],
+            jnp.concatenate([wr_ref[layer, b], wj_ref[layer, b]], axis=1),
+            preferred_element_type=F32,
         )
-
-    rec_gate = jax.nn.sigmoid(mapped(wr_ref))
-    inp_gate = jax.nn.sigmoid(mapped(wj_ref))
+        for b in range(blocks)
+    ]
+    rec_gate = sigmoid(jnp.concatenate([m[:, :block] for m in maps], axis=1))
+    inp_gate = sigmoid(jnp.concatenate([m[:, block:] for m in maps], axis=1))
     log_decay = -8.0 * rec_gate * jax.nn.softplus(-decay_ref[layer : layer + 1, :])
-    hidden = jnp.exp(log_decay) * previous + jnp.sqrt(one_minus_exp(2.0 * log_decay)) * (inp_gate * conv_out)
-    readout_ref[:half] = (hidden * jax.nn.gelu(gate_in)).astype(BF16)
-    for x_ref in extra:
+    decay = jnp.exp(log_decay)
+    hidden = decay * previous + jnp.sqrt(one_minus_square(decay, log_decay)) * (inp_gate * conv_out)
+    readout = (hidden * jax.nn.gelu(gate_in)).astype(BF16)
+    if len(extra) == 2:
+        for k, w_ref in enumerate(extra):
+            depth = w_ref.shape[2]
+            columns = slice(k * depth, (k + 1) * depth)
+            out_ref[:, columns] = jnp.dot(readout, w_ref[layer], preferred_element_type=F32).astype(BF16)
+    else:
+        (x_ref,) = extra
+        out_ref[:half] = readout
         me, z, _ = mesh_place()
         depth = x_ref.shape[1] // 2
         for i in range(lay.chunks // 2):
             start = lay.side(me * (lay.chunks // 2) + i, z)
-            readout_ref[half + i * rows : half + (i + 1) * rows] = x_ref[pl.ds(start, rows), depth:].astype(BF16)
+            out_ref[half + i * rows : half + (i + 1) * rows] = x_ref[pl.ds(start, rows), depth:].astype(BF16)
     value_ref[...] = value_in[:rows].astype(BF16)
     rec_ref[...] = hidden[:rows]
-
-
-def output_kernel(layer, rows_ref, w_ref, w2_ref, out_ref):
-    width = w_ref.shape[2]
-    out_ref[:, :width] = jnp.dot(rows_ref[...], w_ref[layer], preferred_element_type=F32).astype(BF16)
-    out_ref[:, width:] = jnp.dot(rows_ref[...], w2_ref[layer], preferred_element_type=F32).astype(BF16)
 
 
 def last_output_kernel(lay, layer, own_ref, other_ref, w_ref, x_ref, *refs):
@@ -273,11 +315,13 @@
     held[half:] = jnp.dot(other_ref[:half], w_ref[layer], preferred_element_type=F32)
     me, z, core = mesh_place()
     far = other_ref[half:].astype(F32)
-    for mask, out in enumerate(outs):
+    masks = zip(*orders("last", lay.tp))
+    masks = [0] + [jnp.where(core == 0, a, b) if a != b else a for a, b in masks]
+    for k, (mask, out) in enumerate(zip(masks, outs)):
         for i in range(lay.chunks):
             start = lay.place((me ^ mask) * lay.chunks + i, z, core)
             piece = held[pl.ds(start, rows), :]
-            if mask == 0:
+            if k == 0:
                 near = x_ref[pl.ds(lay.side(me * (lay.chunks // 2) + i // 2, z), rows), :depth]
                 piece = piece + jnp.where(core == i % 2, near, far[i // 2 * rows : (i // 2 + 1) * rows])
             out[i * rows : (i + 1) * rows, :] = piece.astype(out.dtype)
@@ -312,9 +356,6 @@
     half, batch = lay.half, lay.batch
     layers = w_input.shape[0]
 
-    tp_masks = range(1, tp)
-    z_masks = [2 * k for k in range(1, dp // 2)]
-
     tall = packed_rows(half, width)
     bits = lambda n: [1 << k for k in range(n.bit_length() - 1)]
     live = call(length_kernel, shape((lay.rows, LANES), jnp.int32), lengths[None, :], flops=COVER)
@@ -355,11 +396,10 @@
                 *weights,
                 *weights2,
             )
-        sums = [summed] + partner_exchange(summed, "dp", z_masks)
+        sums = [summed] + core_exchange([summed], "z", f"sum{layer}")
         if layer == 0:
             out2, *weights2 = [partner_exchange(w, "dp", [1])[0] for w in (w_output,) + weights]
-        if last:
-            block[0] = shape((half + lay.per_tp // 2, width), BF16)
+        block[0] = shape((half + lay.per_tp // 2, width) if last else (half, 2 * depth), BF16)
         readout, value, hidden = call(
             functools.partial(recurrence_kernel, lay, layer, features),
             block,
@@ -369,17 +409,10 @@
             decay_param,
             w_recur,
             w_inject,
-            *([x] if last else []),
+            *([x] if last else [w_output, out2]),
         )
         if not last:
-            partial = call(
-                functools.partial(output_kernel, layer),
-                shape((half, 2 * depth), BF16),
-                readout,
-                w_output,
-                out2,
-            )
-            parts = [partial] + partner_exchange(partial, "tp", tp_masks)
+            parts = [readout] + core_exchange([readout], "tp", f"out{layer}")
             before = (x, got)
         else:
             (other,) = partner_exchange(readout, "dp", [1])
@@ -392,7 +425,7 @@
                 x,
                 scratch=[pltpu.VMEM((batch, depth), F32)],
             )
-            parts = [own] + [partner_exchange(p, "tp", [m])[0] for p, m in zip(pieces, tp_masks)]
+            parts = [own] + core_exchange(pieces, "tp", "last")
         conv_list.append(jnp.concatenate([conv_state[layer, 1:], value[None]], axis=0))
         rec_list.append(hidden)
     mixed = call(final_kernel, shape((lay.per_tp, depth), BF16), *parts)

time: 60.4 us -> 60.4 us (level)
    ppermute x22 -> x10, starting transfers between devices: 28.5 us -> 11 us  [partner_exchange(): got.append(lax.ppermute(value, axis, [(i, i ^ m) for i in range(count)]))]
    ppermute x0 -> x12, starting transfers between devices: none -> 17.3 us  [core_exchange(): got.append(lax.ppermute(values[k % len(values)], ('tp', 'dp'), pairs))]
    ppermute x0 -> x12, waiting for transfers between devices: none -> 15.2 us  [core_exchange(): got.append(lax.ppermute(values[k % len(values)], ('tp', 'dp'), pairs))]
    ppermute x22 -> x10, waiting for transfers between devices: 22 us -> 7.13 us  [partner_exchange(): got.append(lax.ppermute(value, axis, [(i, i ^ m) for i in range(count)]))]
    pallas_call x12 -> x11, Pallas kernels: 3.08 us -> 3.02 us  [call(): pl.pallas_call(kernel, out_shape=outs, in_specs=[spec] * len(args), out_s...]
  transfers between devices with their start and end apart: 22 -> 22, of which waited for: 15 -> 14; matrix products, arithmetic and copies ran while one was open for 2% -> 2% of each run, Pallas kernels for 2% -> 2%
where the time goes in v3:
time: 60.4 us; the launch traced here: 60.2 us
  starting transfers between devices  28.3 us (47%)
  waiting for transfers between devices  22.3 us (37%)
  local copies, waits for them, and re-layouts  4.48 us (7%)
  Pallas kernels  3.02 us (5%)
  other arithmetic  1.25 us (2%)
  between operations  0.77 us (1%)
    ppermute x12, starting transfers between devices, core_exchange(): got.append(lax.ppermute(values[k % len(values)], ('tp', 'dp'), pairs))  17.3 us
    ppermute x12, waiting for transfers between devices, core_exchange(): got.append(lax.ppermute(values[k % len(values)], ('tp', 'dp'), pairs))  15.2 us
    ppermute x10, starting transfers between devices, partner_exchange(): got.append(lax.ppermute(value, axis, [(i, i ^ m) for i in range(count)]))  11 us
    ppermute x10, waiting for transfers between devices, partner_exchange(): got.append(lax.ppermute(value, axis, [(i, i ^ m) for i in range(count)]))  7.13 us
    unnamed x28, local copies, waits for them, and re-layouts  4.48 us
    pallas_call x11, Pallas kernels, call(): pl.pallas_call(kernel, out_shape=outs, in_specs=[spec] * len(args), out_s...  3.02 us
    another operation x3, other arithmetic, blocks(): return (mixed, jnp.stack(conv_list), jnp.stack(rec_list))  1.25 us
  transfers between devices with their start and end apart: 22, of which 14 were waited for; matrix products, arithmetic and copies ran while one was open for 2% of the time, Pallas kernels for 2%

profile of v3, /device:TPU:0, one launch (start us, length us, event | category | flops | bytes accessed | tf_op | source)
XLA Modules:
  0.0 60.2 jit_solution(15217521408067188658)
XLA Ops:
  0.6 0.6 collective-permute-start.8
  1.2 0.1 collective-permute-start.13
  1.3 0.4 collective-permute-start.14
  1.7 2.6 %collective-permute-start = (bf16[1,16,512]{2,1,0:T(8,128)(2,1)}, bf16[1,16,512]{2,1,0:T(8,128)(2,1)S(1)}, u32[]{:S(2)}, u32[]{:S(2)}) collective-permute-start(bf16[1,16,512]{2,1,0:T(8,128)(2,1)} %bitcast.17), channel_id=1, source_target_pairs={{0,8},{8,0},{16,24},{24,16},{1,9},{9,1},{17,25},{25,17},{2,10},{10... | collective-permute-start | bytes 49160 | tf_op jit(solution)/shard_map/ppermute | solution.py:61
  4.3 1.9 %collective-permute-done.second_ref = bf16[1,16,512]{2,1,0:T(8,128)(2,1)S(1)} collective-permute-done((bf16[1,16,512]{2,1,0:T(8,128)(2,1)}, bf16[1,16,512]{2,1,0:T(8,128)(2,1)S(1)}, u32[]{:S(2)}, u32[]{:S(2)}) %collective-permute-start) | collective-permute-done | bytes 16416 | tf_op jit(solution)/shard_map/ppermute | solution.py:61
  6.2 0.7 %copy-done.11 = bf16[16,512]{1,0:T(8,128)(2,1)S(1)} copy-done((bf16[16,512]{1,0:T(8,128)(2,1)S(1)}, bf16[16,512]{1,0:T(8,128)(2,1)}, u32[]{:S(2)}) %copy-start.11) | copy-done | bytes 16408
  6.9 2.1 %collective-permute-start.1 = (bf16[2,16,512]{2,1,0:T(8,128)(2,1)S(1)}, bf16[2,16,512]{2,1,0:T(8,128)(2,1)S(1)}, u32[]{:S(2)}, u32[]{:S(2)}) collective-permute-start(bf16[2,16,512]{2,1,0:T(8,128)(2,1)S(1)} %shard_map.139.low_ref), channel_id=1, source_target_pairs={{0,16},{8,24},{16,0},{24,8},{1,17},{9,25},{17,1},{25,9},{2,18},{10... | collective-permute-start | bytes 98312 | tf_op jit(solution)/shard_map/ppermute | solution.py:61
  9.0 1.9 %collective-permute-done.1.high_ref = bf16[2,16,512]{2,1,0:T(8,128)(2,1)S(1)} collective-permute-done((bf16[2,16,512]{2,1,0:T(8,128)(2,1)S(1)}, bf16[2,16,512]{2,1,0:T(8,128)(2,1)S(1)}, u32[]{:S(2)}, u32[]{:S(2)}) %collective-permute-start.1) | collective-permute-done | bytes 32800 | tf_op jit(solution)/shard_map/ppermute | solution.py:61
  10.9 1.2 %copy-done.1 = bf16[2,512,512]{2,1,0:T(8,128)(2,1)S(1)} copy-done((bf16[2,512,512]{2,1,0:T(8,128)(2,1)S(1)}, bf16[2,512,512]{2,1,0:T(8,128)(2,1)}, u32[]{:S(2)}) %copy-start.1) | copy-done | bytes 1048600
  12.1 1.2 %copy-done.3 = bf16[2,512,512]{2,1,0:T(8,128)(2,1)S(1)} copy-done((bf16[2,512,512]{2,1,0:T(8,128)(2,1)S(1)}, bf16[2,512,512]{2,1,0:T(8,128)(2,1)}, u32[]{:S(2)}) %copy-start.3) | copy-done | bytes 1048600
  13.3 0.3 shard_map.140
  13.6 0.0 copy-start.13
  13.7 0.1 collective-permute-start.2
  13.7 0.6 copy-done.13
  14.3 0.1 shard_map.142.lengths_ref
  14.4 0.7 %copy-done.7 = bf16[2,3,8,512]{3,2,1,0:T(8,128)(2,1)S(1)} copy-done((bf16[2,3,8,512]{3,2,1,0:T(8,128)(2,1)S(1)}, bf16[2,3,8,512]{3,2,1,0:T(8,128)(2,1)}, u32[]{:S(2)}) %copy-start.7) | copy-done | bytes 49176
  15.1 0.0 copy-done.9
  15.1 0.1 shard_map.143
  15.2 2.1 %collective-permute-start.6 = (bf16[1,2,2,8,512]{4,3,2,1,0:T(8,128)(2,1)S(1)}, bf16[1,2,2,8,512]{4,3,2,1,0:T(8,128)(2,1)S(1)}, u32[]{:S(2)}, u32[]{:S(2)}) collective-permute-start(bf16[1,2,2,8,512]{4,3,2,1,0:T(8,128)(2,1)S(1)} %bitcast.15), channel_id=1, source_target_pairs={{0,2},{1,3},{2,0},{3,1},{4,6},{5,7},{6,4},{7,5},{8,10},{9,11},{10,... | collective-permute-start | bytes 98312 | tf_op jit(solution)/shard_map/ppermute | solution.py:61
  17.4 1.9 %collective-permute-done.6.second_ref = bf16[1,2,2,8,512]{4,3,2,1,0:T(8,128)(2,1)S(1)} collective-permute-done((bf16[1,2,2,8,512]{4,3,2,1,0:T(8,128)(2,1)S(1)}, bf16[1,2,2,8,512]{4,3,2,1,0:T(8,128)(2,1)S(1)}, u32[]{:S(2)}, u32[]{:S(2)}) %collective-permute-start.6) | collective-permute-done | bytes 32800 | tf_op jit(solution)/shard_map/ppermute | solution.py:61
  19.3 3.0 %collective-permute-start.7 = (bf16[2,2,2,8,512]{4,3,2,1,0:T(8,128)(2,1)S(1)}, bf16[2,2,2,8,512]{4,3,2,1,0:T(8,128)(2,1)S(1)}, u32[]{:S(2)}, u32[]{:S(2)}) collective-permute-start(bf16[2,2,2,8,512]{4,3,2,1,0:T(8,128)(2,1)S(1)} %shard_map.144.refs_5_), channel_id=1, source_target_pairs={{0,4},{1,5},{2,6},{3,7},{4,0},{5,1},{6,2},{7,3},{8,12},{9,13},{10,... | collective-permute-start | bytes 196616 | tf_op jit(solution)/shard_map/ppermute | solution.py:61
  22.3 0.0 collective-permute-done.2.got_ref
  22.3 1.4 %collective-permute-start.3 = (bf16[264,128]{1,0:T(8,128)(2,1)S(1)}, bf16[264,128]{1,0:T(8,128)(2,1)S(1)}, u32[]{:S(2)}, u32[]{:S(2)}) collective-permute-start(bf16[264,128]{1,0:T(8,128)(2,1)S(1)} %shard_map.141.refs_0_), channel_id=1, source_target_pairs={{0,6},{1,7},{2,4},{3,5},{4,2},{5,3},{6,0},{7,1},{8,14},{9,15},{10,... | collective-permute-start | bytes 202760 | tf_op jit(solution)/shard_map/ppermute | solution.py:89
  23.7 0.8 %collective-permute-done.7.refs_6_ = bf16[2,2,2,8,512]{4,3,2,1,0:T(8,128)(2,1)S(1)} collective-permute-done((bf16[2,2,2,8,512]{4,3,2,1,0:T(8,128)(2,1)S(1)}, bf16[2,2,2,8,512]{4,3,2,1,0:T(8,128)(2,1)S(1)}, u32[]{:S(2)}, u32[]{:S(2)}) %collective-permute-start.7) | collective-permute-done | bytes 65568 | tf_op jit(solution)/shard_map/ppermute | solution.py:61
  24.6 3.0 %collective-permute-start.4 = (bf16[264,128]{1,0:T(8,128)(2,1)S(1)}, bf16[264,128]{1,0:T(8,128)(2,1)S(1)}, u32[]{:S(2)}, u32[]{:S(2)}) collective-permute-start(bf16[264,128]{1,0:T(8,128)(2,1)S(1)} %shard_map.141.refs_0_), channel_id=1, source_target_pairs={{0,2},{1,3},{2,0},{3,1},{4,6},{5,7},{6,4},{7,5},{8,10},{9,11},{10,... | collective-permute-start | bytes 202760 | tf_op jit(solution)/shard_map/ppermute | solution.py:89
  27.6 1.1 %collective-permute-done.3.refs_1_ = bf16[264,128]{1,0:T(8,128)(2,1)S(1)} collective-permute-done((bf16[264,128]{1,0:T(8,128)(2,1)S(1)}, bf16[264,128]{1,0:T(8,128)(2,1)S(1)}, u32[]{:S(2)}, u32[]{:S(2)}) %collective-permute-start.3) | collective-permute-done | bytes 67616 | tf_op jit(solution)/shard_map/ppermute | solution.py:89
  28.7 2.3 %collective-permute-start.5 = (bf16[264,128]{1,0:T(8,128)(2,1)S(1)}, bf16[264,128]{1,0:T(8,128)(2,1)S(1)}, u32[]{:S(2)}, u32[]{:S(2)}) collective-permute-start(bf16[264,128]{1,0:T(8,128)(2,1)S(1)} %shard_map.141.refs_0_), channel_id=1, source_target_pairs={{0,4},{1,5},{2,6},{3,7},{4,0},{5,1},{6,2},{7,3},{8,12},{9,13},{10,... | collective-permute-start | bytes 202760 | tf_op jit(solution)/shard_map/ppermute | solution.py:89
  31.0 0.0 collective-permute-done.4.refs_2_
  31.0 0.0 collective-permute-start.12
  31.0 3.1 %collective-permute-done.5.refs_3_ = bf16[264,128]{1,0:T(8,128)(2,1)S(1)} collective-permute-done((bf16[264,128]{1,0:T(8,128)(2,1)S(1)}, bf16[264,128]{1,0:T(8,128)(2,1)S(1)}, u32[]{:S(2)}, u32[]{:S(2)}) %collective-permute-start.5) | collective-permute-done | bytes 67616 | tf_op jit(solution)/shard_map/ppermute | solution.py:89
  34.2 0.0 collective-permute-done.8.refs_12_
  34.2 0.0 copy-done.5
  34.2 0.0 copy-start.2
  34.2 0.0 copy-start.4
  34.2 0.7 %shard_map.145 = (bf16[32,1024]{1,0:T(8,128)(2,1)S(1)}, bf16[8,512]{1,0:T(8,128)(2,1)S(1)}, f32[8,512]{1,0:T(8,128)S(1)}) custom-call(bf16[264,128]{1,0:T(8,128)(2,1)S(1)} %shard_map.141.refs_0_, bf16[264,128]{1,0:T(8,128)(2,1)S(1)} %collective-permute-done.3.refs_1_, bf16[264,128]{1,0:T(8,128)(2,1)S(1)} %collective-permute-done.4.refs_2_, ...), custom_call_target="tpu_custom_call" | custom-call | flops 1000000 | bytes 1048576 | tf_op jit(solution)/shard_map/pallas_call | solution.py:21
  34.9 1.6 %collective-permute-start.10 = (bf16[32,1024]{1,0:T(8,128)(2,1)S(1)}, bf16[32,1024]{1,0:T(8,128)(2,1)S(1)}, u32[]{:S(2)}, u32[]{:S(2)}) collective-permute-start(bf16[32,1024]{1,0:T(8,128)(2,1)S(1)} %get-tuple-element.25.refs_0_), channel_id=1, source_target_pairs={{0,16},{1,25},{2,18},{3,27},{4,20},{5,29},{6,22},{7,31},{8,24},{9,... | collective-permute-start | bytes 196616 | tf_op jit(solution)/shard_map/ppermute | solution.py:89
  36.4 1.5 %collective-permute-start.11 = (bf16[32,1024]{1,0:T(8,128)(2,1)S(1)}, bf16[32,1024]{1,0:T(8,128)(2,1)S(1)}, u32[]{:S(2)}, u32[]{:S(2)}) collective-permute-start(bf16[32,1024]{1,0:T(8,128)(2,1)S(1)} %get-tuple-element.25.refs_0_), channel_id=1, source_target_pairs={{0,8},{1,9},{2,10},{3,11},{4,12},{5,13},{6,14},{7,15},{8,0},{9,1},... | collective-permute-start | bytes 196616 | tf_op jit(solution)/shard_map/ppermute | solution.py:89
  37.9 0.0 collective-permute-done.12.refs_7_
  37.9 0.5 collective-permute-start.9
  38.4 0.0 collective-permute-done.13.refs_8_
  38.4 0.0 collective-permute-done.14.refs_9_
  38.4 0.8 %collective-permute-done.10.refs_2_ = bf16[32,1024]{1,0:T(8,128)(2,1)S(1)} collective-permute-done((bf16[32,1024]{1,0:T(8,128)(2,1)S(1)}, bf16[32,1024]{1,0:T(8,128)(2,1)S(1)}, u32[]{:S(2)}, u32[]{:S(2)}) %collective-permute-start.10) | collective-permute-done | bytes 65568 | tf_op jit(solution)/shard_map/ppermute | solution.py:89
  39.2 1.5 %collective-permute-done.11.refs_3_ = bf16[32,1024]{1,0:T(8,128)(2,1)S(1)} collective-permute-done((bf16[32,1024]{1,0:T(8,128)(2,1)S(1)}, bf16[32,1024]{1,0:T(8,128)(2,1)S(1)}, u32[]{:S(2)}, u32[]{:S(2)}) %collective-permute-start.11) | collective-permute-done | bytes 65568 | tf_op jit(solution)/shard_map/ppermute | solution.py:89
  40.7 2.4 %collective-permute-done.9.refs_1_ = bf16[32,1024]{1,0:T(8,128)(2,1)S(1)} collective-permute-done((bf16[32,1024]{1,0:T(8,128)(2,1)S(1)}, bf16[32,1024]{1,0:T(8,128)(2,1)S(1)}, u32[]{:S(2)}, u32[]{:S(2)}) %collective-permute-start.9) | collective-permute-done | bytes 65568 | tf_op jit(solution)/shard_map/ppermute | solution.py:89
  43.1 0.4 shard_map.146
  43.5 2.1 %collective-permute-start.15 = (bf16[264,128]{1,0:T(8,128)(2,1)S(1)}, bf16[264,128]{1,0:T(8,128)(2,1)S(1)}, u32[]{:S(2)}, u32[]{:S(2)}) collective-permute-start(bf16[264,128]{1,0:T(8,128)(2,1)S(1)} %get-tuple-element.26.refs_0_), channel_id=1, source_target_pairs={{0,4},{1,5},{2,6},{3,7},{4,0},{5,1},{6,2},{7,3},{8,12},{9,13},{10,... | collective-permute-start | bytes 202760 | tf_op jit(solution)/shard_map/ppermute | solution.py:89
  45.6 0.2 collective-permute-start.16
  45.8 1.3 %collective-permute-start.17 = (bf16[264,128]{1,0:T(8,128)(2,1)S(1)}, bf16[264,128]{1,0:T(8,128)(2,1)S(1)}, u32[]{:S(2)}, u32[]{:S(2)}) collective-permute-start(bf16[264,128]{1,0:T(8,128)(2,1)S(1)} %get-tuple-element.26.refs_0_), channel_id=1, source_target_pairs={{0,2},{1,3},{2,0},{3,1},{4,6},{5,7},{6,4},{7,5},{8,10},{9,11},{10,... | collective-permute-start | bytes 202760 | tf_op jit(solution)/shard_map/ppermute | solution.py:89
  47.1 1.7 %collective-permute-done.15.refs_1_ = bf16[264,128]{1,0:T(8,128)(2,1)S(1)} collective-permute-done((bf16[264,128]{1,0:T(8,128)(2,1)S(1)}, bf16[264,128]{1,0:T(8,128)(2,1)S(1)}, u32[]{:S(2)}, u32[]{:S(2)}) %collective-permute-start.15) | collective-permute-done | bytes 67616 | tf_op jit(solution)/shard_map/ppermute | solution.py:89
  48.8 2.9 %collective-permute-done.16.refs_2_ = bf16[264,128]{1,0:T(8,128)(2,1)S(1)} collective-permute-done((bf16[264,128]{1,0:T(8,128)(2,1)S(1)}, bf16[264,128]{1,0:T(8,128)(2,1)S(1)}, u32[]{:S(2)}, u32[]{:S(2)}) %collective-permute-start.16) | collective-permute-done | bytes 67616 | tf_op jit(solution)/shard_map/ppermute | solution.py:89
  51.7 0.0 collective-permute-done.17.refs_3_
  51.7 0.5 shard_map.147
  52.2 0.1 collective-permute-start.18
  52.3 0.6 %pad_maximum_fusion = bf16[2,3,8,512]{3,2,1,0:T(8,128)(2,1)} fusion(bf16[1,3,8,512]{3,2,1,0:T(8,128)(2,1)S(1)} %get-tuple-element.40, bf16[1,3,8,512]{3,2,1,0:T(8,128)(2,1)S(1)} %get-tuple-element.39), kind=kLoop, calls=%fused_computation | loop fusion | flops 24576 | bytes 98304 | tf_op jit(solution)/shard_map/stack | solution.py:432
  52.9 0.6 collective-permute-done.18.other_ref
  53.5 0.3 shard_map.148
  53.7 0.8 %collective-permute-start.19 = (bf16[16,512]{1,0:T(8,128)(2,1)S(1)}, bf16[16,512]{1,0:T(8,128)(2,1)S(1)}, u32[]{:S(2)}, u32[]{:S(2)}) collective-permute-start(bf16[16,512]{1,0:T(8,128)(2,1)S(1)} %get-tuple-element.30), channel_id=1, source_target_pairs={{0,24},{1,25},{2,26},{3,27},{4,28},{5,29},{6,30},{7,31},{8,16},{9,... | collective-permute-start | bytes 49160 | tf_op jit(solution)/shard_map/ppermute | solution.py:89
  54.5 1.3 %collective-permute-start.20 = (bf16[16,512]{1,0:T(8,128)(2,1)S(1)}, bf16[16,512]{1,0:T(8,128)(2,1)S(1)}, u32[]{:S(2)}, u32[]{:S(2)}) collective-permute-start(bf16[16,512]{1,0:T(8,128)(2,1)S(1)} %get-tuple-element.31), channel_id=1, source_target_pairs={{0,16},{1,17},{2,18},{3,19},{4,20},{5,21},{6,22},{7,23},{8,24},{9,... | collective-permute-start | bytes 49160 | tf_op jit(solution)/shard_map/ppermute | solution.py:89
  55.8 1.5 %collective-permute-start.21 = (bf16[16,512]{1,0:T(8,128)(2,1)S(1)}, bf16[16,512]{1,0:T(8,128)(2,1)S(1)}, u32[]{:S(2)}, u32[]{:S(2)}) collective-permute-start(bf16[16,512]{1,0:T(8,128)(2,1)S(1)} %get-tuple-element.32), channel_id=1, source_target_pairs={{0,8},{1,9},{2,10},{3,11},{4,12},{5,13},{6,14},{7,15},{8,0},{9,1},... | collective-permute-start | bytes 49160 | tf_op jit(solution)/shard_map/ppermute | solution.py:89
  57.3 0.6 %pad_maximum_fusion.1 = f32[2,8,512]{2,1,0:T(8,128)} fusion(f32[1,8,512]{2,1,0:T(8,128)S(1)} %bitcast.20, f32[1,8,512]{2,1,0:T(8,128)S(1)} %bitcast.19), kind=kLoop, calls=%fused_computation.1 | loop fusion | flops 8192 | bytes 65536 | tf_op jit(solution)/shard_map/stack | solution.py:432
  57.9 0.6 collective-permute-done.19.refs_0_
  58.5 0.0 collective-permute-done.20.refs_1_
  58.5 1.0 %collective-permute-done.21.refs_2_ = bf16[16,512]{1,0:T(8,128)(2,1)S(1)} collective-permute-done((bf16[16,512]{1,0:T(8,128)(2,1)S(1)}, bf16[16,512]{1,0:T(8,128)(2,1)S(1)}, u32[]{:S(2)}, u32[]{:S(2)}) %collective-permute-start.21) | collective-permute-done | bytes 16416 | tf_op jit(solution)/shard_map/ppermute | solution.py:89
  59.6 0.6 %shard_map.149 = bf16[16,512]{1,0:T(8,128)(2,1)} custom-call(f32[16,512]{1,0:T(8,128)S(1)} %get-tuple-element.29.own_ref, bf16[16,512]{1,0:T(8,128)(2,1)S(1)} %collective-permute-done.19.refs_0_, bf16[16,512]{1,0:T(8,128)(2,1)S(1)} %collective-permute-done.20.refs_1_, bf16[16,512]{1,0:T(8,128)(2,1)S(1)} %collective-permute-done.21.refs_2_), custom_call_target="tpu_custom_call" | custom-call | flops 1000000 | bytes 1048576 | tf_op jit(solution)/shard_map/pallas_call | solution.py:21
  (23 shorter events, 0.1 us)
Async XLA Ops:
  0.6 33.5 %collective-permute-start.8 = (bf16[2,512,512]{2,1,0:T(8,128)(2,1)}, bf16[2,512,512]{2,1,0:T(8,128)(2,1)S(1)}, u32[]{:S(2)}, u32[]{:S(2)}) collective-permute-start(bf16[2,512,512]{2,1,0:T(8,128)(2,1)} %w_ref.1), channel_id=1, source_target_pairs={{0,1},{1,0},{2,3},{3,2},{4,5},{5,4},{6,7},{7,6},{8,9},{9,8},{10,11... | collective-permute-start | bytes 3145736 | tf_op jit(solution)/shard_map/ppermute | solution.py:61
  1.2 37.2 %collective-permute-start.13 = (bf16[2,512,512]{2,1,0:T(8,128)(2,1)}, bf16[2,512,512]{2,1,0:T(8,128)(2,1)S(1)}, u32[]{:S(2)}, u32[]{:S(2)}) collective-permute-start(bf16[2,512,512]{2,1,0:T(8,128)(2,1)} %refs_5_.1), channel_id=1, source_target_pairs={{0,1},{1,0},{2,3},{3,2},{4,5},{5,4},{6,7},{7,6},{8,9},{9,8},{10,11... | collective-permute-start | bytes 3145736 | tf_op jit(solution)/shard_map/ppermute | solution.py:61
  1.3 37.2 %collective-permute-start.14 = (bf16[2,512,512]{2,1,0:T(8,128)(2,1)}, bf16[2,512,512]{2,1,0:T(8,128)(2,1)S(1)}, u32[]{:S(2)}, u32[]{:S(2)}) collective-permute-start(bf16[2,512,512]{2,1,0:T(8,128)(2,1)} %refs_6_.1), channel_id=1, source_target_pairs={{0,1},{1,0},{2,3},{3,2},{4,5},{5,4},{6,7},{7,6},{8,9},{9,8},{10,11... | collective-permute-start | bytes 3145736 | tf_op jit(solution)/shard_map/ppermute | solution.py:61
  1.7 4.5 %collective-permute-start = (bf16[1,16,512]{2,1,0:T(8,128)(2,1)}, bf16[1,16,512]{2,1,0:T(8,128)(2,1)S(1)}, u32[]{:S(2)}, u32[]{:S(2)}) collective-permute-start(bf16[1,16,512]{2,1,0:T(8,128)(2,1)} %bitcast.17), channel_id=1, source_target_pairs={{0,8},{8,0},{16,24},{24,16},{1,9},{9,1},{17,25},{25,17},{2,10},{10... | collective-permute-start | bytes 49160 | tf_op jit(solution)/shard_map/ppermute | solution.py:61
  6.2 0.7 %copy-start.11 = (bf16[16,512]{1,0:T(8,128)(2,1)S(1)}, bf16[16,512]{1,0:T(8,128)(2,1)}, u32[]{:S(2)}) copy-start(bf16[16,512]{1,0:T(8,128)(2,1)} %param.12) | copy-start | bytes 49156
  6.9 4.0 %copy-start.12 = (f32[2,512]{1,0:T(2,128)S(1)}, f32[2,512]{1,0:T(2,128)}, u32[]{:S(2)}) copy-start(f32[2,512]{1,0:T(2,128)} %refs_4_.1) | copy-start | bytes 12292
  6.9 3.9 %collective-permute-start.1 = (bf16[2,16,512]{2,1,0:T(8,128)(2,1)S(1)}, bf16[2,16,512]{2,1,0:T(8,128)(2,1)S(1)}, u32[]{:S(2)}, u32[]{:S(2)}) collective-permute-start(bf16[2,16,512]{2,1,0:T(8,128)(2,1)S(1)} %shard_map.139.low_ref), channel_id=1, source_target_pairs={{0,16},{8,24},{16,0},{24,8},{1,17},{9,25},{17,1},{25,9},{2,18},{10... | collective-permute-start | bytes 98312 | tf_op jit(solution)/shard_map/ppermute | solution.py:61
  10.9 1.2 %copy-start.1 = (bf16[2,512,512]{2,1,0:T(8,128)(2,1)S(1)}, bf16[2,512,512]{2,1,0:T(8,128)(2,1)}, u32[]{:S(2)}) copy-start(bf16[2,512,512]{2,1,0:T(8,128)(2,1)} %refs_5_.1) | copy-start | bytes 3145732
  12.1 1.2 %copy-start.3 = (bf16[2,512,512]{2,1,0:T(8,128)(2,1)S(1)}, bf16[2,512,512]{2,1,0:T(8,128)(2,1)}, u32[]{:S(2)}) copy-start(bf16[2,512,512]{2,1,0:T(8,128)(2,1)} %refs_6_.1) | copy-start | bytes 3145732
  13.6 0.7 %copy-start.13 = (s32[8]{0:T(128)S(1)}, s32[8]{0:T(128)}, u32[]{:S(2)}) copy-start(s32[8]{0:T(128)} %param.21) | copy-start | bytes 100
  13.7 8.6 %collective-permute-start.2 = (bf16[392,128]{1,0:T(8,128)(2,1)S(1)}, bf16[392,128]{1,0:T(8,128)(2,1)S(1)}, u32[]{:S(2)}, u32[]{:S(2)}) collective-permute-start(bf16[392,128]{1,0:T(8,128)(2,1)S(1)} %get-tuple-element.21), channel_id=1, source_target_pairs={{0,1},{1,0},{2,3},{3,2},{4,5},{5,4},{6,7},{7,6},{8,9},{9,8},{10,11... | collective-permute-start | bytes 301064 | tf_op jit(solution)/shard_map/ppermute | solution.py:61
  14.3 0.8 %copy-start.7 = (bf16[2,3,8,512]{3,2,1,0:T(8,128)(2,1)S(1)}, bf16[2,3,8,512]{3,2,1,0:T(8,128)(2,1)}, u32[]{:S(2)}) copy-start(bf16[2,3,8,512]{3,2,1,0:T(8,128)(2,1)} %conv_ref.1) | copy-start | bytes 147460
  14.3 0.8 %copy-start.8 = (bf16[2,4,512]{2,1,0:T(4,128)(2,1)S(1)}, bf16[2,4,512]{2,1,0:T(4,128)(2,1)}, u32[]{:S(2)}) copy-start(bf16[2,4,512]{2,1,0:T(4,128)(2,1)} %refs_7_.3) | copy-start | bytes 24580
  14.3 0.8 %copy-start.9 = (f32[2,8,512]{2,1,0:T(8,128)S(1)}, f32[2,8,512]{2,1,0:T(8,128)}, u32[]{:S(2)}) copy-start(f32[2,8,512]{2,1,0:T(8,128)} %rec_ref.1) | copy-start | bytes 98308
  14.3 19.9 %copy-start = (bf16[2,512,512]{2,1,0:T(8,128)(2,1)S(1)}, bf16[2,512,512]{2,1,0:T(8,128)(2,1)}, u32[]{:S(2)}) copy-start(bf16[2,512,512]{2,1,0:T(8,128)(2,1)} %w_ref.1) | copy-start | bytes 3145732
  15.1 19.1 %copy-start.5 = (bf16[2,4,128,128]{3,2,1,0:T(8,128)(2,1)S(1)}, bf16[2,4,128,128]{3,2,1,0:T(8,128)(2,1)}, u32[]{:S(2)}) copy-start(bf16[2,4,128,128]{3,2,1,0:T(8,128)(2,1)} %refs_9_.3) | copy-start | bytes 786436
  15.1 19.1 %copy-start.6 = (bf16[2,4,128,128]{3,2,1,0:T(8,128)(2,1)S(1)}, bf16[2,4,128,128]{3,2,1,0:T(8,128)(2,1)}, u32[]{:S(2)}) copy-start(bf16[2,4,128,128]{3,2,1,0:T(8,128)(2,1)} %refs_10_.3) | copy-start | bytes 786436
  15.2 4.0 %collective-permute-start.6 = (bf16[1,2,2,8,512]{4,3,2,1,0:T(8,128)(2,1)S(1)}, bf16[1,2,2,8,512]{4,3,2,1,0:T(8,128)(2,1)S(1)}, u32[]{:S(2)}, u32[]{:S(2)}) collective-permute-start(bf16[1,2,2,8,512]{4,3,2,1,0:T(8,128)(2,1)S(1)} %bitcast.15), channel_id=1, source_target_pairs={{0,2},{1,3},{2,0},{3,1},{4,6},{5,7},{6,4},{7,5},{8,10},{9,11},{10,... | collective-permute-start | bytes 98312 | tf_op jit(solution)/shard_map/ppermute | solution.py:61
  19.3 5.3 %collective-permute-start.7 = (bf16[2,2,2,8,512]{4,3,2,1,0:T(8,128)(2,1)S(1)}, bf16[2,2,2,8,512]{4,3,2,1,0:T(8,128)(2,1)S(1)}, u32[]{:S(2)}, u32[]{:S(2)}) collective-permute-start(bf16[2,2,2,8,512]{4,3,2,1,0:T(8,128)(2,1)S(1)} %shard_map.144.refs_5_), channel_id=1, source_target_pairs={{0,4},{1,5},{2,6},{3,7},{4,0},{5,1},{6,2},{7,3},{8,12},{9,13},{10,... | collective-permute-start | bytes 196616 | tf_op jit(solution)/shard_map/ppermute | solution.py:61
  22.3 11.9 %copy-start.10 = (f32[2,512]{1,0:T(2,128)S(1)}, f32[2,512]{1,0:T(2,128)}, u32[]{:S(2)}) copy-start(f32[2,512]{1,0:T(2,128)} %refs_8_.3) | copy-start | bytes 12292
  22.3 6.4 %collective-permute-start.3 = (bf16[264,128]{1,0:T(8,128)(2,1)S(1)}, bf16[264,128]{1,0:T(8,128)(2,1)S(1)}, u32[]{:S(2)}, u32[]{:S(2)}) collective-permute-start(bf16[264,128]{1,0:T(8,128)(2,1)S(1)} %shard_map.141.refs_0_), channel_id=1, source_target_pairs={{0,6},{1,7},{2,4},{3,5},{4,2},{5,3},{6,0},{7,1},{8,14},{9,15},{10,... | collective-permute-start | bytes 202760 | tf_op jit(solution)/shard_map/ppermute | solution.py:89
  24.6 6.4 %collective-permute-start.4 = (bf16[264,128]{1,0:T(8,128)(2,1)S(1)}, bf16[264,128]{1,0:T(8,128)(2,1)S(1)}, u32[]{:S(2)}, u32[]{:S(2)}) collective-permute-start(bf16[264,128]{1,0:T(8,128)(2,1)S(1)} %shard_map.141.refs_0_), channel_id=1, source_target_pairs={{0,2},{1,3},{2,0},{3,1},{4,6},{5,7},{6,4},{7,5},{8,10},{9,11},{10,... | collective-permute-start | bytes 202760 | tf_op jit(solution)/shard_map/ppermute | solution.py:89
  28.7 5.5 %collective-permute-start.5 = (bf16[264,128]{1,0:T(8,128)(2,1)S(1)}, bf16[264,128]{1,0:T(8,128)(2,1)S(1)}, u32[]{:S(2)}, u32[]{:S(2)}) collective-permute-start(bf16[264,128]{1,0:T(8,128)(2,1)S(1)} %shard_map.141.refs_0_), channel_id=1, source_target_pairs={{0,4},{1,5},{2,6},{3,7},{4,0},{5,1},{6,2},{7,3},{8,12},{9,13},{10,... | collective-permute-start | bytes 202760 | tf_op jit(solution)/shard_map/ppermute | solution.py:89
  31.0 6.9 %collective-permute-start.12 = (f32[2,512]{1,0:T(2,128)S(1)}, f32[2,512]{1,0:T(2,128)S(1)}, u32[]{:S(2)}, u32[]{:S(2)}) collective-permute-start(f32[2,512]{1,0:T(2,128)S(1)} %copy-done.12), channel_id=1, source_target_pairs={{0,1},{1,0},{2,3},{3,2},{4,5},{5,4},{6,7},{7,6},{8,9},{9,8},{10,11... | collective-permute-start | bytes 12296 | tf_op jit(solution)/shard_map/ppermute | solution.py:61
  34.2 8.9 %copy-start.2 = (bf16[2,512,512]{2,1,0:T(8,128)(2,1)S(1)}, bf16[2,512,512]{2,1,0:T(8,128)(2,1)}, u32[]{:S(2)}) copy-start(bf16[2,512,512]{2,1,0:T(8,128)(2,1)} %refs_5_.1) | copy-start | bytes 3145732
  34.2 8.9 %copy-start.4 = (bf16[2,512,512]{2,1,0:T(8,128)(2,1)S(1)}, bf16[2,512,512]{2,1,0:T(8,128)(2,1)}, u32[]{:S(2)}) copy-start(bf16[2,512,512]{2,1,0:T(8,128)(2,1)} %refs_6_.1) | copy-start | bytes 3145732
  34.9 4.3 %collective-permute-start.10 = (bf16[32,1024]{1,0:T(8,128)(2,1)S(1)}, bf16[32,1024]{1,0:T(8,128)(2,1)S(1)}, u32[]{:S(2)}, u32[]{:S(2)}) collective-permute-start(bf16[32,1024]{1,0:T(8,128)(2,1)S(1)} %get-tuple-element.25.refs_0_), channel_id=1, source_target_pairs={{0,16},{1,25},{2,18},{3,27},{4,20},{5,29},{6,22},{7,31},{8,24},{9,... | collective-permute-start | bytes 196616 | tf_op jit(solution)/shard_map/ppermute | solution.py:89
  36.4 4.3 %collective-permute-start.11 = (bf16[32,1024]{1,0:T(8,128)(2,1)S(1)}, bf16[32,1024]{1,0:T(8,128)(2,1)S(1)}, u32[]{:S(2)}, u32[]{:S(2)}) collective-permute-start(bf16[32,1024]{1,0:T(8,128)(2,1)S(1)} %get-tuple-element.25.refs_0_), channel_id=1, source_target_pairs={{0,8},{1,9},{2,10},{3,11},{4,12},{5,13},{6,14},{7,15},{8,0},{9,1},... | collective-permute-start | bytes 196616 | tf_op jit(solution)/shard_map/ppermute | solution.py:89
  37.9 5.2 %collective-permute-start.9 = (bf16[32,1024]{1,0:T(8,128)(2,1)S(1)}, bf16[32,1024]{1,0:T(8,128)(2,1)S(1)}, u32[]{:S(2)}, u32[]{:S(2)}) collective-permute-start(bf16[32,1024]{1,0:T(8,128)(2,1)S(1)} %get-tuple-element.25.refs_0_), channel_id=1, source_target_pairs={{0,24},{1,17},{2,26},{3,19},{4,28},{5,21},{6,30},{7,23},{8,16},{9,... | collective-permute-start | bytes 196616 | tf_op jit(solution)/shard_map/ppermute | solution.py:89
  43.5 5.2 %collective-permute-start.15 = (bf16[264,128]{1,0:T(8,128)(2,1)S(1)}, bf16[264,128]{1,0:T(8,128)(2,1)S(1)}, u32[]{:S(2)}, u32[]{:S(2)}) collective-permute-start(bf16[264,128]{1,0:T(8,128)(2,1)S(1)} %get-tuple-element.26.refs_0_), channel_id=1, source_target_pairs={{0,4},{1,5},{2,6},{3,7},{4,0},{5,1},{6,2},{7,3},{8,12},{9,13},{10,... | collective-permute-start | bytes 202760 | tf_op jit(solution)/shard_map/ppermute | solution.py:89
  45.6 6.1 %collective-permute-start.16 = (bf16[264,128]{1,0:T(8,128)(2,1)S(1)}, bf16[264,128]{1,0:T(8,128)(2,1)S(1)}, u32[]{:S(2)}, u32[]{:S(2)}) collective-permute-start(bf16[264,128]{1,0:T(8,128)(2,1)S(1)} %get-tuple-element.26.refs_0_), channel_id=1, source_target_pairs={{0,6},{1,7},{2,4},{3,5},{4,2},{5,3},{6,0},{7,1},{8,14},{9,15},{10,... | collective-permute-start | bytes 202760 | tf_op jit(solution)/shard_map/ppermute | solution.py:89
  45.8 5.9 %collective-permute-start.17 = (bf16[264,128]{1,0:T(8,128)(2,1)S(1)}, bf16[264,128]{1,0:T(8,128)(2,1)S(1)}, u32[]{:S(2)}, u32[]{:S(2)}) collective-permute-start(bf16[264,128]{1,0:T(8,128)(2,1)S(1)} %get-tuple-element.26.refs_0_), channel_id=1, source_target_pairs={{0,2},{1,3},{2,0},{3,1},{4,6},{5,7},{6,4},{7,5},{8,10},{9,11},{10,... | collective-permute-start | bytes 202760 | tf_op jit(solution)/shard_map/ppermute | solution.py:89
  52.2 1.3 %collective-permute-start.18 = (bf16[40,512]{1,0:T(8,128)(2,1)S(1)}, bf16[40,512]{1,0:T(8,128)(2,1)S(1)}, u32[]{:S(2)}, u32[]{:S(2)}) collective-permute-start(bf16[40,512]{1,0:T(8,128)(2,1)S(1)} %get-tuple-element.28.own_ref), channel_id=1, source_target_pairs={{0,1},{1,0},{2,3},{3,2},{4,5},{5,4},{6,7},{7,6},{8,9},{9,8},{10,11... | collective-permute-start | bytes 122888 | tf_op jit(solution)/shard_map/ppermute | solution.py:61
  53.7 4.8 %collective-permute-start.19 = (bf16[16,512]{1,0:T(8,128)(2,1)S(1)}, bf16[16,512]{1,0:T(8,128)(2,1)S(1)}, u32[]{:S(2)}, u32[]{:S(2)}) collective-permute-start(bf16[16,512]{1,0:T(8,128)(2,1)S(1)} %get-tuple-element.30), channel_id=1, source_target_pairs={{0,24},{1,25},{2,26},{3,27},{4,28},{5,29},{6,30},{7,31},{8,16},{9,... | collective-permute-start | bytes 49160 | tf_op jit(solution)/shard_map/ppermute | solution.py:89
  54.5 4.0 %collective-permute-start.20 = (bf16[16,512]{1,0:T(8,128)(2,1)S(1)}, bf16[16,512]{1,0:T(8,128)(2,1)S(1)}, u32[]{:S(2)}, u32[]{:S(2)}) collective-permute-start(bf16[16,512]{1,0:T(8,128)(2,1)S(1)} %get-tuple-element.31), channel_id=1, source_target_pairs={{0,16},{1,17},{2,18},{3,19},{4,20},{5,21},{6,22},{7,23},{8,24},{9,... | collective-permute-start | bytes 49160 | tf_op jit(solution)/shard_map/ppermute | solution.py:89
  55.8 3.7 %collective-permute-start.21 = (bf16[16,512]{1,0:T(8,128)(2,1)S(1)}, bf16[16,512]{1,0:T(8,128)(2,1)S(1)}, u32[]{:S(2)}, u32[]{:S(2)}) collective-permute-start(bf16[16,512]{1,0:T(8,128)(2,1)S(1)} %get-tuple-element.32), channel_id=1, source_target_pairs={{0,8},{1,9},{2,10},{3,11},{4,12},{5,13},{6,14},{7,15},{8,0},{9,1},... | collective-permute-start | bytes 49160 | tf_op jit(solution)/shard_map/ppermute | solution.py:89

commit v4 on v3

--- a/solution.py
+++ b/solution.py
@@ -228,10 +228,6 @@
         )
 
     pack(out_ref, both(wi_ref, wi2_ref), both(wg_ref, wg2_ref), square)
-
-
-def sigmoid(x):
-    return 0.5 * jnp.tanh(0.5 * x) + 0.5
 
 
 def one_minus_square(decay, log_decay):
@@ -285,8 +281,8 @@
         )
         for b in range(blocks)
     ]
-    rec_gate = sigmoid(jnp.concatenate([m[:, :block] for m in maps], axis=1))
-    inp_gate = sigmoid(jnp.concatenate([m[:, block:] for m in maps], axis=1))
+    rec_gate = jax.nn.sigmoid(jnp.concatenate([m[:, :block] for m in maps], axis=1))
+    inp_gate = jax.nn.sigmoid(jnp.concatenate([m[:, block:] for m in maps], axis=1))
     log_decay = -8.0 * rec_gate * jax.nn.softplus(-decay_ref[layer : layer + 1, :])
     decay = jnp.exp(log_decay)
     hidden = decay * previous + jnp.sqrt(one_minus_square(decay, log_decay)) * (inp_gate * conv_out)

time: 60.4 us -> 60.4 us (level)
  no operation moved by 1% of the time
where the time goes in v4:
time: 60.4 us; the launch traced here: 60.1 us
  starting transfers between devices  28.4 us (47%)
  waiting for transfers between devices  22.3 us (37%)
  local copies, waits for them, and re-layouts  4.48 us (7%)
  Pallas kernels  2.96 us (5%)
  other arithmetic  1.25 us (2%)
  between operations  0.76 us (1%)
    ppermute x12, starting transfers between devices, core_exchange(): got.append(lax.ppermute(values[k % len(values)], ('tp', 'dp'), pairs))  17.4 us
    ppermute x12, waiting for transfers between devices, core_exchange(): got.append(lax.ppermute(values[k % len(values)], ('tp', 'dp'), pairs))  15.2 us
    ppermute x10, starting transfers between devices, partner_exchange(): got.append(lax.ppermute(value, axis, [(i, i ^ m) for i in range(count)]))  11 us
    ppermute x10, waiting for transfers between devices, partner_exchange(): got.append(lax.ppermute(value, axis, [(i, i ^ m) for i in range(count)]))  7.13 us
    unnamed x28, local copies, waits for them, and re-layouts  4.48 us
    pallas_call x11, Pallas kernels, call(): pl.pallas_call(kernel, out_shape=outs, in_specs=[spec] * len(args), out_s...  2.96 us
    another operation x3, other arithmetic, blocks(): return (mixed, jnp.stack(conv_list), jnp.stack(rec_list))  1.25 us
  transfers between devices with their start and end apart: 22, of which 14 were waited for; matrix products, arithmetic and copies ran while one was open for 2% of the time, Pallas kernels for 2%

profile of v4, /device:TPU:0, one launch (start us, length us, event | category | flops | bytes accessed | tf_op | source)
XLA Modules:
  0.0 60.1 jit_solution(8614076610335845616)
XLA Ops:
  0.6 0.6 collective-permute-start.8
  1.2 0.1 collective-permute-start.13
  1.3 0.4 collective-permute-start.14
  1.7 2.6 %collective-permute-start = (bf16[1,16,512]{2,1,0:T(8,128)(2,1)}, bf16[1,16,512]{2,1,0:T(8,128)(2,1)S(1)}, u32[]{:S(2)}, u32[]{:S(2)}) collective-permute-start(bf16[1,16,512]{2,1,0:T(8,128)(2,1)} %bitcast.17), channel_id=1, source_target_pairs={{0,8},{8,0},{16,24},{24,16},{1,9},{9,1},{17,25},{25,17},{2,10},{10... | collective-permute-start | bytes 49160 | tf_op jit(solution)/shard_map/ppermute | solution.py:61
  4.3 1.9 %collective-permute-done.second_ref = bf16[1,16,512]{2,1,0:T(8,128)(2,1)S(1)} collective-permute-done((bf16[1,16,512]{2,1,0:T(8,128)(2,1)}, bf16[1,16,512]{2,1,0:T(8,128)(2,1)S(1)}, u32[]{:S(2)}, u32[]{:S(2)}) %collective-permute-start) | collective-permute-done | bytes 16416 | tf_op jit(solution)/shard_map/ppermute | solution.py:61
  6.2 0.7 %copy-done.11 = bf16[16,512]{1,0:T(8,128)(2,1)S(1)} copy-done((bf16[16,512]{1,0:T(8,128)(2,1)S(1)}, bf16[16,512]{1,0:T(8,128)(2,1)}, u32[]{:S(2)}) %copy-start.11) | copy-done | bytes 16408
  6.9 2.1 %collective-permute-start.1 = (bf16[2,16,512]{2,1,0:T(8,128)(2,1)S(1)}, bf16[2,16,512]{2,1,0:T(8,128)(2,1)S(1)}, u32[]{:S(2)}, u32[]{:S(2)}) collective-permute-start(bf16[2,16,512]{2,1,0:T(8,128)(2,1)S(1)} %shard_map.139.low_ref), channel_id=1, source_target_pairs={{0,16},{8,24},{16,0},{24,8},{1,17},{9,25},{17,1},{25,9},{2,18},{10... | collective-permute-start | bytes 98312 | tf_op jit(solution)/shard_map/ppermute | solution.py:61
  9.0 1.9 %collective-permute-done.1.high_ref = bf16[2,16,512]{2,1,0:T(8,128)(2,1)S(1)} collective-permute-done((bf16[2,16,512]{2,1,0:T(8,128)(2,1)S(1)}, bf16[2,16,512]{2,1,0:T(8,128)(2,1)S(1)}, u32[]{:S(2)}, u32[]{:S(2)}) %collective-permute-start.1) | collective-permute-done | bytes 32800 | tf_op jit(solution)/shard_map/ppermute | solution.py:61
  10.9 1.2 %copy-done.1 = bf16[2,512,512]{2,1,0:T(8,128)(2,1)S(1)} copy-done((bf16[2,512,512]{2,1,0:T(8,128)(2,1)S(1)}, bf16[2,512,512]{2,1,0:T(8,128)(2,1)}, u32[]{:S(2)}) %copy-start.1) | copy-done | bytes 1048600
  12.1 1.2 %copy-done.3 = bf16[2,512,512]{2,1,0:T(8,128)(2,1)S(1)} copy-done((bf16[2,512,512]{2,1,0:T(8,128)(2,1)S(1)}, bf16[2,512,512]{2,1,0:T(8,128)(2,1)}, u32[]{:S(2)}) %copy-start.3) | copy-done | bytes 1048600
  13.3 0.3 shard_map.140
  13.6 0.0 copy-start.13
  13.7 0.1 collective-permute-start.2
  13.7 0.6 copy-done.13
  14.3 0.1 shard_map.142.lengths_ref
  14.4 0.7 %copy-done.7 = bf16[2,3,8,512]{3,2,1,0:T(8,128)(2,1)S(1)} copy-done((bf16[2,3,8,512]{3,2,1,0:T(8,128)(2,1)S(1)}, bf16[2,3,8,512]{3,2,1,0:T(8,128)(2,1)}, u32[]{:S(2)}) %copy-start.7) | copy-done | bytes 49176
  15.1 0.0 copy-done.9
  15.1 0.1 shard_map.143
  15.2 2.1 %collective-permute-start.6 = (bf16[1,2,2,8,512]{4,3,2,1,0:T(8,128)(2,1)S(1)}, bf16[1,2,2,8,512]{4,3,2,1,0:T(8,128)(2,1)S(1)}, u32[]{:S(2)}, u32[]{:S(2)}) collective-permute-start(bf16[1,2,2,8,512]{4,3,2,1,0:T(8,128)(2,1)S(1)} %bitcast.15), channel_id=1, source_target_pairs={{0,2},{1,3},{2,0},{3,1},{4,6},{5,7},{6,4},{7,5},{8,10},{9,11},{10,... | collective-permute-start | bytes 98312 | tf_op jit(solution)/shard_map/ppermute | solution.py:61
  17.4 1.9 %collective-permute-done.6.second_ref = bf16[1,2,2,8,512]{4,3,2,1,0:T(8,128)(2,1)S(1)} collective-permute-done((bf16[1,2,2,8,512]{4,3,2,1,0:T(8,128)(2,1)S(1)}, bf16[1,2,2,8,512]{4,3,2,1,0:T(8,128)(2,1)S(1)}, u32[]{:S(2)}, u32[]{:S(2)}) %collective-permute-start.6) | collective-permute-done | bytes 32800 | tf_op jit(solution)/shard_map/ppermute | solution.py:61
  19.3 3.0 %collective-permute-start.7 = (bf16[2,2,2,8,512]{4,3,2,1,0:T(8,128)(2,1)S(1)}, bf16[2,2,2,8,512]{4,3,2,1,0:T(8,128)(2,1)S(1)}, u32[]{:S(2)}, u32[]{:S(2)}) collective-permute-start(bf16[2,2,2,8,512]{4,3,2,1,0:T(8,128)(2,1)S(1)} %shard_map.144.refs_5_), channel_id=1, source_target_pairs={{0,4},{1,5},{2,6},{3,7},{4,0},{5,1},{6,2},{7,3},{8,12},{9,13},{10,... | collective-permute-start | bytes 196616 | tf_op jit(solution)/shard_map/ppermute | solution.py:61
  22.3 0.0 collective-permute-done.2.got_ref
  22.3 1.4 %collective-permute-start.3 = (bf16[264,128]{1,0:T(8,128)(2,1)S(1)}, bf16[264,128]{1,0:T(8,128)(2,1)S(1)}, u32[]{:S(2)}, u32[]{:S(2)}) collective-permute-start(bf16[264,128]{1,0:T(8,128)(2,1)S(1)} %shard_map.141.refs_0_), channel_id=1, source_target_pairs={{0,6},{1,7},{2,4},{3,5},{4,2},{5,3},{6,0},{7,1},{8,14},{9,15},{10,... | collective-permute-start | bytes 202760 | tf_op jit(solution)/shard_map/ppermute | solution.py:89
  23.7 0.8 %collective-permute-done.7.refs_6_ = bf16[2,2,2,8,512]{4,3,2,1,0:T(8,128)(2,1)S(1)} collective-permute-done((bf16[2,2,2,8,512]{4,3,2,1,0:T(8,128)(2,1)S(1)}, bf16[2,2,2,8,512]{4,3,2,1,0:T(8,128)(2,1)S(1)}, u32[]{:S(2)}, u32[]{:S(2)}) %collective-permute-start.7) | collective-permute-done | bytes 65568 | tf_op jit(solution)/shard_map/ppermute | solution.py:61
  24.6 3.0 %collective-permute-start.4 = (bf16[264,128]{1,0:T(8,128)(2,1)S(1)}, bf16[264,128]{1,0:T(8,128)(2,1)S(1)}, u32[]{:S(2)}, u32[]{:S(2)}) collective-permute-start(bf16[264,128]{1,0:T(8,128)(2,1)S(1)} %shard_map.141.refs_0_), channel_id=1, source_target_pairs={{0,2},{1,3},{2,0},{3,1},{4,6},{5,7},{6,4},{7,5},{8,10},{9,11},{10,... | collective-permute-start | bytes 202760 | tf_op jit(solution)/shard_map/ppermute | solution.py:89
  27.6 1.1 %collective-permute-done.3.refs_1_ = bf16[264,128]{1,0:T(8,128)(2,1)S(1)} collective-permute-done((bf16[264,128]{1,0:T(8,128)(2,1)S(1)}, bf16[264,128]{1,0:T(8,128)(2,1)S(1)}, u32[]{:S(2)}, u32[]{:S(2)}) %collective-permute-start.3) | collective-permute-done | bytes 67616 | tf_op jit(solution)/shard_map/ppermute | solution.py:89
  28.7 2.3 %collective-permute-start.5 = (bf16[264,128]{1,0:T(8,128)(2,1)S(1)}, bf16[264,128]{1,0:T(8,128)(2,1)S(1)}, u32[]{:S(2)}, u32[]{:S(2)}) collective-permute-start(bf16[264,128]{1,0:T(8,128)(2,1)S(1)} %shard_map.141.refs_0_), channel_id=1, source_target_pairs={{0,4},{1,5},{2,6},{3,7},{4,0},{5,1},{6,2},{7,3},{8,12},{9,13},{10,... | collective-permute-start | bytes 202760 | tf_op jit(solution)/shard_map/ppermute | solution.py:89
  31.0 0.0 collective-permute-done.4.refs_2_
  31.0 0.0 collective-permute-start.12
  31.0 3.1 %collective-permute-done.5.refs_3_ = bf16[264,128]{1,0:T(8,128)(2,1)S(1)} collective-permute-done((bf16[264,128]{1,0:T(8,128)(2,1)S(1)}, bf16[264,128]{1,0:T(8,128)(2,1)S(1)}, u32[]{:S(2)}, u32[]{:S(2)}) %collective-permute-start.5) | collective-permute-done | bytes 67616 | tf_op jit(solution)/shard_map/ppermute | solution.py:89
  34.2 0.0 collective-permute-done.8.refs_12_
  34.2 0.0 copy-done.5
  34.2 0.0 copy-start.2
  34.2 0.0 copy-start.4
  34.2 0.6 %shard_map.145 = (bf16[32,1024]{1,0:T(8,128)(2,1)S(1)}, bf16[8,512]{1,0:T(8,128)(2,1)S(1)}, f32[8,512]{1,0:T(8,128)S(1)}) custom-call(bf16[264,128]{1,0:T(8,128)(2,1)S(1)} %shard_map.141.refs_0_, bf16[264,128]{1,0:T(8,128)(2,1)S(1)} %collective-permute-done.3.refs_1_, bf16[264,128]{1,0:T(8,128)(2,1)S(1)} %collective-permute-done.4.refs_2_, ...), custom_call_target="tpu_custom_call" | custom-call | flops 1000000 | bytes 1048576 | tf_op jit(solution)/shard_map/pallas_call | solution.py:21
  34.8 1.6 %collective-permute-start.10 = (bf16[32,1024]{1,0:T(8,128)(2,1)S(1)}, bf16[32,1024]{1,0:T(8,128)(2,1)S(1)}, u32[]{:S(2)}, u32[]{:S(2)}) collective-permute-start(bf16[32,1024]{1,0:T(8,128)(2,1)S(1)} %get-tuple-element.25.refs_0_), channel_id=1, source_target_pairs={{0,16},{1,25},{2,18},{3,27},{4,20},{5,29},{6,22},{7,31},{8,24},{9,... | collective-permute-start | bytes 196616 | tf_op jit(solution)/shard_map/ppermute | solution.py:89
  36.4 1.5 %collective-permute-start.11 = (bf16[32,1024]{1,0:T(8,128)(2,1)S(1)}, bf16[32,1024]{1,0:T(8,128)(2,1)S(1)}, u32[]{:S(2)}, u32[]{:S(2)}) collective-permute-start(bf16[32,1024]{1,0:T(8,128)(2,1)S(1)} %get-tuple-element.25.refs_0_), channel_id=1, source_target_pairs={{0,8},{1,9},{2,10},{3,11},{4,12},{5,13},{6,14},{7,15},{8,0},{9,1},... | collective-permute-start | bytes 196616 | tf_op jit(solution)/shard_map/ppermute | solution.py:89
  37.9 0.0 collective-permute-done.12.refs_7_
  37.9 0.5 collective-permute-start.9
  38.4 0.0 collective-permute-done.13.refs_8_
  38.4 0.0 collective-permute-done.14.refs_9_
  38.4 0.8 %collective-permute-done.10.refs_2_ = bf16[32,1024]{1,0:T(8,128)(2,1)S(1)} collective-permute-done((bf16[32,1024]{1,0:T(8,128)(2,1)S(1)}, bf16[32,1024]{1,0:T(8,128)(2,1)S(1)}, u32[]{:S(2)}, u32[]{:S(2)}) %collective-permute-start.10) | collective-permute-done | bytes 65568 | tf_op jit(solution)/shard_map/ppermute | solution.py:89
  39.2 1.5 %collective-permute-done.11.refs_3_ = bf16[32,1024]{1,0:T(8,128)(2,1)S(1)} collective-permute-done((bf16[32,1024]{1,0:T(8,128)(2,1)S(1)}, bf16[32,1024]{1,0:T(8,128)(2,1)S(1)}, u32[]{:S(2)}, u32[]{:S(2)}) %collective-permute-start.11) | collective-permute-done | bytes 65568 | tf_op jit(solution)/shard_map/ppermute | solution.py:89
  40.7 2.4 %collective-permute-done.9.refs_1_ = bf16[32,1024]{1,0:T(8,128)(2,1)S(1)} collective-permute-done((bf16[32,1024]{1,0:T(8,128)(2,1)S(1)}, bf16[32,1024]{1,0:T(8,128)(2,1)S(1)}, u32[]{:S(2)}, u32[]{:S(2)}) %collective-permute-start.9) | collective-permute-done | bytes 65568 | tf_op jit(solution)/shard_map/ppermute | solution.py:89
  43.1 0.4 shard_map.146
  43.5 2.1 %collective-permute-start.15 = (bf16[264,128]{1,0:T(8,128)(2,1)S(1)}, bf16[264,128]{1,0:T(8,128)(2,1)S(1)}, u32[]{:S(2)}, u32[]{:S(2)}) collective-permute-start(bf16[264,128]{1,0:T(8,128)(2,1)S(1)} %get-tuple-element.26.refs_0_), channel_id=1, source_target_pairs={{0,4},{1,5},{2,6},{3,7},{4,0},{5,1},{6,2},{7,3},{8,12},{9,13},{10,... | collective-permute-start | bytes 202760 | tf_op jit(solution)/shard_map/ppermute | solution.py:89
  45.6 0.2 collective-permute-start.16
  45.8 1.3 %collective-permute-start.17 = (bf16[264,128]{1,0:T(8,128)(2,1)S(1)}, bf16[264,128]{1,0:T(8,128)(2,1)S(1)}, u32[]{:S(2)}, u32[]{:S(2)}) collective-permute-start(bf16[264,128]{1,0:T(8,128)(2,1)S(1)} %get-tuple-element.26.refs_0_), channel_id=1, source_target_pairs={{0,2},{1,3},{2,0},{3,1},{4,6},{5,7},{6,4},{7,5},{8,10},{9,11},{10,... | collective-permute-start | bytes 202760 | tf_op jit(solution)/shard_map/ppermute | solution.py:89
  47.0 1.7 %collective-permute-done.15.refs_1_ = bf16[264,128]{1,0:T(8,128)(2,1)S(1)} collective-permute-done((bf16[264,128]{1,0:T(8,128)(2,1)S(1)}, bf16[264,128]{1,0:T(8,128)(2,1)S(1)}, u32[]{:S(2)}, u32[]{:S(2)}) %collective-permute-start.15) | collective-permute-done | bytes 67616 | tf_op jit(solution)/shard_map/ppermute | solution.py:89
  48.7 2.9 %collective-permute-done.16.refs_2_ = bf16[264,128]{1,0:T(8,128)(2,1)S(1)} collective-permute-done((bf16[264,128]{1,0:T(8,128)(2,1)S(1)}, bf16[264,128]{1,0:T(8,128)(2,1)S(1)}, u32[]{:S(2)}, u32[]{:S(2)}) %collective-permute-start.16) | collective-permute-done | bytes 67616 | tf_op jit(solution)/shard_map/ppermute | solution.py:89
  51.7 0.0 collective-permute-done.17.refs_3_
  51.7 0.5 shard_map.147
  52.1 0.1 collective-permute-start.18
  52.2 0.6 %pad_maximum_fusion = bf16[2,3,8,512]{3,2,1,0:T(8,128)(2,1)} fusion(bf16[1,3,8,512]{3,2,1,0:T(8,128)(2,1)S(1)} %get-tuple-element.40, bf16[1,3,8,512]{3,2,1,0:T(8,128)(2,1)S(1)} %get-tuple-element.39), kind=kLoop, calls=%fused_computation | loop fusion | flops 24576 | bytes 98304 | tf_op jit(solution)/shard_map/stack | solution.py:428
  52.8 0.6 collective-permute-done.18.other_ref
  53.4 0.3 shard_map.148
  53.7 0.8 %collective-permute-start.19 = (bf16[16,512]{1,0:T(8,128)(2,1)S(1)}, bf16[16,512]{1,0:T(8,128)(2,1)S(1)}, u32[]{:S(2)}, u32[]{:S(2)}) collective-permute-start(bf16[16,512]{1,0:T(8,128)(2,1)S(1)} %get-tuple-element.30), channel_id=1, source_target_pairs={{0,24},{1,25},{2,26},{3,27},{4,28},{5,29},{6,30},{7,31},{8,16},{9,... | collective-permute-start | bytes 49160 | tf_op jit(solution)/shard_map/ppermute | solution.py:89
  54.5 1.3 %collective-permute-start.20 = (bf16[16,512]{1,0:T(8,128)(2,1)S(1)}, bf16[16,512]{1,0:T(8,128)(2,1)S(1)}, u32[]{:S(2)}, u32[]{:S(2)}) collective-permute-start(bf16[16,512]{1,0:T(8,128)(2,1)S(1)} %get-tuple-element.31), channel_id=1, source_target_pairs={{0,16},{1,17},{2,18},{3,19},{4,20},{5,21},{6,22},{7,23},{8,24},{9,... | collective-permute-start | bytes 49160 | tf_op jit(solution)/shard_map/ppermute | solution.py:89
  55.8 1.5 %collective-permute-start.21 = (bf16[16,512]{1,0:T(8,128)(2,1)S(1)}, bf16[16,512]{1,0:T(8,128)(2,1)S(1)}, u32[]{:S(2)}, u32[]{:S(2)}) collective-permute-start(bf16[16,512]{1,0:T(8,128)(2,1)S(1)} %get-tuple-element.32), channel_id=1, source_target_pairs={{0,8},{1,9},{2,10},{3,11},{4,12},{5,13},{6,14},{7,15},{8,0},{9,1},... | collective-permute-start | bytes 49160 | tf_op jit(solution)/shard_map/ppermute | solution.py:89
  57.3 0.6 %pad_maximum_fusion.1 = f32[2,8,512]{2,1,0:T(8,128)} fusion(f32[1,8,512]{2,1,0:T(8,128)S(1)} %bitcast.20, f32[1,8,512]{2,1,0:T(8,128)S(1)} %bitcast.19), kind=kLoop, calls=%fused_computation.1 | loop fusion | flops 8192 | bytes 65536 | tf_op jit(solution)/shard_map/stack | solution.py:428
  57.9 0.6 collective-permute-done.19.refs_0_
  58.5 0.0 collective-permute-done.20.refs_1_
  58.5 1.0 %collective-permute-done.21.refs_2_ = bf16[16,512]{1,0:T(8,128)(2,1)S(1)} collective-permute-done((bf16[16,512]{1,0:T(8,128)(2,1)S(1)}, bf16[16,512]{1,0:T(8,128)(2,1)S(1)}, u32[]{:S(2)}, u32[]{:S(2)}) %collective-permute-start.21) | collective-permute-done | bytes 16416 | tf_op jit(solution)/shard_map/ppermute | solution.py:89
  59.5 0.6 %shard_map.149 = bf16[16,512]{1,0:T(8,128)(2,1)} custom-call(f32[16,512]{1,0:T(8,128)S(1)} %get-tuple-element.29.own_ref, bf16[16,512]{1,0:T(8,128)(2,1)S(1)} %collective-permute-done.19.refs_0_, bf16[16,512]{1,0:T(8,128)(2,1)S(1)} %collective-permute-done.20.refs_1_, bf16[16,512]{1,0:T(8,128)(2,1)S(1)} %collective-permute-done.21.refs_2_), custom_call_target="tpu_custom_call" | custom-call | flops 1000000 | bytes 1048576 | tf_op jit(solution)/shard_map/pallas_call | solution.py:21
  (23 shorter events, 0.1 us)
Async XLA Ops:
  0.6 33.5 %collective-permute-start.8 = (bf16[2,512,512]{2,1,0:T(8,128)(2,1)}, bf16[2,512,512]{2,1,0:T(8,128)(2,1)S(1)}, u32[]{:S(2)}, u32[]{:S(2)}) collective-permute-start(bf16[2,512,512]{2,1,0:T(8,128)(2,1)} %w_ref.1), channel_id=1, source_target_pairs={{0,1},{1,0},{2,3},{3,2},{4,5},{5,4},{6,7},{7,6},{8,9},{9,8},{10,11... | collective-permute-start | bytes 3145736 | tf_op jit(solution)/shard_map/ppermute | solution.py:61
  1.2 37.2 %collective-permute-start.13 = (bf16[2,512,512]{2,1,0:T(8,128)(2,1)}, bf16[2,512,512]{2,1,0:T(8,128)(2,1)S(1)}, u32[]{:S(2)}, u32[]{:S(2)}) collective-permute-start(bf16[2,512,512]{2,1,0:T(8,128)(2,1)} %refs_5_.1), channel_id=1, source_target_pairs={{0,1},{1,0},{2,3},{3,2},{4,5},{5,4},{6,7},{7,6},{8,9},{9,8},{10,11... | collective-permute-start | bytes 3145736 | tf_op jit(solution)/shard_map/ppermute | solution.py:61
  1.3 37.1 %collective-permute-start.14 = (bf16[2,512,512]{2,1,0:T(8,128)(2,1)}, bf16[2,512,512]{2,1,0:T(8,128)(2,1)S(1)}, u32[]{:S(2)}, u32[]{:S(2)}) collective-permute-start(bf16[2,512,512]{2,1,0:T(8,128)(2,1)} %refs_6_.1), channel_id=1, source_target_pairs={{0,1},{1,0},{2,3},{3,2},{4,5},{5,4},{6,7},{7,6},{8,9},{9,8},{10,11... | collective-permute-start | bytes 3145736 | tf_op jit(solution)/shard_map/ppermute | solution.py:61
  1.7 4.5 %collective-permute-start = (bf16[1,16,512]{2,1,0:T(8,128)(2,1)}, bf16[1,16,512]{2,1,0:T(8,128)(2,1)S(1)}, u32[]{:S(2)}, u32[]{:S(2)}) collective-permute-start(bf16[1,16,512]{2,1,0:T(8,128)(2,1)} %bitcast.17), channel_id=1, source_target_pairs={{0,8},{8,0},{16,24},{24,16},{1,9},{9,1},{17,25},{25,17},{2,10},{10... | collective-permute-start | bytes 49160 | tf_op jit(solution)/shard_map/ppermute | solution.py:61
  6.2 0.7 %copy-start.11 = (bf16[16,512]{1,0:T(8,128)(2,1)S(1)}, bf16[16,512]{1,0:T(8,128)(2,1)}, u32[]{:S(2)}) copy-start(bf16[16,512]{1,0:T(8,128)(2,1)} %param.12) | copy-start | bytes 49156
  6.9 4.0 %copy-start.12 = (f32[2,512]{1,0:T(2,128)S(1)}, f32[2,512]{1,0:T(2,128)}, u32[]{:S(2)}) copy-start(f32[2,512]{1,0:T(2,128)} %refs_4_.1) | copy-start | bytes 12292
  6.9 3.9 %collective-permute-start.1 = (bf16[2,16,512]{2,1,0:T(8,128)(2,1)S(1)}, bf16[2,16,512]{2,1,0:T(8,128)(2,1)S(1)}, u32[]{:S(2)}, u32[]{:S(2)}) collective-permute-start(bf16[2,16,512]{2,1,0:T(8,128)(2,1)S(1)} %shard_map.139.low_ref), channel_id=1, source_target_pairs={{0,16},{8,24},{16,0},{24,8},{1,17},{9,25},{17,1},{25,9},{2,18},{10... | collective-permute-start | bytes 98312 | tf_op jit(solution)/shard_map/ppermute | solution.py:61
  10.9 1.2 %copy-start.1 = (bf16[2,512,512]{2,1,0:T(8,128)(2,1)S(1)}, bf16[2,512,512]{2,1,0:T(8,128)(2,1)}, u32[]{:S(2)}) copy-start(bf16[2,512,512]{2,1,0:T(8,128)(2,1)} %refs_5_.1) | copy-start | bytes 3145732
  12.1 1.2 %copy-start.3 = (bf16[2,512,512]{2,1,0:T(8,128)(2,1)S(1)}, bf16[2,512,512]{2,1,0:T(8,128)(2,1)}, u32[]{:S(2)}) copy-start(bf16[2,512,512]{2,1,0:T(8,128)(2,1)} %refs_6_.1) | copy-start | bytes 3145732
  13.6 0.7 %copy-start.13 = (s32[8]{0:T(128)S(1)}, s32[8]{0:T(128)}, u32[]{:S(2)}) copy-start(s32[8]{0:T(128)} %param.21) | copy-start | bytes 100
  13.7 8.6 %collective-permute-start.2 = (bf16[392,128]{1,0:T(8,128)(2,1)S(1)}, bf16[392,128]{1,0:T(8,128)(2,1)S(1)}, u32[]{:S(2)}, u32[]{:S(2)}) collective-permute-start(bf16[392,128]{1,0:T(8,128)(2,1)S(1)} %get-tuple-element.21), channel_id=1, source_target_pairs={{0,1},{1,0},{2,3},{3,2},{4,5},{5,4},{6,7},{7,6},{8,9},{9,8},{10,11... | collective-permute-start | bytes 301064 | tf_op jit(solution)/shard_map/ppermute | solution.py:61
  14.3 0.8 %copy-start.7 = (bf16[2,3,8,512]{3,2,1,0:T(8,128)(2,1)S(1)}, bf16[2,3,8,512]{3,2,1,0:T(8,128)(2,1)}, u32[]{:S(2)}) copy-start(bf16[2,3,8,512]{3,2,1,0:T(8,128)(2,1)} %conv_ref.1) | copy-start | bytes 147460
  14.3 0.8 %copy-start.8 = (bf16[2,4,512]{2,1,0:T(4,128)(2,1)S(1)}, bf16[2,4,512]{2,1,0:T(4,128)(2,1)}, u32[]{:S(2)}) copy-start(bf16[2,4,512]{2,1,0:T(4,128)(2,1)} %refs_7_.3) | copy-start | bytes 24580
  14.3 0.8 %copy-start.9 = (f32[2,8,512]{2,1,0:T(8,128)S(1)}, f32[2,8,512]{2,1,0:T(8,128)}, u32[]{:S(2)}) copy-start(f32[2,8,512]{2,1,0:T(8,128)} %rec_ref.1) | copy-start | bytes 98308
  14.3 19.9 %copy-start = (bf16[2,512,512]{2,1,0:T(8,128)(2,1)S(1)}, bf16[2,512,512]{2,1,0:T(8,128)(2,1)}, u32[]{:S(2)}) copy-start(bf16[2,512,512]{2,1,0:T(8,128)(2,1)} %w_ref.1) | copy-start | bytes 3145732
  15.1 19.1 %copy-start.5 = (bf16[2,4,128,128]{3,2,1,0:T(8,128)(2,1)S(1)}, bf16[2,4,128,128]{3,2,1,0:T(8,128)(2,1)}, u32[]{:S(2)}) copy-start(bf16[2,4,128,128]{3,2,1,0:T(8,128)(2,1)} %refs_9_.3) | copy-start | bytes 786436
  15.1 19.1 %copy-start.6 = (bf16[2,4,128,128]{3,2,1,0:T(8,128)(2,1)S(1)}, bf16[2,4,128,128]{3,2,1,0:T(8,128)(2,1)}, u32[]{:S(2)}) copy-start(bf16[2,4,128,128]{3,2,1,0:T(8,128)(2,1)} %refs_10_.3) | copy-start | bytes 786436
  15.2 4.0 %collective-permute-start.6 = (bf16[1,2,2,8,512]{4,3,2,1,0:T(8,128)(2,1)S(1)}, bf16[1,2,2,8,512]{4,3,2,1,0:T(8,128)(2,1)S(1)}, u32[]{:S(2)}, u32[]{:S(2)}) collective-permute-start(bf16[1,2,2,8,512]{4,3,2,1,0:T(8,128)(2,1)S(1)} %bitcast.15), channel_id=1, source_target_pairs={{0,2},{1,3},{2,0},{3,1},{4,6},{5,7},{6,4},{7,5},{8,10},{9,11},{10,... | collective-permute-start | bytes 98312 | tf_op jit(solution)/shard_map/ppermute | solution.py:61
  19.3 5.3 %collective-permute-start.7 = (bf16[2,2,2,8,512]{4,3,2,1,0:T(8,128)(2,1)S(1)}, bf16[2,2,2,8,512]{4,3,2,1,0:T(8,128)(2,1)S(1)}, u32[]{:S(2)}, u32[]{:S(2)}) collective-permute-start(bf16[2,2,2,8,512]{4,3,2,1,0:T(8,128)(2,1)S(1)} %shard_map.144.refs_5_), channel_id=1, source_target_pairs={{0,4},{1,5},{2,6},{3,7},{4,0},{5,1},{6,2},{7,3},{8,12},{9,13},{10,... | collective-permute-start | bytes 196616 | tf_op jit(solution)/shard_map/ppermute | solution.py:61
  22.3 11.9 %copy-start.10 = (f32[2,512]{1,0:T(2,128)S(1)}, f32[2,512]{1,0:T(2,128)}, u32[]{:S(2)}) copy-start(f32[2,512]{1,0:T(2,128)} %refs_8_.3) | copy-start | bytes 12292
  22.3 6.4 %collective-permute-start.3 = (bf16[264,128]{1,0:T(8,128)(2,1)S(1)}, bf16[264,128]{1,0:T(8,128)(2,1)S(1)}, u32[]{:S(2)}, u32[]{:S(2)}) collective-permute-start(bf16[264,128]{1,0:T(8,128)(2,1)S(1)} %shard_map.141.refs_0_), channel_id=1, source_target_pairs={{0,6},{1,7},{2,4},{3,5},{4,2},{5,3},{6,0},{7,1},{8,14},{9,15},{10,... | collective-permute-start | bytes 202760 | tf_op jit(solution)/shard_map/ppermute | solution.py:89
  24.6 6.4 %collective-permute-start.4 = (bf16[264,128]{1,0:T(8,128)(2,1)S(1)}, bf16[264,128]{1,0:T(8,128)(2,1)S(1)}, u32[]{:S(2)}, u32[]{:S(2)}) collective-permute-start(bf16[264,128]{1,0:T(8,128)(2,1)S(1)} %shard_map.141.refs_0_), channel_id=1, source_target_pairs={{0,2},{1,3},{2,0},{3,1},{4,6},{5,7},{6,4},{7,5},{8,10},{9,11},{10,... | collective-permute-start | bytes 202760 | tf_op jit(solution)/shard_map/ppermute | solution.py:89
  28.7 5.5 %collective-permute-start.5 = (bf16[264,128]{1,0:T(8,128)(2,1)S(1)}, bf16[264,128]{1,0:T(8,128)(2,1)S(1)}, u32[]{:S(2)}, u32[]{:S(2)}) collective-permute-start(bf16[264,128]{1,0:T(8,128)(2,1)S(1)} %shard_map.141.refs_0_), channel_id=1, source_target_pairs={{0,4},{1,5},{2,6},{3,7},{4,0},{5,1},{6,2},{7,3},{8,12},{9,13},{10,... | collective-permute-start | bytes 202760 | tf_op jit(solution)/shard_map/ppermute | solution.py:89
  31.0 6.9 %collective-permute-start.12 = (f32[2,512]{1,0:T(2,128)S(1)}, f32[2,512]{1,0:T(2,128)S(1)}, u32[]{:S(2)}, u32[]{:S(2)}) collective-permute-start(f32[2,512]{1,0:T(2,128)S(1)} %copy-done.12), channel_id=1, source_target_pairs={{0,1},{1,0},{2,3},{3,2},{4,5},{5,4},{6,7},{7,6},{8,9},{9,8},{10,11... | collective-permute-start | bytes 12296 | tf_op jit(solution)/shard_map/ppermute | solution.py:61
  34.2 8.9 %copy-start.2 = (bf16[2,512,512]{2,1,0:T(8,128)(2,1)S(1)}, bf16[2,512,512]{2,1,0:T(8,128)(2,1)}, u32[]{:S(2)}) copy-start(bf16[2,512,512]{2,1,0:T(8,128)(2,1)} %refs_5_.1) | copy-start | bytes 3145732
  34.2 8.9 %copy-start.4 = (bf16[2,512,512]{2,1,0:T(8,128)(2,1)S(1)}, bf16[2,512,512]{2,1,0:T(8,128)(2,1)}, u32[]{:S(2)}) copy-start(bf16[2,512,512]{2,1,0:T(8,128)(2,1)} %refs_6_.1) | copy-start | bytes 3145732
  34.8 4.3 %collective-permute-start.10 = (bf16[32,1024]{1,0:T(8,128)(2,1)S(1)}, bf16[32,1024]{1,0:T(8,128)(2,1)S(1)}, u32[]{:S(2)}, u32[]{:S(2)}) collective-permute-start(bf16[32,1024]{1,0:T(8,128)(2,1)S(1)} %get-tuple-element.25.refs_0_), channel_id=1, source_target_pairs={{0,16},{1,25},{2,18},{3,27},{4,20},{5,29},{6,22},{7,31},{8,24},{9,... | collective-permute-start | bytes 196616 | tf_op jit(solution)/shard_map/ppermute | solution.py:89
  36.4 4.3 %collective-permute-start.11 = (bf16[32,1024]{1,0:T(8,128)(2,1)S(1)}, bf16[32,1024]{1,0:T(8,128)(2,1)S(1)}, u32[]{:S(2)}, u32[]{:S(2)}) collective-permute-start(bf16[32,1024]{1,0:T(8,128)(2,1)S(1)} %get-tuple-element.25.refs_0_), channel_id=1, source_target_pairs={{0,8},{1,9},{2,10},{3,11},{4,12},{5,13},{6,14},{7,15},{8,0},{9,1},... | collective-permute-start | bytes 196616 | tf_op jit(solution)/shard_map/ppermute | solution.py:89
  37.9 5.2 %collective-permute-start.9 = (bf16[32,1024]{1,0:T(8,128)(2,1)S(1)}, bf16[32,1024]{1,0:T(8,128)(2,1)S(1)}, u32[]{:S(2)}, u32[]{:S(2)}) collective-permute-start(bf16[32,1024]{1,0:T(8,128)(2,1)S(1)} %get-tuple-element.25.refs_0_), channel_id=1, source_target_pairs={{0,24},{1,17},{2,26},{3,19},{4,28},{5,21},{6,30},{7,23},{8,16},{9,... | collective-permute-start | bytes 196616 | tf_op jit(solution)/shard_map/ppermute | solution.py:89
  43.5 5.2 %collective-permute-start.15 = (bf16[264,128]{1,0:T(8,128)(2,1)S(1)}, bf16[264,128]{1,0:T(8,128)(2,1)S(1)}, u32[]{:S(2)}, u32[]{:S(2)}) collective-permute-start(bf16[264,128]{1,0:T(8,128)(2,1)S(1)} %get-tuple-element.26.refs_0_), channel_id=1, source_target_pairs={{0,4},{1,5},{2,6},{3,7},{4,0},{5,1},{6,2},{7,3},{8,12},{9,13},{10,... | collective-permute-start | bytes 202760 | tf_op jit(solution)/shard_map/ppermute | solution.py:89
  45.6 6.1 %collective-permute-start.16 = (bf16[264,128]{1,0:T(8,128)(2,1)S(1)}, bf16[264,128]{1,0:T(8,128)(2,1)S(1)}, u32[]{:S(2)}, u32[]{:S(2)}) collective-permute-start(bf16[264,128]{1,0:T(8,128)(2,1)S(1)} %get-tuple-element.26.refs_0_), channel_id=1, source_target_pairs={{0,6},{1,7},{2,4},{3,5},{4,2},{5,3},{6,0},{7,1},{8,14},{9,15},{10,... | collective-permute-start | bytes 202760 | tf_op jit(solution)/shard_map/ppermute | solution.py:89
  45.8 5.9 %collective-permute-start.17 = (bf16[264,128]{1,0:T(8,128)(2,1)S(1)}, bf16[264,128]{1,0:T(8,128)(2,1)S(1)}, u32[]{:S(2)}, u32[]{:S(2)}) collective-permute-start(bf16[264,128]{1,0:T(8,128)(2,1)S(1)} %get-tuple-element.26.refs_0_), channel_id=1, source_target_pairs={{0,2},{1,3},{2,0},{3,1},{4,6},{5,7},{6,4},{7,5},{8,10},{9,11},{10,... | collective-permute-start | bytes 202760 | tf_op jit(solution)/shard_map/ppermute | solution.py:89
  52.1 1.3 %collective-permute-start.18 = (bf16[40,512]{1,0:T(8,128)(2,1)S(1)}, bf16[40,512]{1,0:T(8,128)(2,1)S(1)}, u32[]{:S(2)}, u32[]{:S(2)}) collective-permute-start(bf16[40,512]{1,0:T(8,128)(2,1)S(1)} %get-tuple-element.28.own_ref), channel_id=1, source_target_pairs={{0,1},{1,0},{2,3},{3,2},{4,5},{5,4},{6,7},{7,6},{8,9},{9,8},{10,11... | collective-permute-start | bytes 122888 | tf_op jit(solution)/shard_map/ppermute | solution.py:61
  53.7 4.8 %collective-permute-start.19 = (bf16[16,512]{1,0:T(8,128)(2,1)S(1)}, bf16[16,512]{1,0:T(8,128)(2,1)S(1)}, u32[]{:S(2)}, u32[]{:S(2)}) collective-permute-start(bf16[16,512]{1,0:T(8,128)(2,1)S(1)} %get-tuple-element.30), channel_id=1, source_target_pairs={{0,24},{1,25},{2,26},{3,27},{4,28},{5,29},{6,30},{7,31},{8,16},{9,... | collective-permute-start | bytes 49160 | tf_op jit(solution)/shard_map/ppermute | solution.py:89
  54.5 4.0 %collective-permute-start.20 = (bf16[16,512]{1,0:T(8,128)(2,1)S(1)}, bf16[16,512]{1,0:T(8,128)(2,1)S(1)}, u32[]{:S(2)}, u32[]{:S(2)}) collective-permute-start(bf16[16,512]{1,0:T(8,128)(2,1)S(1)} %get-tuple-element.31), channel_id=1, source_target_pairs={{0,16},{1,17},{2,18},{3,19},{4,20},{5,21},{6,22},{7,23},{8,24},{9,... | collective-permute-start | bytes 49160 | tf_op jit(solution)/shard_map/ppermute | solution.py:89
  55.8 3.7 %collective-permute-start.21 = (bf16[16,512]{1,0:T(8,128)(2,1)S(1)}, bf16[16,512]{1,0:T(8,128)(2,1)S(1)}, u32[]{:S(2)}, u32[]{:S(2)}) collective-permute-start(bf16[16,512]{1,0:T(8,128)(2,1)S(1)} %get-tuple-element.32), channel_id=1, source_target_pairs={{0,8},{1,9},{2,10},{3,11},{4,12},{5,13},{6,14},{7,15},{8,0},{9,1},... | collective-permute-start | bytes 49160 | tf_op jit(solution)/shard_map/ppermute | solution.py:89

commit v5 on v4

--- a/solution.py
+++ b/solution.py
@@ -224,7 +224,7 @@
 
     def both(w, w2):
         return jnp.dot(scaled, w[layer], preferred_element_type=F32) + jnp.dot(
-            scaled2, w2[layer], preferred_element_type=F32
+            scaled2, w2[layer - 1], preferred_element_type=F32
         )
 
     pack(out_ref, both(wi_ref, wi2_ref), both(wg_ref, wg2_ref), square)
@@ -394,7 +394,9 @@
             )
         sums = [summed] + core_exchange([summed], "z", f"sum{layer}")
         if layer == 0:
-            out2, *weights2 = [partner_exchange(w, "dp", [1])[0] for w in (w_output,) + weights]
+            out2, *weights2 = [
+                partner_exchange(w, "dp", [1])[0] for w in (w_output[:-1], norm_gain, w_input[1:], w_gate[1:])
+            ]
         block[0] = shape((half + lay.per_tp // 2, width) if last else (half, 2 * depth), BF16)
         readout, value, hidden = call(
             functools.partial(recurrence_kernel, lay, layer, features),

time: 60.4 us -> 58.5 us (0.969)
  local copies, waits for them, and re-layouts: 4.48 us -> 2.64 us
    unnamed x28 -> x24, local copies, waits for them, and re-layouts: 4.48 us -> 1.34 us
    slice x0 -> x3, local copies, waits for them, and re-layouts: none -> 1.29 us  [the longest x1 1.22 us: blocks(): w_output[:-1]]
where the time goes in v5:
time: 58.5 us; the launch traced here: 58.3 us
  starting transfers between devices  28.5 us (49%)
  waiting for transfers between devices  22.1 us (38%)
  Pallas kernels  2.96 us (5%)
  local copies, waits for them, and re-layouts  2.64 us (5%)
  other arithmetic  1.25 us (2%)
  between operations  0.78 us (1%)
    ppermute x12, starting transfers between devices, core_exchange(): got.append(lax.ppermute(values[k % len(values)], ('tp', 'dp'), pairs))  17.4 us
    ppermute x12, waiting for transfers between devices, core_exchange(): got.append(lax.ppermute(values[k % len(values)], ('tp', 'dp'), pairs))  15.2 us
    ppermute x10, starting transfers between devices, partner_exchange(): got.append(lax.ppermute(value, axis, [(i, i ^ m) for i in range(count)]))  11.2 us
    ppermute x10, waiting for transfers between devices, partner_exchange(): got.append(lax.ppermute(value, axis, [(i, i ^ m) for i in range(count)]))  6.92 us
    pallas_call x11, Pallas kernels, call(): pl.pallas_call(kernel, out_shape=outs, in_specs=[spec] * len(args), out_s...  2.96 us
    unnamed x24, local copies, waits for them, and re-layouts  1.34 us
    another operation x3, other arithmetic, blocks(): return (mixed, jnp.stack(conv_list), jnp.stack(rec_list))  1.25 us
    slice x1, local copies, waits for them, and re-layouts, blocks(): w_output[:-1]  1.22 us
  transfers between devices with their start and end apart: 22, of which 14 were waited for; matrix products, arithmetic and copies ran while one was open for 2% of the time, Pallas kernels for 2%

profile of v5, /device:TPU:0, one launch (start us, length us, event | category | flops | bytes accessed | tf_op | source)
XLA Modules:
  0.0 58.3 jit_solution(1809071848982878750)
XLA Ops:
  0.6 0.0 copy-start
  0.6 0.0 copy-start.1
  0.7 1.2 %slice.15 = bf16[1,512,512]{2,1,0:T(8,128)(2,1)S(1)} slice(bf16[2,512,512]{2,1,0:T(8,128)(2,1)} %w_ref.1), slice={[0:1], [0:512], [0:512]} | slice | bytes 1048576 | tf_op jit(solution)/shard_map/slice | solution.py:398
  1.9 0.6 collective-permute-start.8
  2.5 0.0 copy-start.10
  2.5 0.1 collective-permute-start.13
  2.6 0.0 copy-done.1
  2.7 0.5 collective-permute-start.14
  3.2 0.0 copy-done.10
  3.2 2.6 %collective-permute-start = (bf16[1,16,512]{2,1,0:T(8,128)(2,1)S(1)}, bf16[1,16,512]{2,1,0:T(8,128)(2,1)S(1)}, u32[]{:S(2)}, u32[]{:S(2)}) collective-permute-start(bf16[1,16,512]{2,1,0:T(8,128)(2,1)S(1)} %bitcast.17), channel_id=1, source_target_pairs={{0,8},{8,0},{16,24},{24,16},{1,9},{9,1},{17,25},{25,17},{2,10},{10... | collective-permute-start | bytes 49160 | tf_op jit(solution)/shard_map/ppermute | solution.py:61
  5.8 1.7 %collective-permute-done.second_ref = bf16[1,16,512]{2,1,0:T(8,128)(2,1)S(1)} collective-permute-done((bf16[1,16,512]{2,1,0:T(8,128)(2,1)S(1)}, bf16[1,16,512]{2,1,0:T(8,128)(2,1)S(1)}, u32[]{:S(2)}, u32[]{:S(2)}) %collective-permute-start) | collective-permute-done | bytes 16416 | tf_op jit(solution)/shard_map/ppermute | solution.py:61
  7.5 2.1 %collective-permute-start.1 = (bf16[2,16,512]{2,1,0:T(8,128)(2,1)S(1)}, bf16[2,16,512]{2,1,0:T(8,128)(2,1)S(1)}, u32[]{:S(2)}, u32[]{:S(2)}) collective-permute-start(bf16[2,16,512]{2,1,0:T(8,128)(2,1)S(1)} %shard_map.139.low_ref), channel_id=1, source_target_pairs={{0,16},{8,24},{16,0},{24,8},{1,17},{9,25},{17,1},{25,9},{2,18},{10... | collective-permute-start | bytes 98312 | tf_op jit(solution)/shard_map/ppermute | solution.py:61
  9.6 1.9 %collective-permute-done.1.high_ref = bf16[2,16,512]{2,1,0:T(8,128)(2,1)S(1)} collective-permute-done((bf16[2,16,512]{2,1,0:T(8,128)(2,1)S(1)}, bf16[2,16,512]{2,1,0:T(8,128)(2,1)S(1)}, u32[]{:S(2)}, u32[]{:S(2)}) %collective-permute-start.1) | collective-permute-done | bytes 32800 | tf_op jit(solution)/shard_map/ppermute | solution.py:61
  11.5 0.3 shard_map.140
  11.8 0.0 copy-start.11
  11.8 0.1 collective-permute-start.2
  11.9 0.6 copy-done.11
  12.5 0.1 shard_map.142.lengths_ref
  12.6 0.7 %copy-done.5 = bf16[2,3,8,512]{3,2,1,0:T(8,128)(2,1)S(1)} copy-done((bf16[2,3,8,512]{3,2,1,0:T(8,128)(2,1)S(1)}, bf16[2,3,8,512]{3,2,1,0:T(8,128)(2,1)}, u32[]{:S(2)}) %copy-start.5) | copy-done | bytes 49176
  13.3 0.1 shard_map.143
  13.4 2.1 %collective-permute-start.6 = (bf16[1,2,2,8,512]{4,3,2,1,0:T(8,128)(2,1)S(1)}, bf16[1,2,2,8,512]{4,3,2,1,0:T(8,128)(2,1)S(1)}, u32[]{:S(2)}, u32[]{:S(2)}) collective-permute-start(bf16[1,2,2,8,512]{4,3,2,1,0:T(8,128)(2,1)S(1)} %bitcast.15), channel_id=1, source_target_pairs={{0,2},{1,3},{2,0},{3,1},{4,6},{5,7},{6,4},{7,5},{8,10},{9,11},{10,... | collective-permute-start | bytes 98312 | tf_op jit(solution)/shard_map/ppermute | solution.py:61
  15.5 1.9 %collective-permute-done.6.second_ref = bf16[1,2,2,8,512]{4,3,2,1,0:T(8,128)(2,1)S(1)} collective-permute-done((bf16[1,2,2,8,512]{4,3,2,1,0:T(8,128)(2,1)S(1)}, bf16[1,2,2,8,512]{4,3,2,1,0:T(8,128)(2,1)S(1)}, u32[]{:S(2)}, u32[]{:S(2)}) %collective-permute-start.6) | collective-permute-done | bytes 32800 | tf_op jit(solution)/shard_map/ppermute | solution.py:61
  17.4 3.0 %collective-permute-start.7 = (bf16[2,2,2,8,512]{4,3,2,1,0:T(8,128)(2,1)S(1)}, bf16[2,2,2,8,512]{4,3,2,1,0:T(8,128)(2,1)S(1)}, u32[]{:S(2)}, u32[]{:S(2)}) collective-permute-start(bf16[2,2,2,8,512]{4,3,2,1,0:T(8,128)(2,1)S(1)} %shard_map.144.refs_5_), channel_id=1, source_target_pairs={{0,4},{1,5},{2,6},{3,7},{4,0},{5,1},{6,2},{7,3},{8,12},{9,13},{10,... | collective-permute-start | bytes 196616 | tf_op jit(solution)/shard_map/ppermute | solution.py:61
  20.5 0.0 collective-permute-done.2.got_ref
  20.5 1.4 %collective-permute-start.3 = (bf16[264,128]{1,0:T(8,128)(2,1)S(1)}, bf16[264,128]{1,0:T(8,128)(2,1)S(1)}, u32[]{:S(2)}, u32[]{:S(2)}) collective-permute-start(bf16[264,128]{1,0:T(8,128)(2,1)S(1)} %shard_map.141.refs_0_), channel_id=1, source_target_pairs={{0,6},{1,7},{2,4},{3,5},{4,2},{5,3},{6,0},{7,1},{8,14},{9,15},{10,... | collective-permute-start | bytes 202760 | tf_op jit(solution)/shard_map/ppermute | solution.py:89
  21.9 0.8 %collective-permute-done.7.refs_6_ = bf16[2,2,2,8,512]{4,3,2,1,0:T(8,128)(2,1)S(1)} collective-permute-done((bf16[2,2,2,8,512]{4,3,2,1,0:T(8,128)(2,1)S(1)}, bf16[2,2,2,8,512]{4,3,2,1,0:T(8,128)(2,1)S(1)}, u32[]{:S(2)}, u32[]{:S(2)}) %collective-permute-start.7) | collective-permute-done | bytes 65568 | tf_op jit(solution)/shard_map/ppermute | solution.py:61
  22.7 3.0 %collective-permute-start.4 = (bf16[264,128]{1,0:T(8,128)(2,1)S(1)}, bf16[264,128]{1,0:T(8,128)(2,1)S(1)}, u32[]{:S(2)}, u32[]{:S(2)}) collective-permute-start(bf16[264,128]{1,0:T(8,128)(2,1)S(1)} %shard_map.141.refs_0_), channel_id=1, source_target_pairs={{0,2},{1,3},{2,0},{3,1},{4,6},{5,7},{6,4},{7,5},{8,10},{9,11},{10,... | collective-permute-start | bytes 202760 | tf_op jit(solution)/shard_map/ppermute | solution.py:89
  25.7 1.1 %collective-permute-done.3.refs_1_ = bf16[264,128]{1,0:T(8,128)(2,1)S(1)} collective-permute-done((bf16[264,128]{1,0:T(8,128)(2,1)S(1)}, bf16[264,128]{1,0:T(8,128)(2,1)S(1)}, u32[]{:S(2)}, u32[]{:S(2)}) %collective-permute-start.3) | collective-permute-done | bytes 67616 | tf_op jit(solution)/shard_map/ppermute | solution.py:89
  26.8 2.3 %collective-permute-start.5 = (bf16[264,128]{1,0:T(8,128)(2,1)S(1)}, bf16[264,128]{1,0:T(8,128)(2,1)S(1)}, u32[]{:S(2)}, u32[]{:S(2)}) collective-permute-start(bf16[264,128]{1,0:T(8,128)(2,1)S(1)} %shard_map.141.refs_0_), channel_id=1, source_target_pairs={{0,4},{1,5},{2,6},{3,7},{4,0},{5,1},{6,2},{7,3},{8,12},{9,13},{10,... | collective-permute-start | bytes 202760 | tf_op jit(solution)/shard_map/ppermute | solution.py:89
  29.2 0.0 collective-permute-done.4.refs_2_
  29.2 0.0 collective-permute-start.12
  29.2 3.1 %collective-permute-done.5.refs_3_ = bf16[264,128]{1,0:T(8,128)(2,1)S(1)} collective-permute-done((bf16[264,128]{1,0:T(8,128)(2,1)S(1)}, bf16[264,128]{1,0:T(8,128)(2,1)S(1)}, u32[]{:S(2)}, u32[]{:S(2)}) %collective-permute-start.5) | collective-permute-done | bytes 67616 | tf_op jit(solution)/shard_map/ppermute | solution.py:89
  32.3 0.0 collective-permute-done.8.refs_12_
  32.3 0.0 copy-done.2
  32.4 0.6 %shard_map.145 = (bf16[32,1024]{1,0:T(8,128)(2,1)S(1)}, bf16[8,512]{1,0:T(8,128)(2,1)S(1)}, f32[8,512]{1,0:T(8,128)S(1)}) custom-call(bf16[264,128]{1,0:T(8,128)(2,1)S(1)} %shard_map.141.refs_0_, bf16[264,128]{1,0:T(8,128)(2,1)S(1)} %collective-permute-done.3.refs_1_, bf16[264,128]{1,0:T(8,128)(2,1)S(1)} %collective-permute-done.4.refs_2_, ...), custom_call_target="tpu_custom_call" | custom-call | flops 1000000 | bytes 1048576 | tf_op jit(solution)/shard_map/pallas_call | solution.py:21
  33.0 1.6 %collective-permute-start.10 = (bf16[32,1024]{1,0:T(8,128)(2,1)S(1)}, bf16[32,1024]{1,0:T(8,128)(2,1)S(1)}, u32[]{:S(2)}, u32[]{:S(2)}) collective-permute-start(bf16[32,1024]{1,0:T(8,128)(2,1)S(1)} %get-tuple-element.25.refs_0_), channel_id=1, source_target_pairs={{0,16},{1,25},{2,18},{3,27},{4,20},{5,29},{6,22},{7,31},{8,24},{9,... | collective-permute-start | bytes 196616 | tf_op jit(solution)/shard_map/ppermute | solution.py:89
  34.6 1.5 %collective-permute-start.11 = (bf16[32,1024]{1,0:T(8,128)(2,1)S(1)}, bf16[32,1024]{1,0:T(8,128)(2,1)S(1)}, u32[]{:S(2)}, u32[]{:S(2)}) collective-permute-start(bf16[32,1024]{1,0:T(8,128)(2,1)S(1)} %get-tuple-element.25.refs_0_), channel_id=1, source_target_pairs={{0,8},{1,9},{2,10},{3,11},{4,12},{5,13},{6,14},{7,15},{8,0},{9,1},... | collective-permute-start | bytes 196616 | tf_op jit(solution)/shard_map/ppermute | solution.py:89
  36.1 0.0 collective-permute-done.12.refs_7_
  36.1 0.5 collective-permute-start.9
  36.5 0.0 collective-permute-done.13.refs_8_
  36.5 0.0 collective-permute-done.14.refs_9_
  36.5 0.8 %collective-permute-done.10.refs_2_ = bf16[32,1024]{1,0:T(8,128)(2,1)S(1)} collective-permute-done((bf16[32,1024]{1,0:T(8,128)(2,1)S(1)}, bf16[32,1024]{1,0:T(8,128)(2,1)S(1)}, u32[]{:S(2)}, u32[]{:S(2)}) %collective-permute-start.10) | collective-permute-done | bytes 65568 | tf_op jit(solution)/shard_map/ppermute | solution.py:89
  37.3 1.5 %collective-permute-done.11.refs_3_ = bf16[32,1024]{1,0:T(8,128)(2,1)S(1)} collective-permute-done((bf16[32,1024]{1,0:T(8,128)(2,1)S(1)}, bf16[32,1024]{1,0:T(8,128)(2,1)S(1)}, u32[]{:S(2)}, u32[]{:S(2)}) %collective-permute-start.11) | collective-permute-done | bytes 65568 | tf_op jit(solution)/shard_map/ppermute | solution.py:89
  38.8 2.4 %collective-permute-done.9.refs_1_ = bf16[32,1024]{1,0:T(8,128)(2,1)S(1)} collective-permute-done((bf16[32,1024]{1,0:T(8,128)(2,1)S(1)}, bf16[32,1024]{1,0:T(8,128)(2,1)S(1)}, u32[]{:S(2)}, u32[]{:S(2)}) %collective-permute-start.9) | collective-permute-done | bytes 65568 | tf_op jit(solution)/shard_map/ppermute | solution.py:89
  41.2 0.4 shard_map.146
  41.7 2.1 %collective-permute-start.15 = (bf16[264,128]{1,0:T(8,128)(2,1)S(1)}, bf16[264,128]{1,0:T(8,128)(2,1)S(1)}, u32[]{:S(2)}, u32[]{:S(2)}) collective-permute-start(bf16[264,128]{1,0:T(8,128)(2,1)S(1)} %get-tuple-element.26.refs_0_), channel_id=1, source_target_pairs={{0,4},{1,5},{2,6},{3,7},{4,0},{5,1},{6,2},{7,3},{8,12},{9,13},{10,... | collective-permute-start | bytes 202760 | tf_op jit(solution)/shard_map/ppermute | solution.py:89
  43.7 0.2 collective-permute-start.16
  43.9 1.3 %collective-permute-start.17 = (bf16[264,128]{1,0:T(8,128)(2,1)S(1)}, bf16[264,128]{1,0:T(8,128)(2,1)S(1)}, u32[]{:S(2)}, u32[]{:S(2)}) collective-permute-start(bf16[264,128]{1,0:T(8,128)(2,1)S(1)} %get-tuple-element.26.refs_0_), channel_id=1, source_target_pairs={{0,2},{1,3},{2,0},{3,1},{4,6},{5,7},{6,4},{7,5},{8,10},{9,11},{10,... | collective-permute-start | bytes 202760 | tf_op jit(solution)/shard_map/ppermute | solution.py:89
  45.2 1.7 %collective-permute-done.15.refs_1_ = bf16[264,128]{1,0:T(8,128)(2,1)S(1)} collective-permute-done((bf16[264,128]{1,0:T(8,128)(2,1)S(1)}, bf16[264,128]{1,0:T(8,128)(2,1)S(1)}, u32[]{:S(2)}, u32[]{:S(2)}) %collective-permute-start.15) | collective-permute-done | bytes 67616 | tf_op jit(solution)/shard_map/ppermute | solution.py:89
  46.9 2.9 %collective-permute-done.16.refs_2_ = bf16[264,128]{1,0:T(8,128)(2,1)S(1)} collective-permute-done((bf16[264,128]{1,0:T(8,128)(2,1)S(1)}, bf16[264,128]{1,0:T(8,128)(2,1)S(1)}, u32[]{:S(2)}, u32[]{:S(2)}) %collective-permute-start.16) | collective-permute-done | bytes 67616 | tf_op jit(solution)/shard_map/ppermute | solution.py:89
  49.8 0.0 collective-permute-done.17.refs_3_
  49.8 0.5 shard_map.147
  50.3 0.1 collective-permute-start.18
  50.4 0.6 %pad_maximum_fusion = bf16[2,3,8,512]{3,2,1,0:T(8,128)(2,1)} fusion(bf16[1,3,8,512]{3,2,1,0:T(8,128)(2,1)S(1)} %get-tuple-element.40, bf16[1,3,8,512]{3,2,1,0:T(8,128)(2,1)S(1)} %get-tuple-element.39), kind=kLoop, calls=%fused_computation | loop fusion | flops 24576 | bytes 98304 | tf_op jit(solution)/shard_map/stack | solution.py:430
  51.0 0.6 collective-permute-done.18.other_ref
  51.6 0.3 shard_map.148
  51.9 0.8 %collective-permute-start.19 = (bf16[16,512]{1,0:T(8,128)(2,1)S(1)}, bf16[16,512]{1,0:T(8,128)(2,1)S(1)}, u32[]{:S(2)}, u32[]{:S(2)}) collective-permute-start(bf16[16,512]{1,0:T(8,128)(2,1)S(1)} %get-tuple-element.30), channel_id=1, source_target_pairs={{0,24},{1,25},{2,26},{3,27},{4,28},{5,29},{6,30},{7,31},{8,16},{9,... | collective-permute-start | bytes 49160 | tf_op jit(solution)/shard_map/ppermute | solution.py:89
  52.6 1.3 %collective-permute-start.20 = (bf16[16,512]{1,0:T(8,128)(2,1)S(1)}, bf16[16,512]{1,0:T(8,128)(2,1)S(1)}, u32[]{:S(2)}, u32[]{:S(2)}) collective-permute-start(bf16[16,512]{1,0:T(8,128)(2,1)S(1)} %get-tuple-element.31), channel_id=1, source_target_pairs={{0,16},{1,17},{2,18},{3,19},{4,20},{5,21},{6,22},{7,23},{8,24},{9,... | collective-permute-start | bytes 49160 | tf_op jit(solution)/shard_map/ppermute | solution.py:89
  53.9 1.5 %collective-permute-start.21 = (bf16[16,512]{1,0:T(8,128)(2,1)S(1)}, bf16[16,512]{1,0:T(8,128)(2,1)S(1)}, u32[]{:S(2)}, u32[]{:S(2)}) collective-permute-start(bf16[16,512]{1,0:T(8,128)(2,1)S(1)} %get-tuple-element.32), channel_id=1, source_target_pairs={{0,8},{1,9},{2,10},{3,11},{4,12},{5,13},{6,14},{7,15},{8,0},{9,1},... | collective-permute-start | bytes 49160 | tf_op jit(solution)/shard_map/ppermute | solution.py:89
  55.4 0.6 %pad_maximum_fusion.1 = f32[2,8,512]{2,1,0:T(8,128)} fusion(f32[1,8,512]{2,1,0:T(8,128)S(1)} %bitcast.20, f32[1,8,512]{2,1,0:T(8,128)S(1)} %bitcast.19), kind=kLoop, calls=%fused_computation.1 | loop fusion | flops 8192 | bytes 65536 | tf_op jit(solution)/shard_map/stack | solution.py:430
  56.0 0.6 %collective-permute-done.19.refs_0_ = bf16[16,512]{1,0:T(8,128)(2,1)S(1)} collective-permute-done((bf16[16,512]{1,0:T(8,128)(2,1)S(1)}, bf16[16,512]{1,0:T(8,128)(2,1)S(1)}, u32[]{:S(2)}, u32[]{:S(2)}) %collective-permute-start.19) | collective-permute-done | bytes 16416 | tf_op jit(solution)/shard_map/ppermute | solution.py:89
  56.6 0.0 collective-permute-done.20.refs_1_
  56.6 1.0 %collective-permute-done.21.refs_2_ = bf16[16,512]{1,0:T(8,128)(2,1)S(1)} collective-permute-done((bf16[16,512]{1,0:T(8,128)(2,1)S(1)}, bf16[16,512]{1,0:T(8,128)(2,1)S(1)}, u32[]{:S(2)}, u32[]{:S(2)}) %collective-permute-start.21) | collective-permute-done | bytes 16416 | tf_op jit(solution)/shard_map/ppermute | solution.py:89
  57.7 0.6 %shard_map.149 = bf16[16,512]{1,0:T(8,128)(2,1)} custom-call(f32[16,512]{1,0:T(8,128)S(1)} %get-tuple-element.29.own_ref, bf16[16,512]{1,0:T(8,128)(2,1)S(1)} %collective-permute-done.19.refs_0_, bf16[16,512]{1,0:T(8,128)(2,1)S(1)} %collective-permute-done.20.refs_1_, bf16[16,512]{1,0:T(8,128)(2,1)S(1)} %collective-permute-done.21.refs_2_), custom_call_target="tpu_custom_call" | custom-call | flops 1000000 | bytes 1048576 | tf_op jit(solution)/shard_map/pallas_call | solution.py:21
  (22 shorter events, 0.1 us)
Async XLA Ops:
  0.6 1.8 %copy-start = (bf16[2,512,512]{2,1,0:T(8,128)(2,1)S(1)}, bf16[2,512,512]{2,1,0:T(8,128)(2,1)}, u32[]{:S(2)}) copy-start(bf16[2,512,512]{2,1,0:T(8,128)(2,1)} %refs_5_.1) | copy-start | bytes 3145732
  0.6 2.0 %copy-start.1 = (bf16[2,512,512]{2,1,0:T(8,128)(2,1)S(1)}, bf16[2,512,512]{2,1,0:T(8,128)(2,1)}, u32[]{:S(2)}) copy-start(bf16[2,512,512]{2,1,0:T(8,128)(2,1)} %refs_6_.1) | copy-start | bytes 3145732
  1.9 30.5 %collective-permute-start.8 = (bf16[1,512,512]{2,1,0:T(8,128)(2,1)S(1)}, bf16[1,512,512]{2,1,0:T(8,128)(2,1)S(1)}, u32[]{:S(2)}, u32[]{:S(2)}) collective-permute-start(bf16[1,512,512]{2,1,0:T(8,128)(2,1)S(1)} %slice.15), channel_id=1, source_target_pairs={{0,1},{1,0},{2,3},{3,2},{4,5},{5,4},{6,7},{7,6},{8,9},{9,8},{10,11... | collective-permute-start | bytes 1572872 | tf_op jit(solution)/shard_map/ppermute | solution.py:61
  2.5 0.7 %copy-start.10 = (bf16[16,512]{1,0:T(8,128)(2,1)S(1)}, bf16[16,512]{1,0:T(8,128)(2,1)}, u32[]{:S(2)}) copy-start(bf16[16,512]{1,0:T(8,128)(2,1)} %param.12) | copy-start | bytes 49156
  2.5 34.1 %collective-permute-start.13 = (bf16[1,512,512]{2,1,0:T(8,128)(2,1)S(1)}, bf16[1,512,512]{2,1,0:T(8,128)(2,1)S(1)}, u32[]{:S(2)}, u32[]{:S(2)}) collective-permute-start(bf16[1,512,512]{2,1,0:T(8,128)(2,1)S(1)} %slice.16), channel_id=1, source_target_pairs={{0,1},{1,0},{2,3},{3,2},{4,5},{5,4},{6,7},{7,6},{8,9},{9,8},{10,11... | collective-permute-start | bytes 1572872 | tf_op jit(solution)/shard_map/ppermute | solution.py:61
  2.7 33.9 %collective-permute-start.14 = (bf16[1,512,512]{2,1,0:T(8,128)(2,1)S(1)}, bf16[1,512,512]{2,1,0:T(8,128)(2,1)S(1)}, u32[]{:S(2)}, u32[]{:S(2)}) collective-permute-start(bf16[1,512,512]{2,1,0:T(8,128)(2,1)S(1)} %slice.17), channel_id=1, source_target_pairs={{0,1},{1,0},{2,3},{3,2},{4,5},{5,4},{6,7},{7,6},{8,9},{9,8},{10,11... | collective-permute-start | bytes 1572872 | tf_op jit(solution)/shard_map/ppermute | solution.py:61
  3.2 8.3 %copy-start.8 = (f32[2,512]{1,0:T(2,128)S(1)}, f32[2,512]{1,0:T(2,128)}, u32[]{:S(2)}) copy-start(f32[2,512]{1,0:T(2,128)} %refs_4_.1) | copy-start | bytes 12292
  3.2 4.3 %collective-permute-start = (bf16[1,16,512]{2,1,0:T(8,128)(2,1)S(1)}, bf16[1,16,512]{2,1,0:T(8,128)(2,1)S(1)}, u32[]{:S(2)}, u32[]{:S(2)}) collective-permute-start(bf16[1,16,512]{2,1,0:T(8,128)(2,1)S(1)} %bitcast.17), channel_id=1, source_target_pairs={{0,8},{8,0},{16,24},{24,16},{1,9},{9,1},{17,25},{25,17},{2,10},{10... | collective-permute-start | bytes 49160 | tf_op jit(solution)/shard_map/ppermute | solution.py:61
  7.5 3.9 %collective-permute-start.1 = (bf16[2,16,512]{2,1,0:T(8,128)(2,1)S(1)}, bf16[2,16,512]{2,1,0:T(8,128)(2,1)S(1)}, u32[]{:S(2)}, u32[]{:S(2)}) collective-permute-start(bf16[2,16,512]{2,1,0:T(8,128)(2,1)S(1)} %shard_map.139.low_ref), channel_id=1, source_target_pairs={{0,16},{8,24},{16,0},{24,8},{1,17},{9,25},{17,1},{25,9},{2,18},{10... | collective-permute-start | bytes 98312 | tf_op jit(solution)/shard_map/ppermute | solution.py:61
  11.8 0.7 %copy-start.11 = (s32[8]{0:T(128)S(1)}, s32[8]{0:T(128)}, u32[]{:S(2)}) copy-start(s32[8]{0:T(128)} %param.21) | copy-start | bytes 100
  11.8 8.6 %collective-permute-start.2 = (bf16[392,128]{1,0:T(8,128)(2,1)S(1)}, bf16[392,128]{1,0:T(8,128)(2,1)S(1)}, u32[]{:S(2)}, u32[]{:S(2)}) collective-permute-start(bf16[392,128]{1,0:T(8,128)(2,1)S(1)} %get-tuple-element.21), channel_id=1, source_target_pairs={{0,1},{1,0},{2,3},{3,2},{4,5},{5,4},{6,7},{7,6},{8,9},{9,8},{10,11... | collective-permute-start | bytes 301064 | tf_op jit(solution)/shard_map/ppermute | solution.py:61
  12.5 0.8 %copy-start.5 = (bf16[2,3,8,512]{3,2,1,0:T(8,128)(2,1)S(1)}, bf16[2,3,8,512]{3,2,1,0:T(8,128)(2,1)}, u32[]{:S(2)}) copy-start(bf16[2,3,8,512]{3,2,1,0:T(8,128)(2,1)} %conv_ref.1) | copy-start | bytes 147460
  12.5 0.8 %copy-start.6 = (bf16[2,4,512]{2,1,0:T(4,128)(2,1)S(1)}, bf16[2,4,512]{2,1,0:T(4,128)(2,1)}, u32[]{:S(2)}) copy-start(bf16[2,4,512]{2,1,0:T(4,128)(2,1)} %refs_7_.3) | copy-start | bytes 24580
  12.5 0.8 %copy-start.7 = (f32[2,8,512]{2,1,0:T(8,128)S(1)}, f32[2,8,512]{2,1,0:T(8,128)}, u32[]{:S(2)}) copy-start(f32[2,8,512]{2,1,0:T(8,128)} %rec_ref.1) | copy-start | bytes 98308
  12.5 19.9 %copy-start.2 = (bf16[2,512,512]{2,1,0:T(8,128)(2,1)S(1)}, bf16[2,512,512]{2,1,0:T(8,128)(2,1)}, u32[]{:S(2)}) copy-start(bf16[2,512,512]{2,1,0:T(8,128)(2,1)} %w_ref.1) | copy-start | bytes 3145732
  13.3 19.1 %copy-start.3 = (bf16[2,4,128,128]{3,2,1,0:T(8,128)(2,1)S(1)}, bf16[2,4,128,128]{3,2,1,0:T(8,128)(2,1)}, u32[]{:S(2)}) copy-start(bf16[2,4,128,128]{3,2,1,0:T(8,128)(2,1)} %refs_9_.3) | copy-start | bytes 786436
  13.3 19.1 %copy-start.4 = (bf16[2,4,128,128]{3,2,1,0:T(8,128)(2,1)S(1)}, bf16[2,4,128,128]{3,2,1,0:T(8,128)(2,1)}, u32[]{:S(2)}) copy-start(bf16[2,4,128,128]{3,2,1,0:T(8,128)(2,1)} %refs_10_.3) | copy-start | bytes 786436
  13.4 4.0 %collective-permute-start.6 = (bf16[1,2,2,8,512]{4,3,2,1,0:T(8,128)(2,1)S(1)}, bf16[1,2,2,8,512]{4,3,2,1,0:T(8,128)(2,1)S(1)}, u32[]{:S(2)}, u32[]{:S(2)}) collective-permute-start(bf16[1,2,2,8,512]{4,3,2,1,0:T(8,128)(2,1)S(1)} %bitcast.15), channel_id=1, source_target_pairs={{0,2},{1,3},{2,0},{3,1},{4,6},{5,7},{6,4},{7,5},{8,10},{9,11},{10,... | collective-permute-start | bytes 98312 | tf_op jit(solution)/shard_map/ppermute | solution.py:61
  17.4 5.3 %collective-permute-start.7 = (bf16[2,2,2,8,512]{4,3,2,1,0:T(8,128)(2,1)S(1)}, bf16[2,2,2,8,512]{4,3,2,1,0:T(8,128)(2,1)S(1)}, u32[]{:S(2)}, u32[]{:S(2)}) collective-permute-start(bf16[2,2,2,8,512]{4,3,2,1,0:T(8,128)(2,1)S(1)} %shard_map.144.refs_5_), channel_id=1, source_target_pairs={{0,4},{1,5},{2,6},{3,7},{4,0},{5,1},{6,2},{7,3},{8,12},{9,13},{10,... | collective-permute-start | bytes 196616 | tf_op jit(solution)/shard_map/ppermute | solution.py:61
  20.5 11.9 %copy-start.9 = (f32[2,512]{1,0:T(2,128)S(1)}, f32[2,512]{1,0:T(2,128)}, u32[]{:S(2)}) copy-start(f32[2,512]{1,0:T(2,128)} %refs_8_.3) | copy-start | bytes 12292
  20.5 6.4 %collective-permute-start.3 = (bf16[264,128]{1,0:T(8,128)(2,1)S(1)}, bf16[264,128]{1,0:T(8,128)(2,1)S(1)}, u32[]{:S(2)}, u32[]{:S(2)}) collective-permute-start(bf16[264,128]{1,0:T(8,128)(2,1)S(1)} %shard_map.141.refs_0_), channel_id=1, source_target_pairs={{0,6},{1,7},{2,4},{3,5},{4,2},{5,3},{6,0},{7,1},{8,14},{9,15},{10,... | collective-permute-start | bytes 202760 | tf_op jit(solution)/shard_map/ppermute | solution.py:89
  22.7 6.4 %collective-permute-start.4 = (bf16[264,128]{1,0:T(8,128)(2,1)S(1)}, bf16[264,128]{1,0:T(8,128)(2,1)S(1)}, u32[]{:S(2)}, u32[]{:S(2)}) collective-permute-start(bf16[264,128]{1,0:T(8,128)(2,1)S(1)} %shard_map.141.refs_0_), channel_id=1, source_target_pairs={{0,2},{1,3},{2,0},{3,1},{4,6},{5,7},{6,4},{7,5},{8,10},{9,11},{10,... | collective-permute-start | bytes 202760 | tf_op jit(solution)/shard_map/ppermute | solution.py:89
  26.8 5.5 %collective-permute-start.5 = (bf16[264,128]{1,0:T(8,128)(2,1)S(1)}, bf16[264,128]{1,0:T(8,128)(2,1)S(1)}, u32[]{:S(2)}, u32[]{:S(2)}) collective-permute-start(bf16[264,128]{1,0:T(8,128)(2,1)S(1)} %shard_map.141.refs_0_), channel_id=1, source_target_pairs={{0,4},{1,5},{2,6},{3,7},{4,0},{5,1},{6,2},{7,3},{8,12},{9,13},{10,... | collective-permute-start | bytes 202760 | tf_op jit(solution)/shard_map/ppermute | solution.py:89
  29.2 6.9 %collective-permute-start.12 = (f32[2,512]{1,0:T(2,128)S(1)}, f32[2,512]{1,0:T(2,128)S(1)}, u32[]{:S(2)}, u32[]{:S(2)}) collective-permute-start(f32[2,512]{1,0:T(2,128)S(1)} %copy-done.8), channel_id=1, source_target_pairs={{0,1},{1,0},{2,3},{3,2},{4,5},{5,4},{6,7},{7,6},{8,9},{9,8},{10,11... | collective-permute-start | bytes 12296 | tf_op jit(solution)/shard_map/ppermute | solution.py:61
  33.0 4.3 %collective-permute-start.10 = (bf16[32,1024]{1,0:T(8,128)(2,1)S(1)}, bf16[32,1024]{1,0:T(8,128)(2,1)S(1)}, u32[]{:S(2)}, u32[]{:S(2)}) collective-permute-start(bf16[32,1024]{1,0:T(8,128)(2,1)S(1)} %get-tuple-element.25.refs_0_), channel_id=1, source_target_pairs={{0,16},{1,25},{2,18},{3,27},{4,20},{5,29},{6,22},{7,31},{8,24},{9,... | collective-permute-start | bytes 196616 | tf_op jit(solution)/shard_map/ppermute | solution.py:89
  34.6 4.3 %collective-permute-start.11 = (bf16[32,1024]{1,0:T(8,128)(2,1)S(1)}, bf16[32,1024]{1,0:T(8,128)(2,1)S(1)}, u32[]{:S(2)}, u32[]{:S(2)}) collective-permute-start(bf16[32,1024]{1,0:T(8,128)(2,1)S(1)} %get-tuple-element.25.refs_0_), channel_id=1, source_target_pairs={{0,8},{1,9},{2,10},{3,11},{4,12},{5,13},{6,14},{7,15},{8,0},{9,1},... | collective-permute-start | bytes 196616 | tf_op jit(solution)/shard_map/ppermute | solution.py:89
  36.1 5.2 %collective-permute-start.9 = (bf16[32,1024]{1,0:T(8,128)(2,1)S(1)}, bf16[32,1024]{1,0:T(8,128)(2,1)S(1)}, u32[]{:S(2)}, u32[]{:S(2)}) collective-permute-start(bf16[32,1024]{1,0:T(8,128)(2,1)S(1)} %get-tuple-element.25.refs_0_), channel_id=1, source_target_pairs={{0,24},{1,17},{2,26},{3,19},{4,28},{5,21},{6,30},{7,23},{8,16},{9,... | collective-permute-start | bytes 196616 | tf_op jit(solution)/shard_map/ppermute | solution.py:89
  41.7 5.2 %collective-permute-start.15 = (bf16[264,128]{1,0:T(8,128)(2,1)S(1)}, bf16[264,128]{1,0:T(8,128)(2,1)S(1)}, u32[]{:S(2)}, u32[]{:S(2)}) collective-permute-start(bf16[264,128]{1,0:T(8,128)(2,1)S(1)} %get-tuple-element.26.refs_0_), channel_id=1, source_target_pairs={{0,4},{1,5},{2,6},{3,7},{4,0},{5,1},{6,2},{7,3},{8,12},{9,13},{10,... | collective-permute-start | bytes 202760 | tf_op jit(solution)/shard_map/ppermute | solution.py:89
  43.7 6.1 %collective-permute-start.16 = (bf16[264,128]{1,0:T(8,128)(2,1)S(1)}, bf16[264,128]{1,0:T(8,128)(2,1)S(1)}, u32[]{:S(2)}, u32[]{:S(2)}) collective-permute-start(bf16[264,128]{1,0:T(8,128)(2,1)S(1)} %get-tuple-element.26.refs_0_), channel_id=1, source_target_pairs={{0,6},{1,7},{2,4},{3,5},{4,2},{5,3},{6,0},{7,1},{8,14},{9,15},{10,... | collective-permute-start | bytes 202760 | tf_op jit(solution)/shard_map/ppermute | solution.py:89
  43.9 5.9 %collective-permute-start.17 = (bf16[264,128]{1,0:T(8,128)(2,1)S(1)}, bf16[264,128]{1,0:T(8,128)(2,1)S(1)}, u32[]{:S(2)}, u32[]{:S(2)}) collective-permute-start(bf16[264,128]{1,0:T(8,128)(2,1)S(1)} %get-tuple-element.26.refs_0_), channel_id=1, source_target_pairs={{0,2},{1,3},{2,0},{3,1},{4,6},{5,7},{6,4},{7,5},{8,10},{9,11},{10,... | collective-permute-start | bytes 202760 | tf_op jit(solution)/shard_map/ppermute | solution.py:89
  50.3 1.3 %collective-permute-start.18 = (bf16[40,512]{1,0:T(8,128)(2,1)S(1)}, bf16[40,512]{1,0:T(8,128)(2,1)S(1)}, u32[]{:S(2)}, u32[]{:S(2)}) collective-permute-start(bf16[40,512]{1,0:T(8,128)(2,1)S(1)} %get-tuple-element.28.own_ref), channel_id=1, source_target_pairs={{0,1},{1,0},{2,3},{3,2},{4,5},{5,4},{6,7},{7,6},{8,9},{9,8},{10,11... | collective-permute-start | bytes 122888 | tf_op jit(solution)/shard_map/ppermute | solution.py:61
  51.9 4.8 %collective-permute-start.19 = (bf16[16,512]{1,0:T(8,128)(2,1)S(1)}, bf16[16,512]{1,0:T(8,128)(2,1)S(1)}, u32[]{:S(2)}, u32[]{:S(2)}) collective-permute-start(bf16[16,512]{1,0:T(8,128)(2,1)S(1)} %get-tuple-element.30), channel_id=1, source_target_pairs={{0,24},{1,25},{2,26},{3,27},{4,28},{5,29},{6,30},{7,31},{8,16},{9,... | collective-permute-start | bytes 49160 | tf_op jit(solution)/shard_map/ppermute | solution.py:89
  52.6 4.0 %collective-permute-start.20 = (bf16[16,512]{1,0:T(8,128)(2,1)S(1)}, bf16[16,512]{1,0:T(8,128)(2,1)S(1)}, u32[]{:S(2)}, u32[]{:S(2)}) collective-permute-start(bf16[16,512]{1,0:T(8,128)(2,1)S(1)} %get-tuple-element.31), channel_id=1, source_target_pairs={{0,16},{1,17},{2,18},{3,19},{4,20},{5,21},{6,22},{7,23},{8,24},{9,... | collective-permute-start | bytes 49160 | tf_op jit(solution)/shard_map/ppermute | solution.py:89
  53.9 3.7 %collective-permute-start.21 = (bf16[16,512]{1,0:T(8,128)(2,1)S(1)}, bf16[16,512]{1,0:T(8,128)(2,1)S(1)}, u32[]{:S(2)}, u32[]{:S(2)}) collective-permute-start(bf16[16,512]{1,0:T(8,128)(2,1)S(1)} %get-tuple-element.32), channel_id=1, source_target_pairs={{0,8},{1,9},{2,10},{3,11},{4,12},{5,13},{6,14},{7,15},{8,0},{9,1},... | collective-permute-start | bytes 49160 | tf_op jit(solution)/shard_map/ppermute | solution.py:89
